TPU v7x, 32 devices: a whole 2x2x4 slice. The times are simulated.
32 devices in a mesh: sp: 8 (over z, x), tp: 4 (over y, core).
Axes of the slice: x: 2, y: 2, z: 4, core: 2. Of those that a mesh axis runs over, the one named last changes fastest.
Arguments:
- probe_vectors: bfloat16 [1024, 2048], P('sp', 'tp'), may hold values from -6 to 6
- address_vectors: bfloat16 [1024, 2048], P('sp', 'tp'), may hold values from -6 to 6
- content_vectors: bfloat16 [1024, 2048], P('sp', 'tp'), may hold values from -6 to 6
- storage_raw_signal: float32 [16, 1024], P('tp', 'sp'), may hold values from -8 to 4
- fade_raw_signal: float32 [16, 1024], P('tp', 'sp'), may hold values from -6 to 6
- channel_fade_exponent: float32 [16], P('tp'), may hold values from -9 to 0
- extra_fade_amount: float32 [16, 1024], P('tp', 'sp'), may hold values from -1 to 0
- sequence_label: int32 [1024], P('sp'), may hold values from 0 to 2, never falling along the last dimension, each value on 1 to 768 neighbouring positions
- exit_valve_raw_signal: bfloat16 [1024, 2048], P('sp', 'tp'), may hold values from -6 to 6
- final_projection_matrix: bfloat16 [2048, 2048], P('tp'), may hold values from -0.125 to 0.125
- incoming_rows_matrix: bfloat16 [1024, 2048], P('sp', 'tp'), may hold values from -48 to 48
- initial_rescale_factor: float32 [2048], P('tp'), may hold values from 0 to 3
- specialist_picks: int32 [1024, 2], P('sp'), may hold values from 0 to 7, all different within a row; in each aligned block of 128 rows (0 to 127, 128 to 255, ...) at most 36 rows name the same one
- picked_specialist_share: bfloat16 [1024, 2], P('sp'), may hold values from 0.29882812 to 1.1953125
- specialist_valve_matrix: bfloat16 [8, 2048, 4096], P('sp', None, 'tp'), may hold values from -0.125 to 0.125
- specialist_raising_matrix: bfloat16 [8, 2048, 4096], P('sp', None, 'tp'), may hold values from -0.125 to 0.125
- specialist_lowering_matrix: bfloat16 [8, 4096, 2048], P('sp', 'tp'), may hold values from -0.09375 to 0.09375
- common_valve_matrix: bfloat16 [2048, 512], P(None, 'tp'), may hold values from -0.125 to 0.125
- common_raising_matrix: bfloat16 [2048, 512], P(None, 'tp'), may hold values from -0.125 to 0.125
- common_lowering_matrix: bfloat16 [512, 2048], P('tp'), may hold values from -0.25 to 0.25
- latter_rescale_factor: float32 [2048], P('tp'), may hold values from 0.1 to 1.9
Outputs:
- result: bfloat16 [1024, 2048], P('sp', 'tp')
Inputs may be any that keep to these rules, and one draw needn't show every extreme that they name: `sequence_label`: document numbers never fall; a document has 1 to 768 positions, one exactly 768. `specialist_picks`: each row names 2 different experts; among the rows of one index of sp no expert is named more than 36 times, a bound that some block reaches.
All inputs are finite; a program needn't handle non-finite values.
Results may differ from a plain program's by a relative error of at most 0.018.
Values may be sent and summed in bfloat16 or wider, within the bound.
No kernel may reach another device: no remote copies, remote signals or barrier semaphores. Data moves between devices by JAX's collectives and lax.ppermute only.
A program may use at most 64 MiB of HBM per device.

v0:
```python
import functools

import jax
import jax.numpy as jnp
from jax import lax
from jax.experimental import pallas as pl
from jax.experimental.pallas import tpu as pltpu
from jax.sharding import PartitionSpec as P


DK = 128
DV = 128
ALPHA = 2.0**0.25
F32 = jnp.float32
BF16 = jnp.bfloat16


def dot(left, right, contract=((1,), (0,))):
    return lax.dot_general(left, right, (contract, ((), ())), preferred_element_type=F32)


def split(array):
    high = array.astype(BF16)
    return high, (array - high.astype(F32)).astype(BF16)


def dot3(left, right):
    left_high, left_low = split(left)
    right_high, right_low = split(right)
    return dot(left_high, right_high) + (dot(left_high, right_low) + dot(left_low, right_high))


def dot_left(left, right):
    high, low = split(left)
    return dot(high, right) + dot(low, right)


def triangular_inverses(lowers, rows, cols):
    size = lowers[0].shape[0]
    identity = jnp.where(rows == cols, 1.0, 0.0)

    def once(left, right):
        return dot(left.astype(BF16), right.astype(BF16))

    def solve(powers, inverses, ratio, block):
        if block == 1:
            inverses = [x - p for p, x in zip(powers, inverses)]
            if ratio > 2:
                powers = [once(p, p) for p in powers]
        elif ratio > 2:
            both = [once(p, jnp.concatenate([p, x], 1)) for p, x in zip(powers, inverses)]
            powers = [pair[:, :size] for pair in both]
            inverses = [x - pair[:, size:] for pair, x in zip(both, inverses)]
        else:
            return [x - once(p, x) for p, x in zip(powers, inverses)]
        if ratio > 2:
            inverses = [x + once(p, x) for p, x in zip(powers, inverses)]
        return inverses

    inverses = [identity for _ in lowers]
    block = 1
    while block < size:
        ratio = min(4, size // block)
        wide = block * ratio
        inside = (rows // wide == cols // wide) & (rows // block != cols // block)
        parts = [jnp.where(inside, lower, 0.0) for lower in lowers]
        if block > 1:
            parts = [once(x, part) for x, part in zip(inverses, parts)]
        inverses = solve(parts, inverses, ratio, block)
        block = wide
    errors = [(identity - x) - dot3(lower, x) for lower, x in zip(lowers, inverses)]
    return [x + once(x, error) for x, error in zip(inverses, errors)]


def delta_kernel(*refs):
    q_ref, k_ref, v_ref, store_ref, fade_ref, extra_ref, rate_ref, label_ref, ms_ref, local_ref, query_ref = refs
    length = q_ref.shape[0]
    heads = store_ref.shape[0]
    every = range(heads)
    rows = lax.broadcasted_iota(jnp.int32, (length, length), 0)
    cols = lax.broadcasted_iota(jnp.int32, (length, length), 1)
    diagonal = rows == cols
    lower = rows >= cols
    strict = rows > cols
    identity = jnp.where(diagonal, 1.0, 0.0)

    def to_col(row):
        return jnp.sum(jnp.where(diagonal, row, 0.0), 1, keepdims=True)

    def to_row(col):
        return jnp.sum(jnp.where(diagonal, col, 0.0), 0, keepdims=True)

    label_row = label_ref[...].astype(F32)
    label_col = to_col(label_row)
    first = label_col[:1]
    last = label_col[length - 1 :]
    same = lower & (label_col == label_row)
    carried = jnp.where(label_col == first, 1.0, 0.0)
    closing = jnp.where(label_col == last, 1.0, 0.0)
    through = jnp.where(first == last, 1.0, 0.0)
    fade = fade_ref[...]
    soft = jnp.maximum(fade, 0.0) + jnp.log(1.0 + jnp.exp(-jnp.abs(fade)))
    gates = 1.0 / (1.0 + jnp.exp(-store_ref[...]))
    extra = extra_ref[...]
    rates = rate_ref[...]
    at = [slice(h * DK, (h + 1) * DK) for h in every]
    queries = [q_ref[:, at[h]] for h in every]
    keys = [k_ref[:, at[h]] for h in every]
    values = [v_ref[:, at[h]] for h in every]

    def scale_of(array):
        wide = array.astype(F32)
        return lax.rsqrt(jnp.sum(wide * wide, 1, keepdims=True) + 1e-06)

    key_scales = [scale_of(key) for key in keys]
    query_scales = [scale_of(query) * DK ** (-0.5) for query in queries]
    products = [dot(key, key, ((1,), (1,))) for key in keys]
    scores = [dot(query, key, ((1,), (1,))) for query, key in zip(queries, keys)]
    gate_rows = [gates[h : h + 1] for h in every]
    gate_cols = [to_col(gate_rows[h]) for h in every]
    decays = [
        extra[h : h + 1] - jnp.exp(rates[:, h : h + 1]) * soft[h : h + 1] for h in every
    ]
    totals = [jnp.sum(jnp.where(lower, decay, 0.0), 1, keepdims=True) for decay in decays]
    ends = [total[length - 1 :] for total in totals]
    reaches = [
        jnp.where(same, jnp.exp(jnp.where(lower, total - to_row(total), 0.0)), 0.0) for total in totals
    ]
    growths = [jnp.exp(total) * carried for total in totals]
    reaches = [reaches[h] * to_row(key_scales[h]) for h in every]
    couplings = [
        jnp.where(strict, products[h] * (key_scales[h] * gate_cols[h]) * reaches[h], 0.0) for h in every
    ]
    scores = [(scores[h] * query_scales[h] * reaches[h]).astype(BF16) for h in every]
    inverses = triangular_inverses(couplings, rows, cols)
    fresh = [dot_left(inverses[h] * gate_rows[h], values[h]) for h in every]
    erase = [
        dot_left(inverses[h] * to_row(gate_cols[h] * key_scales[h] * growths[h]), keys[h]) for h in every
    ]
    both = [jnp.concatenate([fresh[h], erase[h]], 1) for h in every]
    tails = [key_scales[h] * jnp.exp(ends[h] - totals[h]) * closing for h in every]
    carries = [dot(keys[h], (both[h] * tails[h]).astype(BF16), ((0,), (0,))) for h in every]
    seen = [dot(scores[h], both[h].astype(BF16)) for h in every]
    for h in every:
        final = jnp.exp(ends[h]) * through
        ms_ref[h, :DK] = (final * identity[:DK, :DK] - carries[h][:, DV:]).astype(BF16)
        ms_ref[h, DK : DK + DK] = carries[h][:, :DV].astype(BF16)
        ms_ref[h, DK + DK : DK + DK + 8] = jnp.broadcast_to(first, (8, DV)).astype(BF16)
        ms_ref[h, DK + DK + 8 :] = jnp.broadcast_to(last, (8, DV)).astype(BF16)
        local_ref[:, at[h]] = seen[h][:, :DV]
        query_ref[:, at[h]] = queries[h].astype(F32) * (query_scales[h] * growths[h]) - seen[h][:, DV:]


def first_label(ms_ref, j):
    return ms_ref[j, DK + DK : DK + DK + 8].astype(F32)[:1]


def last_label(ms_ref, j):
    return ms_ref[j, DK + DK + 8 :].astype(F32)[:1]


def fold_kernel(ms_ref, state_ref, map_ref, leaving_ref):
    blocks = ms_ref.shape[0]
    for j in range(blocks):
        onto = ms_ref[j, :DK]
        add = ms_ref[j, DK : DK + DK].astype(F32)
        if j == 0:
            state = add
            reach = onto.astype(F32)
        else:
            joined = jnp.where(first_label(ms_ref, j) == last_label(ms_ref, j - 1), 1.0, 0.0)
            state = state * joined
            reach = (reach * joined).astype(BF16)
            state_ref[j - 1] = state
            map_ref[j - 1] = reach
            high, low = split(state)
            moved = dot(onto, jnp.concatenate([high, low, reach], 1))
            state = moved[:, :DV] + moved[:, DV : DV + DV] + add
            reach = moved[:, DV + DV :]
    state_ref[blocks - 1] = state
    map_ref[blocks - 1] = reach.astype(BF16)
    leaving_ref[:DK] = state.astype(BF16)
    leaving_ref[DK:] = ms_ref[blocks - 1, DK + DK :]


def enter_kernel(got_ref, ms_ref, state_ref, map_ref, entering_ref):
    blocks = ms_ref.shape[0]
    last = got_ref[DK + 8 :].astype(F32)[:1]
    joined = jnp.where(first_label(ms_ref, 0) == last, 1.0, 0.0)
    state = (got_ref[:DK].astype(F32) * joined).astype(BF16)
    entering_ref[0] = state
    for j in range(1, blocks):
        entering_ref[j] = (state_ref[j - 1] + dot(map_ref[j - 1], state)).astype(BF16)


def leave_kernel(got_ref, ms_ref, state_ref, map_ref, leaving_ref):
    blocks = ms_ref.shape[0]
    last = got_ref[DK + 8 :].astype(F32)[:1]
    joined = jnp.where(first_label(ms_ref, 0) == last, 1.0, 0.0)
    state = (got_ref[:DK].astype(F32) * joined).astype(BF16)
    leaving_ref[:DK] = (state_ref[blocks - 1] + dot(map_ref[blocks - 1], state)).astype(BF16)
    leaving_ref[DK:] = ms_ref[blocks - 1, DK + DK :]


def project_kernel(place_ref, local_ref, query_ref, state_ref, valve_ref, weight_ref, *out_refs):
    heads = state_ref.shape[0]
    pieces = []
    for h in range(heads):
        at = slice(h * DV, (h + 1) * DV)
        mixed = local_ref[:, at] + dot_left(query_ref[:, at], state_ref[h])
        scaled = mixed * lax.rsqrt(jnp.mean(mixed * mixed, 1, keepdims=True) + 1e-06)
        valve = valve_ref[:, at].astype(F32)
        pieces.append((scaled * (valve / (1.0 + jnp.exp(-valve)))).astype(BF16))
    heads_out = jnp.concatenate(pieces, 1) if heads > 1 else pieces[0]
    width = out_refs[0].shape[1]
    for offset in range(len(out_refs) - 1, -1, -1):
        start = pl.multiple_of((place_ref[0] ^ offset) * width, width)
        out_refs[offset][...] = dot(heads_out, weight_ref[:, pl.ds(start, width)]).astype(BF16)


def silu(array):
    return array / (1.0 + jnp.exp(-array))


def join_pairs(place_ref, piece_refs, row_refs):
    width = piece_refs[0].shape[1]
    odd = place_ref[0] & 1
    for pair, row_ref in enumerate(row_refs):
        row_ref[:, pl.ds(pl.multiple_of(odd * width, width), width)] = piece_refs[2 * pair][...]
        row_ref[:, pl.ds(pl.multiple_of((1 - odd) * width, width), width)] = piece_refs[2 * pair + 1][...]


def products(place_ref, offsets, row_refs, weights):
    result = None
    for pair, row_ref in enumerate(row_refs):
        wide = row_ref.shape[1]
        start = pl.multiple_of(((place_ref[0] ^ offsets[2 * pair]) // 2) * wide, wide)
        term = dot(row_ref[...], weights(pl.ds(start, wide)))
        result = term if result is None else result + term
    return result


def expert_kernel(offsets, others, step, slots, capacity, *refs):
    place_ref = refs[0]
    count = len(offsets)
    pairs = count // 2
    piece_refs = refs[1 : 1 + count]
    valve_ref, raise_ref, cv_ref, cr_ref = refs[1 + count : 5 + count]
    refs = refs[5 + count :]
    row_refs = refs[len(refs) - pairs :]
    join_pairs(place_ref, piece_refs, row_refs)
    first = others == 0
    if first:
        gate_ref, lift_ref, cgate_ref, clift_ref = refs[:4]
    else:
        own_ref, gate_ref, lift_ref, cgate_ref, clift_ref, lower_ref, cl_ref = refs[:7]
        out_refs = refs[7 : 7 + others]
        hidden_ref, shared_ref = refs[7 + others : 9 + others]
        rows = lax.broadcasted_iota(jnp.int32, (slots, 128), 0)
        cols = lax.broadcasted_iota(jnp.int32, (slots, 128), 1)
        base = capacity // 8 * 8
        shares = []
        for source in range(own_ref.shape[0] // slots):
            info = own_ref[source * slots + base : source * slots + base + 8, :].astype(F32)
            info = info[capacity - base : capacity - base + 1]
            shares.append(jnp.sum(jnp.where(rows == cols, info[:, :128], 0.0), 1, keepdims=True))
        share = jnp.concatenate(shares, 0)

    cgate = products(place_ref, offsets, row_refs, lambda at: cv_ref[at, :])
    clift = products(place_ref, offsets, row_refs, lambda at: cr_ref[at, :])
    if first:
        cgate_ref[...] = cgate
        clift_ref[...] = clift
    else:
        flag = jnp.where(share < 0.0, 1.0, 0.0)
        shared_ref[...] = (silu(cgate_ref[...] + cgate) * (clift_ref[...] + clift) * flag).astype(BF16)
        share = jnp.abs(share)

    def chunk(i, _):
        cut = pl.ds(pl.multiple_of(i * step, step), step)
        gate = products(place_ref, offsets, row_refs, lambda at: valve_ref[0, at, cut])
        lift = products(place_ref, offsets, row_refs, lambda at: raise_ref[0, at, cut])
        if first:
            gate_ref[:, cut] = gate
            lift_ref[:, cut] = lift
        else:
            hidden_ref[:, cut] = (silu(gate_ref[:, cut] + gate) * (lift_ref[:, cut] + lift) * share).astype(BF16)
        return 0

    lax.fori_loop(0, valve_ref.shape[2] // step, chunk, 0)
    if not first:
        width = piece_refs[0].shape[1]
        for offset in range(others - 1, -1, -1):
            cut = pl.ds(pl.multiple_of((place_ref[0] ^ offset) * width, width), width)
            term = dot(hidden_ref[...], lower_ref[0, :, cut]) + dot(shared_ref[...], cl_ref[:, cut])
            out_refs[offset][...] = term.astype(BF16)


def swap(array, axis, bit):
    size = lax.axis_size(axis)
    return lax.ppermute(array, axis, [(i, i ^ bit) for i in range(size)])


def scatter_sum(blocks, axis):
    bit = 1
    while len(blocks) > 1:
        kept = {}
        for k in range(len(blocks) - 1, 0, -2):
            got = swap(blocks[k].astype(BF16), axis, bit)
            kept[k // 2] = blocks[k - 1].astype(F32) + got.astype(F32)
        blocks = [kept[k] for k in range(len(blocks) // 2)]
        bit *= 2
    return blocks[0].astype(F32)


def sum_all(array, axis):
    bit = 1
    while bit < lax.axis_size(axis):
        array = array + swap(array, axis, bit)
        bit *= 2
    return array


def gather_pieces(array, axis):
    size = lax.axis_size(axis)
    pieces = {0: array}
    bit = size // 2
    while bit:
        for k, piece in list(pieces.items()):
            pieces[k ^ bit] = swap(piece, axis, bit)
        bit //= 2
    return pieces


def feature_norm(summed, gain):
    width = summed.shape[-1] * lax.axis_size("tp")
    sums = sum_all(jnp.stack([jnp.sum(summed, -1), jnp.sum(summed * summed, -1)]), "tp")
    row_mean = sums[0] / width
    row_var = sums[1] / width - row_mean * row_mean
    return (summed - row_mean[:, None]) * lax.rsqrt(row_var[:, None] + 1e-05) * gain


def call(kernel, outs, *args, in_specs=None, out_specs=None, limit=12, flops=4 * 10**9, **kw):
    shapes = [jax.ShapeDtypeStruct(shape, kind) for shape, kind in outs]
    moved = sum(array.size * array.dtype.itemsize for array in args)
    return pl.pallas_call(
        kernel,
        out_shape=shapes,
        in_specs=in_specs or [vmem()] * len(args),
        out_specs=out_specs or [vmem()] * len(outs),
        compiler_params=pltpu.CompilerParams(vmem_limit_bytes=limit * 1024 * 1024),
        cost_estimate=pl.CostEstimate(flops=flops, bytes_accessed=moved, transcendentals=0),
        **kw,
    )(*args)


def smem():
    return pl.BlockSpec(memory_space=pltpu.SMEM)


def vmem():
    return pl.BlockSpec(memory_space=pltpu.VMEM)


def shards(
    probe_vectors,
    address_vectors,
    content_vectors,
    storage_raw_signal,
    fade_raw_signal,
    channel_fade_exponent,
    extra_fade_amount,
    sequence_label,
    exit_valve_raw_signal,
    final_projection_matrix,
    incoming_rows_matrix,
    initial_rescale_factor,
    specialist_picks,
    picked_specialist_share,
    specialist_valve_matrix,
    specialist_raising_matrix,
    specialist_lowering_matrix,
    common_valve_matrix,
    common_raising_matrix,
    common_lowering_matrix,
    latter_rescale_factor,
):
    tokens, width = incoming_rows_matrix.shape
    heads = storage_raw_signal.shape[0]
    n_sp = lax.axis_size("sp")
    n_tp = lax.axis_size("tp")

    place = lax.axis_index("tp").astype(jnp.int32)[None]

    inputs = (
        probe_vectors,
        address_vectors,
        content_vectors,
        storage_raw_signal,
        fade_raw_signal,
        extra_fade_amount,
        channel_fade_exponent[None, :],
        sequence_label[None, :],
    )
    shapes = [((heads, DK + DK + 16, DV), BF16), ((tokens, heads * DV), F32), ((tokens, heads * DK), F32)]

    def one_step(shape):
        return pl.BlockSpec(shape, lambda i: (0,) * len(shape))

    ms, local, query = call(
        delta_kernel,
        shapes,
        *inputs,
        grid=(1,),
        in_specs=[one_step(array.shape) for array in inputs],
        out_specs=[one_step(shape) for shape, _ in shapes],
        limit=61,
        flops=2 * 10**9,
    )

    groups = [[s * heads + i for i in range(heads)] for s in range(n_sp // heads)]

    def exchange(blocks):
        if heads == 1:
            return blocks
        return lax.all_to_all(blocks, "sp", 0, 0, axis_index_groups=groups, tiled=True)

    mine = exchange(ms)
    states, maps, leaving = call(
        fold_kernel,
        [((heads, DK, DV), F32), ((heads, DK, DK), BF16), ((DK + 16, DV), BF16)],
        mine,
    )
    onward = [(i, i + heads) for i in range(n_sp - heads)]

    def hop(_, leaving):
        got = lax.ppermute(leaving, "sp", onward)
        return call(leave_kernel, [((DK + 16, DV), BF16)], got, mine, states, maps)[0]

    segments = n_sp // heads
    if segments > 2:
        leaving = lax.fori_loop(0, segments - 2, hop, leaving)
    got = lax.ppermute(leaving, "sp", onward)
    (entering,) = call(enter_kernel, [((heads, DK, DV), BF16)], got, mine, states, maps)
    entering = exchange(entering)

    partial = call(
        project_kernel,
        [((tokens, width), BF16)] * n_tp,
        place,
        local,
        query,
        entering,
        exit_valve_raw_signal,
        final_projection_matrix,
        in_specs=[smem()] + [vmem()] * 5,
    )
    projected = scatter_sum(partial, "tp")
    middle = feature_norm(
        ALPHA * incoming_rows_matrix.astype(F32) + projected, initial_rescale_factor
    ).astype(BF16)

    top = specialist_picks.shape[1]
    experts = specialist_valve_matrix.shape[0] * n_sp
    capacity = max(2, 9 * tokens * top // (8 * experts))
    slots = (capacity + 8) // 8 * 8
    named = specialist_picks.T[:, None, :] == jnp.arange(experts, dtype=jnp.int32)[None, :, None]
    taken = jnp.any(named, 0)
    earlier = jnp.arange(tokens)[:, None] < jnp.arange(tokens)[None, :]
    rank = jnp.dot(taken.astype(BF16), earlier.astype(BF16), preferred_element_type=F32)
    slot_index = jnp.arange(slots, dtype=jnp.int32)
    chosen = taken[:, None, :] & (rank.astype(jnp.int32)[:, None, :] == slot_index[None, :, None])
    chosen = chosen & (slot_index < capacity)[None, :, None]
    pick = chosen.astype(BF16).reshape(experts * slots, tokens)
    share = picked_specialist_share.astype(F32).T[:, None, :]
    sign = jnp.where(jnp.arange(top) == 0, -1.0, 1.0)[:, None, None]
    signed = jnp.sum(jnp.where(named, share * sign, 0.0), 0)
    slot_share = jnp.sum(jnp.where(chosen, signed[:, None, :], 0.0), 2)
    lane = jnp.arange(width, dtype=jnp.int32)
    info = jnp.pad(slot_share, ((0, 0), (0, width - slots)))
    info = jnp.where((slot_index == capacity)[None, :, None], info[:, None, :], 0.0)
    sent = jnp.dot(pick, middle, preferred_element_type=F32).reshape(experts, slots, width)
    sent = (sent + info).astype(BF16)
    arrived = lax.all_to_all(sent, "sp", 0, 0, tiled=True).reshape(experts * slots, width)

    by_offset = gather_pieces(arrived, "tp")
    hidden = specialist_valve_matrix.shape[2]
    shared = common_valve_matrix.shape[1]
    total = experts * slots
    step = min(hidden, 256)
    weights = (specialist_valve_matrix, specialist_raising_matrix, common_valve_matrix, common_raising_matrix)
    work = 4 * total * width * (hidden + shared)
    near, far = list(range(2)), list(range(2, n_tp))
    partial = call(
        functools.partial(expert_kernel, near, 0, step, slots, capacity),
        [((total, hidden), F32)] * 2 + [((total, shared), F32)] * 2,
        place,
        *[by_offset[k] for k in near],
        *weights,
        in_specs=[smem()] + [vmem()] * 6,
        scratch_shapes=[pltpu.VMEM((total, 2 * width), BF16)],
        flops=work * 2,
    )
    results = call(
        functools.partial(expert_kernel, far, n_tp, step, slots, capacity),
        [((total, width), BF16)] * n_tp,
        place,
        *[by_offset[k] for k in far],
        *weights,
        arrived,
        *partial,
        specialist_lowering_matrix,
        common_lowering_matrix,
        in_specs=[smem()] + [vmem()] * (n_tp + 9),
        scratch_shapes=[pltpu.VMEM((total, hidden), BF16), pltpu.VMEM((total, shared), BF16)]
        + [pltpu.VMEM((total, 2 * width), BF16)] * (n_tp // 2 - 1),
        flops=work * n_tp,
    )
    summed = scatter_sum(results, "tp").astype(BF16).reshape(experts, slots, width)
    returned = lax.all_to_all(summed, "sp", 0, 0, tiled=True).reshape(total, width)
    mixture = lax.dot_general(
        pick, returned, (((0,), (0,)), ((), ())), preferred_element_type=F32
    )
    second_sum = ALPHA * middle.astype(F32) + mixture
    return feature_norm(second_sum, latter_rescale_factor).astype(BF16)


def solution(mesh):
    placed = (
        P("sp", "tp"),
        P("sp", "tp"),
        P("sp", "tp"),
        P("tp", "sp"),
        P("tp", "sp"),
        P("tp"),
        P("tp", "sp"),
        P("sp"),
        P("sp", "tp"),
        P("tp", None),
        P("sp", "tp"),
        P("tp"),
        P("sp", None),
        P("sp", None),
        P("sp", None, "tp"),
        P("sp", None, "tp"),
        P("sp", "tp", None),
        P(None, "tp"),
        P(None, "tp"),
        P("tp", None),
        P("tp"),
    )

    return jax.shard_map(shards, mesh=mesh, in_specs=placed, out_specs=P("sp", "tp"), check_vma=False)
```

profile of v0, /device:TPU:0, one launch (start us, length us, event | category | flops | bytes accessed | tf_op | source)
XLA Modules:
  0.0 108.3 jit_solution(11264154711154296092)
XLA Ops:
  0.0 4.7 %shard_map.199 = (bf16[4,272,128]{2,1,0:T(8,128)(2,1)}, f32[128,512]{1,0:T(8,128)}, f32[128,512]{1,0:T(8,128)}) custom-call(bf16[128,512]{1,0:T(8,128)(2,1)} %refs_0_.1, bf16[128,512]{1,0:T(8,128)(2,1)} %refs_1_.1, bf16[128,512]{1,0:T(8,128)(2,1)} %refs_2_.1, f32[4,128]{1,0:T(4,128)} %refs_3_.3, f32[4,128]{1,0:T(4,128)} %refs_4_.3, f32[4,128]{1,0:T(4,128)} %refs_5_.3, ...), custom_call_target="tpu_custom_call" | custom-call | flops 2000000000 | bytes 399888 | tf_op jit(solution)/shard_map/pallas_call | solution.py:346
  4.7 11.4 %all_to_all.20.ms_ref = bf16[4,272,128]{2,1,0:T(8,128)(2,1)S(1)} all-to-all(bf16[4,272,128]{2,1,0:T(8,128)(2,1)} %get-tuple-element.25), channel_id=1, replica_groups={{0,4,8,12},{16,20,24,28},{1,5,9,13},{17,21,25,29},{2,6,10,14},{18,22,26..., dimensions={0} | all-to-all | bytes 557056 | tf_op jit(solution)/shard_map/all_to_all | solution.py:426
  16.1 0.5 shard_map.200
  16.6 4.5 %collective-permute-start = (bf16[144,128]{1,0:T(8,128)(2,1)S(1)}, bf16[144,128]{1,0:T(8,128)(2,1)S(1)}, u32[]{:S(2)}, u32[]{:S(2)}) collective-permute-start(bf16[144,128]{1,0:T(8,128)(2,1)S(1)} %get-tuple-element.26), channel_id=1, source_target_pairs={{0,16},{4,20},{8,24},{12,28},{1,17},{5,21},{9,25},{13,29},{2,18},{... | collective-permute-start | bytes 110600 | tf_op jit(solution)/shard_map/ppermute | solution.py:443
  21.1 1.6 %collective-permute-done.got_ref = bf16[144,128]{1,0:T(8,128)(2,1)S(1)} collective-permute-done((bf16[144,128]{1,0:T(8,128)(2,1)S(1)}, bf16[144,128]{1,0:T(8,128)(2,1)S(1)}, u32[]{:S(2)}, u32[]{:S(2)}) %collective-permute-start) | collective-permute-done | bytes 36896 | tf_op jit(solution)/shard_map/ppermute | solution.py:443
  22.7 0.8 shard_map.201
  23.6 3.5 %all-to-all-start.1 = ((bf16[4,128,128]{2,1,0:T(8,128)(2,1)}), bf16[4,128,128]{2,1,0:T(8,128)(2,1)S(1)}, u32[]{:S(2)}, u32[]{:S(2)}) async-start(bf16[4,128,128]{2,1,0:T(8,128)(2,1)} %shard_map.201), calls=%async_computation.1 | async-start | bytes 262144 | tf_op jit(solution)/shard_map/all_to_all | solution.py:426
  27.0 0.0 copy-done.11
  27.1 5.0 %all-to-all-done.1.state_ref = bf16[4,128,128]{2,1,0:T(8,128)(2,1)S(1)} async-done(((bf16[4,128,128]{2,1,0:T(8,128)(2,1)}), bf16[4,128,128]{2,1,0:T(8,128)(2,1)S(1)}, u32[]{:S(2)}, u32[]{:S(2)}) %all-to-all-start.1) | async-done | bytes 131104 | tf_op jit(solution)/shard_map/all_to_all | solution.py:426
  32.0 0.0 copy-done.6
  32.0 0.0 copy-done.7
  32.0 0.0 copy-done.8
  32.0 0.0 copy-done.9
  32.1 0.0 copy-start.13
  32.1 0.0 copy-start.10
  32.1 0.0 copy-start.14
  32.1 0.0 copy-start
  32.1 0.0 copy-start.1
  32.1 0.0 copy-start.3
  32.1 0.0 copy-start.4
  32.1 0.7 shard_map.202
  32.8 0.1 collective-permute-start.2
  32.9 0.1 convolution_convert_fusion
  33.1 0.5 collective-permute-start.1
  33.6 0.7 collective-permute-done.2
  34.3 1.6 %collective-permute-start.3 = (bf16[128,512]{1,0:T(8,128)(2,1)S(1)}, bf16[128,512]{1,0:T(8,128)(2,1)S(1)}, u32[]{:S(2)}, u32[]{:S(2)}) collective-permute-start(bf16[128,512]{1,0:T(8,128)(2,1)S(1)} %add_convert_fusion.2), channel_id=1, source_target_pairs={{0,2},{1,3},{2,0},{3,1},{4,6},{5,7},{6,4},{7,5},{8,10},{9,11},{10,... | collective-permute-start | bytes 393224 | tf_op jit(solution)/shard_map/ppermute | solution.py:301
  35.9 0.0 copy-done.13
  35.9 0.1 multiply_bitcast_fusion
  36.0 0.0 collective-permute-done.1
  36.0 4.0 %collective-permute-done.3 = bf16[128,512]{1,0:T(8,128)(2,1)S(1)} collective-permute-done((bf16[128,512]{1,0:T(8,128)(2,1)S(1)}, bf16[128,512]{1,0:T(8,128)(2,1)S(1)}, u32[]{:S(2)}, u32[]{:S(2)}) %collective-permute-start.3) | collective-permute-done | bytes 131104 | tf_op jit(solution)/shard_map/ppermute | solution.py:301
  39.9 0.0 copy-done.10
  39.9 0.2 fusion.21
  40.1 0.1 collective-permute-start.4
  40.2 1.1 %collective-permute-done.4 = f32[2,128]{1,0:T(2,128)S(1)} collective-permute-done((f32[2,128]{1,0:T(2,128)S(1)}, f32[2,128]{1,0:T(2,128)S(1)}, u32[]{:S(2)}, u32[]{:S(2)}) %collective-permute-start.4) | collective-permute-done | bytes 1056 | tf_op jit(solution)/shard_map/ppermute | solution.py:301
  41.3 1.6 %collective-permute-start.5 = (f32[2,128]{1,0:T(2,128)S(1)}, f32[2,128]{1,0:T(2,128)S(1)}, u32[]{:S(2)}, u32[]{:S(2)}) collective-permute-start(f32[2,128]{1,0:T(2,128)S(1)} %fusion.19), channel_id=1, source_target_pairs={{0,2},{1,3},{2,0},{3,1},{4,6},{5,7},{6,4},{7,5},{8,10},{9,11},{10,... | collective-permute-start | bytes 3080 | tf_op jit(solution)/shard_map/ppermute | solution.py:301
  42.9 0.2 select_reduce_fusion
  43.1 1.9 %collective-permute-done.5 = f32[2,128]{1,0:T(2,128)S(1)} collective-permute-done((f32[2,128]{1,0:T(2,128)S(1)}, f32[2,128]{1,0:T(2,128)S(1)}, u32[]{:S(2)}, u32[]{:S(2)}) %collective-permute-start.5) | collective-permute-done | bytes 1056 | tf_op jit(solution)/shard_map/ppermute | solution.py:301
  45.0 0.3 fusion
  45.4 14.7 %all_to_all.21 = bf16[8,40,512]{2,1,0:T(8,128)(2,1)S(1)} all-to-all(bf16[8,40,512]{2,1,0:T(8,128)(2,1)S(1)} %fusion), channel_id=1, replica_groups=mesh['sp'=8,'tp'=4] {'sp'}, dimensions={0} | all-to-all | bytes 655360 | tf_op jit(solution)/shard_map/all_to_all | solution.py:484
  60.1 1.5 %collective-permute-start.6 = (bf16[320,512]{1,0:T(8,128)(2,1)S(1)}, bf16[320,512]{1,0:T(8,128)(2,1)S(1)}, u32[]{:S(2)}, u32[]{:S(2)}) collective-permute-start(bf16[320,512]{1,0:T(8,128)(2,1)S(1)} %bitcast.41), channel_id=1, source_target_pairs={{0,2},{1,3},{2,0},{3,1},{4,6},{5,7},{6,4},{7,5},{8,10},{9,11},{10,... | collective-permute-start | bytes 983048 | tf_op jit(solution)/shard_map/ppermute | solution.py:301
  61.6 0.0 collective-permute-start.8
  61.6 5.6 %collective-permute-done.6.refs_1_ = bf16[320,512]{1,0:T(8,128)(2,1)S(1)} collective-permute-done((bf16[320,512]{1,0:T(8,128)(2,1)S(1)}, bf16[320,512]{1,0:T(8,128)(2,1)S(1)}, u32[]{:S(2)}, u32[]{:S(2)}) %collective-permute-start.6) | collective-permute-done | bytes 327712 | tf_op jit(solution)/shard_map/ppermute | solution.py:301
  67.1 0.0 collective-permute-start.7
  67.1 0.0 collective-permute-done.8.refs_2_
  67.2 0.0 copy-done
  67.2 2.6 %shard_map.203 = (f32[320,1024]{1,0:T(8,128)S(1)}, f32[320,1024]{1,0:T(8,128)S(1)}, f32[320,128]{1,0:T(8,128)S(1)}, f32[320,128]{1,0:T(8,128)S(1)}) custom-call(s32[1]{0:T(128)} %bitcast.place_ref.refs_0_, bf16[320,512]{1,0:T(8,128)(2,1)S(1)} %bitcast.43, bf16[320,512]{1,0:T(8,128)(2,1)S(1)} %collective-permute-done.8.refs_2_, ...), custom_call_target="tpu_custom_call" | custom-call | flops 1509949440 | bytes 10092548 | tf_op jit(solution)/shard_map/pallas_call | solution.py:346
  69.8 0.0 collective-permute-done.7.refs_2_
  69.9 0.0 copy-start.12
  69.9 4.7 %shard_map.204 = (bf16[320,512]{1,0:T(8,128)(2,1)S(1)}, bf16[320,512]{1,0:T(8,128)(2,1)S(1)}, bf16[320,512]{1,0:T(8,128)(2,1)S(1)}, bf16[320,512]{1,0:T(8,128)(2,1)S(1)}) custom-call(s32[1]{0:T(128)} %bitcast.place_ref.refs_0_, bf16[320,512]{1,0:T(8,128)(2,1)S(1)} %collective-permute-done.6.refs_1_, bf16[320,512]{1,0:T(8,128)(2,1)S(1)} %collective-permute-done.7.refs_2_, ...), custom_call_target="tpu_custom_call" | custom-call | flops 3019898880 | bytes 18087940 | tf_op jit(solution)/shard_map/pallas_call | solution.py:346
  74.6 0.6 collective-permute-start.10
  75.2 0.1 collective-permute-start.9
  75.3 1.2 %collective-permute-done.10 = bf16[320,512]{1,0:T(8,128)(2,1)S(1)} collective-permute-done((bf16[320,512]{1,0:T(8,128)(2,1)S(1)}, bf16[320,512]{1,0:T(8,128)(2,1)S(1)}, u32[]{:S(2)}, u32[]{:S(2)}) %collective-permute-start.10) | collective-permute-done | bytes 327712 | tf_op jit(solution)/shard_map/ppermute | solution.py:301
  76.4 0.1 add_convert_fusion.1
  76.5 1.6 %collective-permute-start.11 = (bf16[320,512]{1,0:T(8,128)(2,1)S(1)}, bf16[320,512]{1,0:T(8,128)(2,1)S(1)}, u32[]{:S(2)}, u32[]{:S(2)}) collective-permute-start(bf16[320,512]{1,0:T(8,128)(2,1)S(1)} %add_convert_fusion.1), channel_id=1, source_target_pairs={{0,2},{1,3},{2,0},{3,1},{4,6},{5,7},{6,4},{7,5},{8,10},{9,11},{10,... | collective-permute-start | bytes 983048 | tf_op jit(solution)/shard_map/ppermute | solution.py:301
  78.1 0.0 collective-permute-done.9
  78.1 8.5 %collective-permute-done.11 = bf16[320,512]{1,0:T(8,128)(2,1)S(1)} collective-permute-done((bf16[320,512]{1,0:T(8,128)(2,1)S(1)}, bf16[320,512]{1,0:T(8,128)(2,1)S(1)}, u32[]{:S(2)}, u32[]{:S(2)}) %collective-permute-start.11) | collective-permute-done | bytes 327712 | tf_op jit(solution)/shard_map/ppermute | solution.py:301
  86.6 0.1 add_convert_fusion
  86.7 15.4 %all_to_all.22 = bf16[8,40,512]{2,1,0:T(8,128)(2,1)S(1)} all-to-all(bf16[8,40,512]{2,1,0:T(8,128)(2,1)S(1)} %bitcast.45), channel_id=1, replica_groups=mesh['sp'=8,'tp'=4] {'sp'}, dimensions={0} | all-to-all | bytes 655360 | tf_op jit(solution)/shard_map/all_to_all | solution.py:520
  102.1 0.4 fusion.20
  102.6 0.1 collective-permute-start.12
  102.6 1.1 %collective-permute-done.12 = f32[2,128]{1,0:T(2,128)S(1)} collective-permute-done((f32[2,128]{1,0:T(2,128)S(1)}, f32[2,128]{1,0:T(2,128)S(1)}, u32[]{:S(2)}, u32[]{:S(2)}) %collective-permute-start.12) | collective-permute-done | bytes 1056 | tf_op jit(solution)/shard_map/ppermute | solution.py:301
  103.8 1.6 %collective-permute-start.13 = (f32[2,128]{1,0:T(2,128)S(1)}, f32[2,128]{1,0:T(2,128)S(1)}, u32[]{:S(2)}, u32[]{:S(2)}) collective-permute-start(f32[2,128]{1,0:T(2,128)S(1)} %fusion.18), channel_id=1, source_target_pairs={{0,2},{1,3},{2,0},{3,1},{4,6},{5,7},{6,4},{7,5},{8,10},{9,11},{10,... | collective-permute-start | bytes 3080 | tf_op jit(solution)/shard_map/ppermute | solution.py:301
  105.4 2.1 %collective-permute-done.13 = f32[2,128]{1,0:T(2,128)S(1)} collective-permute-done((f32[2,128]{1,0:T(2,128)S(1)}, f32[2,128]{1,0:T(2,128)S(1)}, u32[]{:S(2)}, u32[]{:S(2)}) %collective-permute-start.13) | collective-permute-done | bytes 1056 | tf_op jit(solution)/shard_map/ppermute | solution.py:301
  107.5 0.8 multiply_convert_fusion
  (30 shorter events, 0.2 us)
Async XLA Ops:
  16.6 6.1 %collective-permute-start = (bf16[144,128]{1,0:T(8,128)(2,1)S(1)}, bf16[144,128]{1,0:T(8,128)(2,1)S(1)}, u32[]{:S(2)}, u32[]{:S(2)}) collective-permute-start(bf16[144,128]{1,0:T(8,128)(2,1)S(1)} %get-tuple-element.26), channel_id=1, source_target_pairs={{0,16},{4,20},{8,24},{12,28},{1,17},{5,21},{9,25},{13,29},{2,18},{... | collective-permute-start | bytes 110600 | tf_op jit(solution)/shard_map/ppermute | solution.py:443
  22.7 4.3 %copy-start.11 = (s32[128,2]{0,1:T(2,128)S(1)}, s32[128,2]{0,1:T(2,128)}, u32[]{:S(2)}) copy-start(s32[128,2]{0,1:T(2,128)} %param.33) | copy-start | bytes 3076
  22.7 9.3 %copy-start.6 = (bf16[512,2048]{1,0:T(8,128)(2,1)S(1)}, bf16[512,2048]{1,0:T(8,128)(2,1)}, u32[]{:S(2)}) copy-start(bf16[512,2048]{1,0:T(8,128)(2,1)} %weight_ref.1) | copy-start | bytes 6291460
  22.7 9.3 %copy-start.7 = (bf16[128,512]{1,0:T(8,128)(2,1)S(1)}, bf16[128,512]{1,0:T(8,128)(2,1)}, u32[]{:S(2)}) copy-start(bf16[128,512]{1,0:T(8,128)(2,1)} %valve_ref.1) | copy-start | bytes 393220
  22.7 9.3 %copy-start.8 = (f32[128,512]{1,0:T(8,128)S(1)}, f32[128,512]{1,0:T(8,128)}, u32[]{:S(2)}) copy-start(f32[128,512]{1,0:T(8,128)} %get-tuple-element.23.local_ref) | copy-start | bytes 786436
  22.7 9.3 %copy-start.9 = (f32[128,512]{1,0:T(8,128)S(1)}, f32[128,512]{1,0:T(8,128)}, u32[]{:S(2)}) copy-start(f32[128,512]{1,0:T(8,128)} %get-tuple-element.24.query_ref) | copy-start | bytes 786436
  23.6 8.5 %all-to-all-start.1 = ((bf16[4,128,128]{2,1,0:T(8,128)(2,1)}), bf16[4,128,128]{2,1,0:T(8,128)(2,1)S(1)}, u32[]{:S(2)}, u32[]{:S(2)}) async-start(bf16[4,128,128]{2,1,0:T(8,128)(2,1)} %shard_map.201), calls=%async_computation.1 | async-start | bytes 262144 | tf_op jit(solution)/shard_map/all_to_all | solution.py:426
  32.1 3.8 %copy-start.13 = (bf16[128,2]{0,1:T(2,128)(2,1)S(1)}, bf16[128,2]{0,1:T(2,128)(2,1)}, u32[]{:S(2)}) copy-start(bf16[128,2]{0,1:T(2,128)(2,1)} %param.34) | copy-start | bytes 1540
  32.1 7.8 %copy-start.10 = (bf16[128,512]{1,0:T(8,128)(2,1)S(1)}, bf16[128,512]{1,0:T(8,128)(2,1)}, u32[]{:S(2)}) copy-start(bf16[128,512]{1,0:T(8,128)(2,1)} %param.31) | copy-start | bytes 393220
  32.1 12.9 %copy-start.14 = (f32[512]{0:T(512)S(1)}, f32[512]{0:T(512)}, u32[]{:S(2)}) copy-start(f32[512]{0:T(512)} %param.32) | copy-start | bytes 6148
  32.1 35.1 %copy-start = (bf16[1,2048,1024]{2,1,0:T(8,128)(2,1)S(1)}, bf16[1,2048,1024]{2,1,0:T(8,128)(2,1)}, u32[]{:S(2)}) copy-start(bf16[1,2048,1024]{2,1,0:T(8,128)(2,1)} %refs_3_.5) | copy-start | bytes 12582916
  32.1 35.1 %copy-start.1 = (bf16[1,2048,1024]{2,1,0:T(8,128)(2,1)S(1)}, bf16[1,2048,1024]{2,1,0:T(8,128)(2,1)}, u32[]{:S(2)}) copy-start(bf16[1,2048,1024]{2,1,0:T(8,128)(2,1)} %refs_4_.5) | copy-start | bytes 12582916
  32.1 35.1 %copy-start.3 = (bf16[2048,128]{1,0:T(8,128)(2,1)S(1)}, bf16[2048,128]{1,0:T(8,128)(2,1)}, u32[]{:S(2)}) copy-start(bf16[2048,128]{1,0:T(8,128)(2,1)} %refs_5_.5) | copy-start | bytes 1572868
  32.1 35.1 %copy-start.4 = (bf16[2048,128]{1,0:T(8,128)(2,1)S(1)}, bf16[2048,128]{1,0:T(8,128)(2,1)}, u32[]{:S(2)}) copy-start(bf16[2048,128]{1,0:T(8,128)(2,1)} %refs_6_.3) | copy-start | bytes 1572868
  32.8 1.4 %collective-permute-start.2 = (bf16[128,512]{1,0:T(8,128)(2,1)S(1)}, bf16[128,512]{1,0:T(8,128)(2,1)S(1)}, u32[]{:S(2)}, u32[]{:S(2)}) collective-permute-start(bf16[128,512]{1,0:T(8,128)(2,1)S(1)} %get-tuple-element.32), channel_id=1, source_target_pairs={{0,1},{1,0},{2,3},{3,2},{4,5},{5,4},{6,7},{7,6},{8,9},{9,8},{10,11... | collective-permute-start | bytes 393224 | tf_op jit(solution)/shard_map/ppermute | solution.py:301
  33.1 2.9 %collective-permute-start.1 = (bf16[128,512]{1,0:T(8,128)(2,1)S(1)}, bf16[128,512]{1,0:T(8,128)(2,1)S(1)}, u32[]{:S(2)}, u32[]{:S(2)}) collective-permute-start(bf16[128,512]{1,0:T(8,128)(2,1)S(1)} %get-tuple-element.30), channel_id=1, source_target_pairs={{0,1},{1,0},{2,3},{3,2},{4,5},{5,4},{6,7},{7,6},{8,9},{9,8},{10,11... | collective-permute-start | bytes 393224 | tf_op jit(solution)/shard_map/ppermute | solution.py:301
  34.3 5.6 %collective-permute-start.3 = (bf16[128,512]{1,0:T(8,128)(2,1)S(1)}, bf16[128,512]{1,0:T(8,128)(2,1)S(1)}, u32[]{:S(2)}, u32[]{:S(2)}) collective-permute-start(bf16[128,512]{1,0:T(8,128)(2,1)S(1)} %add_convert_fusion.2), channel_id=1, source_target_pairs={{0,2},{1,3},{2,0},{3,1},{4,6},{5,7},{6,4},{7,5},{8,10},{9,11},{10,... | collective-permute-start | bytes 393224 | tf_op jit(solution)/shard_map/ppermute | solution.py:301
  40.1 1.2 %collective-permute-start.4 = (f32[2,128]{1,0:T(2,128)S(1)}, f32[2,128]{1,0:T(2,128)S(1)}, u32[]{:S(2)}, u32[]{:S(2)}) collective-permute-start(f32[2,128]{1,0:T(2,128)S(1)} %pad_maximum_fusion), channel_id=1, source_target_pairs={{0,1},{1,0},{2,3},{3,2},{4,5},{5,4},{6,7},{7,6},{8,9},{9,8},{10,11... | collective-permute-start | bytes 3080 | tf_op jit(solution)/shard_map/ppermute | solution.py:301
  41.3 3.6 %collective-permute-start.5 = (f32[2,128]{1,0:T(2,128)S(1)}, f32[2,128]{1,0:T(2,128)S(1)}, u32[]{:S(2)}, u32[]{:S(2)}) collective-permute-start(f32[2,128]{1,0:T(2,128)S(1)} %fusion.19), channel_id=1, source_target_pairs={{0,2},{1,3},{2,0},{3,1},{4,6},{5,7},{6,4},{7,5},{8,10},{9,11},{10,... | collective-permute-start | bytes 3080 | tf_op jit(solution)/shard_map/ppermute | solution.py:301
  60.1 9.8 %copy-start.2 = (bf16[1,1024,2048]{2,1,0:T(8,128)(2,1)S(1)}, bf16[1,1024,2048]{2,1,0:T(8,128)(2,1)}, u32[]{:S(2)}) copy-start(bf16[1,1024,2048]{2,1,0:T(8,128)(2,1)} %refs_12_.1) | copy-start | bytes 12582916
  60.1 9.8 %copy-start.5 = (bf16[128,2048]{1,0:T(8,128)(2,1)S(1)}, bf16[128,2048]{1,0:T(8,128)(2,1)}, u32[]{:S(2)}) copy-start(bf16[128,2048]{1,0:T(8,128)(2,1)} %refs_13_.1) | copy-start | bytes 1572868
  60.1 7.1 %collective-permute-start.6 = (bf16[320,512]{1,0:T(8,128)(2,1)S(1)}, bf16[320,512]{1,0:T(8,128)(2,1)S(1)}, u32[]{:S(2)}, u32[]{:S(2)}) collective-permute-start(bf16[320,512]{1,0:T(8,128)(2,1)S(1)} %bitcast.41), channel_id=1, source_target_pairs={{0,2},{1,3},{2,0},{3,1},{4,6},{5,7},{6,4},{7,5},{8,10},{9,11},{10,... | collective-permute-start | bytes 983048 | tf_op jit(solution)/shard_map/ppermute | solution.py:301
  61.6 5.6 %collective-permute-start.8 = (bf16[320,512]{1,0:T(8,128)(2,1)S(1)}, bf16[320,512]{1,0:T(8,128)(2,1)S(1)}, u32[]{:S(2)}, u32[]{:S(2)}) collective-permute-start(bf16[320,512]{1,0:T(8,128)(2,1)S(1)} %bitcast.42), channel_id=1, source_target_pairs={{0,1},{1,0},{2,3},{3,2},{4,5},{5,4},{6,7},{7,6},{8,9},{9,8},{10,11... | collective-permute-start | bytes 983048 | tf_op jit(solution)/shard_map/ppermute | solution.py:301
  67.1 2.7 %collective-permute-start.7 = (bf16[320,512]{1,0:T(8,128)(2,1)S(1)}, bf16[320,512]{1,0:T(8,128)(2,1)S(1)}, u32[]{:S(2)}, u32[]{:S(2)}) collective-permute-start(bf16[320,512]{1,0:T(8,128)(2,1)S(1)} %collective-permute-done.6.refs_1_), channel_id=1, source_target_pairs={{0,1},{1,0},{2,3},{3,2},{4,5},{5,4},{6,7},{7,6},{8,9},{9,8},{10,11... | collective-permute-start | bytes 983048 | tf_op jit(solution)/shard_map/ppermute | solution.py:301
  69.9 37.6 %copy-start.12 = (f32[512]{0:T(512)S(1)}, f32[512]{0:T(512)}, u32[]{:S(2)}) copy-start(f32[512]{0:T(512)} %param.41) | copy-start | bytes 6148
  74.6 1.8 %collective-permute-start.10 = (bf16[320,512]{1,0:T(8,128)(2,1)S(1)}, bf16[320,512]{1,0:T(8,128)(2,1)S(1)}, u32[]{:S(2)}, u32[]{:S(2)}) collective-permute-start(bf16[320,512]{1,0:T(8,128)(2,1)S(1)} %get-tuple-element.40), channel_id=1, source_target_pairs={{0,1},{1,0},{2,3},{3,2},{4,5},{5,4},{6,7},{7,6},{8,9},{9,8},{10,11... | collective-permute-start | bytes 983048 | tf_op jit(solution)/shard_map/ppermute | solution.py:301
  75.2 2.9 %collective-permute-start.9 = (bf16[320,512]{1,0:T(8,128)(2,1)S(1)}, bf16[320,512]{1,0:T(8,128)(2,1)S(1)}, u32[]{:S(2)}, u32[]{:S(2)}) collective-permute-start(bf16[320,512]{1,0:T(8,128)(2,1)S(1)} %get-tuple-element.38), channel_id=1, source_target_pairs={{0,1},{1,0},{2,3},{3,2},{4,5},{5,4},{6,7},{7,6},{8,9},{9,8},{10,11... | collective-permute-start | bytes 983048 | tf_op jit(solution)/shard_map/ppermute | solution.py:301
  76.5 10.1 %collective-permute-start.11 = (bf16[320,512]{1,0:T(8,128)(2,1)S(1)}, bf16[320,512]{1,0:T(8,128)(2,1)S(1)}, u32[]{:S(2)}, u32[]{:S(2)}) collective-permute-start(bf16[320,512]{1,0:T(8,128)(2,1)S(1)} %add_convert_fusion.1), channel_id=1, source_target_pairs={{0,2},{1,3},{2,0},{3,1},{4,6},{5,7},{6,4},{7,5},{8,10},{9,11},{10,... | collective-permute-start | bytes 983048 | tf_op jit(solution)/shard_map/ppermute | solution.py:301
  102.6 1.2 %collective-permute-start.12 = (f32[2,128]{1,0:T(2,128)S(1)}, f32[2,128]{1,0:T(2,128)S(1)}, u32[]{:S(2)}, u32[]{:S(2)}) collective-permute-start(f32[2,128]{1,0:T(2,128)S(1)} %pad_maximum_fusion.1), channel_id=1, source_target_pairs={{0,1},{1,0},{2,3},{3,2},{4,5},{5,4},{6,7},{7,6},{8,9},{9,8},{10,11... | collective-permute-start | bytes 3080 | tf_op jit(solution)/shard_map/ppermute | solution.py:301
  103.8 3.6 %collective-permute-start.13 = (f32[2,128]{1,0:T(2,128)S(1)}, f32[2,128]{1,0:T(2,128)S(1)}, u32[]{:S(2)}, u32[]{:S(2)}) collective-permute-start(f32[2,128]{1,0:T(2,128)S(1)} %fusion.18), channel_id=1, source_target_pairs={{0,2},{1,3},{2,0},{3,1},{4,6},{5,7},{6,4},{7,5},{8,10},{9,11},{10,... | collective-permute-start | bytes 3080 | tf_op jit(solution)/shard_map/ppermute | solution.py:301
where the time goes:
time: 109 us; the launch traced here: 108 us
  blocking collectives  41.5 us (38%)
  waiting for transfers between devices  32.7 us (30%)
  starting transfers between devices  17.1 us (16%)
  Pallas kernels  14.1 us (13%)
  other arithmetic  1.55 us (1%)
    ppermute x13, waiting for transfers between devices, swap(): return lax.ppermute(array, axis, [(i, i ^ bit) for i in range(size)])  26.1 us
    all_to_all x1, blocking collectives, shards(): lax.all_to_all(summed, 'sp', 0, 0, tiled=True).reshape(total, width)  15.4 us
    all_to_all x1, blocking collectives, shards(): lax.all_to_all(sent, 'sp', 0, 0, tiled=True).reshape(experts * slots, width)  14.7 us
    pallas_call x6, Pallas kernels, call(): pl.pallas_call(kernel, out_shape=shapes, in_specs=in_specs or [vmem()] *...  14.1 us
    all_to_all x1, blocking collectives, exchange(): lax.all_to_all(blocks, 'sp', 0, 0, axis_index_groups=groups, tiled=True)  11.4 us
    ppermute x13, starting transfers between devices, swap(): return lax.ppermute(array, axis, [(i, i ^ bit) for i in range(size)])  9.16 us
    all_to_all x1, waiting for transfers between devices, exchange(): lax.all_to_all(blocks, 'sp', 0, 0, axis_index_groups=groups, tiled=True)  4.96 us
    ppermute x1, starting transfers between devices, shards(): got = lax.ppermute(leaving, 'sp', onward)  4.51 us
  transfers between devices with their start and end apart: 15, of which 11 were waited for; matrix products, arithmetic and copies ran while one was open for 0% of the time, Pallas kernels for 2%

commit v1 on v0

v1 whole, which is shorter than its diff:
```python
import functools

import jax
import jax.numpy as jnp
from jax import lax
from jax.experimental import pallas as pl
from jax.experimental.pallas import tpu as pltpu
from jax.sharding import PartitionSpec as P


DK = 128
DV = 128
ALPHA = 2.0**0.25
F32 = jnp.float32
BF16 = jnp.bfloat16


def dot(left, right, contract=((1,), (0,))):
    return lax.dot_general(left, right, (contract, ((), ())), preferred_element_type=F32)


def split(array):
    high = array.astype(BF16)
    return high, (array - high.astype(F32)).astype(BF16)


def dot3(left, right):
    left_high, left_low = split(left)
    right_high, right_low = split(right)
    return dot(left_high, right_high) + (dot(left_high, right_low) + dot(left_low, right_high))


def dot_left(left, right):
    high, low = split(left)
    return dot(high, right) + dot(low, right)


def triangular_inverses(lowers, rows, cols):
    size = lowers[0].shape[0]
    identity = jnp.where(rows == cols, 1.0, 0.0)

    def once(left, right):
        return dot(left.astype(BF16), right.astype(BF16))

    def solve(powers, inverses, ratio, block):
        if block == 1:
            inverses = [x - p for p, x in zip(powers, inverses)]
            if ratio > 2:
                powers = [once(p, p) for p in powers]
        elif ratio > 2:
            both = [once(p, jnp.concatenate([p, x], 1)) for p, x in zip(powers, inverses)]
            powers = [pair[:, :size] for pair in both]
            inverses = [x - pair[:, size:] for pair, x in zip(both, inverses)]
        else:
            return [x - once(p, x) for p, x in zip(powers, inverses)]
        if ratio > 2:
            inverses = [x + once(p, x) for p, x in zip(powers, inverses)]
        return inverses

    inverses = [identity for _ in lowers]
    block = 1
    while block < size:
        ratio = min(4, size // block)
        wide = block * ratio
        inside = (rows // wide == cols // wide) & (rows // block != cols // block)
        parts = [jnp.where(inside, lower, 0.0) for lower in lowers]
        if block > 1:
            parts = [once(x, part) for x, part in zip(inverses, parts)]
        inverses = solve(parts, inverses, ratio, block)
        block = wide
    errors = [(identity - x) - dot3(lower, x) for lower, x in zip(lowers, inverses)]
    return [x + once(x, error) for x, error in zip(inverses, errors)]


def delta_kernel(*refs):
    place_ref, q_ref, k_ref, v_ref, store_ref, fade_ref, extra_ref, rate_ref, label_ref = refs[:9]
    ms_refs = refs[9:-2]
    local_ref, query_ref = refs[-2:]
    length = q_ref.shape[0]
    heads = store_ref.shape[0]
    every = range(heads)
    rows = lax.broadcasted_iota(jnp.int32, (length, length), 0)
    cols = lax.broadcasted_iota(jnp.int32, (length, length), 1)
    diagonal = rows == cols
    lower = rows >= cols
    strict = rows > cols
    identity = jnp.where(diagonal, 1.0, 0.0)

    def to_col(row):
        return jnp.sum(jnp.where(diagonal, row, 0.0), 1, keepdims=True)

    def to_row(col):
        return jnp.sum(jnp.where(diagonal, col, 0.0), 0, keepdims=True)

    label_row = label_ref[...].astype(F32)
    label_col = to_col(label_row)
    first = label_col[:1]
    last = label_col[length - 1 :]
    same = lower & (label_col == label_row)
    carried = jnp.where(label_col == first, 1.0, 0.0)
    closing = jnp.where(label_col == last, 1.0, 0.0)
    through = jnp.where(first == last, 1.0, 0.0)
    names = [place_ref[0] ^ k for k in every]
    at = [pl.ds(pl.multiple_of(name * DK, DK), DK) for name in names]
    queries = [q_ref[:, at[h]] for h in every]
    keys = [k_ref[:, at[h]] for h in every]
    values = [v_ref[:, at[h]] for h in every]
    row = [pl.ds(name, 1) for name in names]
    fades = [fade_ref[row[h], :] for h in every]
    softs = [jnp.maximum(fade, 0.0) + jnp.log(1.0 + jnp.exp(-jnp.abs(fade))) for fade in fades]
    rates = [jnp.exp(jnp.full((1, length), rate_ref[names[h]], F32)) for h in every]

    def scale_of(array):
        wide = array.astype(F32)
        return lax.rsqrt(jnp.sum(wide * wide, 1, keepdims=True) + 1e-06)

    key_scales = [scale_of(key) for key in keys]
    query_scales = [scale_of(query) * DK ** (-0.5) for query in queries]
    products = [dot(key, key, ((1,), (1,))) for key in keys]
    scores = [dot(query, key, ((1,), (1,))) for query, key in zip(queries, keys)]
    gate_rows = [1.0 / (1.0 + jnp.exp(-store_ref[row[h], :])) for h in every]
    gate_cols = [to_col(gate_rows[h]) for h in every]
    decays = [extra_ref[row[h], :] - rates[h] * softs[h] for h in every]
    totals = [jnp.sum(jnp.where(lower, decay, 0.0), 1, keepdims=True) for decay in decays]
    ends = [total[length - 1 :] for total in totals]
    reaches = [
        jnp.where(same, jnp.exp(jnp.where(lower, total - to_row(total), 0.0)), 0.0) for total in totals
    ]
    growths = [jnp.exp(total) * carried for total in totals]
    reaches = [reaches[h] * to_row(key_scales[h]) for h in every]
    couplings = [
        jnp.where(strict, products[h] * (key_scales[h] * gate_cols[h]) * reaches[h], 0.0) for h in every
    ]
    scores = [(scores[h] * query_scales[h] * reaches[h]).astype(BF16) for h in every]
    inverses = triangular_inverses(couplings, rows, cols)
    fresh = [dot_left(inverses[h] * gate_rows[h], values[h]) for h in every]
    erase = [
        dot_left(inverses[h] * to_row(gate_cols[h] * key_scales[h] * growths[h]), keys[h]) for h in every
    ]
    both = [jnp.concatenate([fresh[h], erase[h]], 1) for h in every]
    tails = [key_scales[h] * jnp.exp(ends[h] - totals[h]) * closing for h in every]
    carries = [dot(keys[h], (both[h] * tails[h]).astype(BF16), ((0,), (0,))) for h in every]
    seen = [dot(scores[h], both[h].astype(BF16)) for h in every]
    for h in every:
        final = jnp.exp(ends[h]) * through
        ms_refs[h][:DK] = (final * identity[:DK, :DK] - carries[h][:, DV:]).astype(BF16)
        ms_refs[h][DK : DK + DK] = carries[h][:, :DV].astype(BF16)
        ms_refs[h][DK + DK : DK + DK + 8] = jnp.broadcast_to(first, (8, DV)).astype(BF16)
        ms_refs[h][DK + DK + 8 :] = jnp.broadcast_to(last, (8, DV)).astype(BF16)
        local_ref[:, at[h]] = seen[h][:, :DV]
        query_ref[:, at[h]] = queries[h].astype(F32) * (query_scales[h] * growths[h]) - seen[h][:, DV:]


def first_label(ms_ref, j):
    return ms_ref[j, DK + DK : DK + DK + 8].astype(F32)[:1]


def last_label(ms_ref, j):
    return ms_ref[j, DK + DK + 8 :].astype(F32)[:1]


def fold_kernel(place_ref, *refs):
    ms_refs = refs[:-6]
    state_ref, map_ref, start_ref, leaving_ref, end_ref, ms_ref = refs[-6:]
    blocks = len(ms_refs)
    for k in range(blocks):
        ms_ref[place_ref[0] ^ k] = ms_refs[k][...]
    state = jnp.zeros((DK, DV), F32)
    reach = jnp.where(
        lax.broadcasted_iota(jnp.int32, (DK, DK), 0) == lax.broadcasted_iota(jnp.int32, (DK, DK), 1), 1.0, 0.0
    )
    for j in range(blocks):
        if j:
            joined = jnp.where(first_label(ms_ref, j) == last_label(ms_ref, j - 1), 1.0, 0.0)
            state = state * joined
            reach = reach * joined
        onto = ms_ref[j, :DK]
        reach = reach.astype(BF16)
        state_ref[j] = state
        map_ref[j] = reach
        add = ms_ref[j, DK : DK + DK].astype(F32)
        if j:
            high, low = split(state)
            moved = dot(onto, jnp.concatenate([high, low, reach], 1))
            state = moved[:, :DV] + moved[:, DV : DV + DV] + add
            reach = moved[:, DV + DV :]
        else:
            state = add
            reach = onto.astype(F32)
    start_ref[...] = ms_ref[0, DK + DK :]
    leaving_ref[:DK] = state.astype(BF16)
    leaving_ref[DK:] = ms_ref[blocks - 1, DK + DK :]
    end_ref[:DK] = state
    end_ref[DK:] = reach


def arriving(got_ref, start_ref):
    last = got_ref[DK + 8 :].astype(F32)[:1]
    joined = jnp.where(start_ref[:8].astype(F32)[:1] == last, 1.0, 0.0)
    return (got_ref[:DK].astype(F32) * joined).astype(BF16)


def enter_kernel(place_ref, got_ref, start_ref, state_ref, map_ref, *entering_refs):
    state = arriving(got_ref, start_ref)
    for k, entering_ref in enumerate(entering_refs):
        j = place_ref[0] ^ k
        entering_ref[...] = (state_ref[j] + dot(map_ref[j], state)).astype(BF16)


def leave_kernel(got_ref, start_ref, leaving_ref, end_ref, out_ref):
    state = arriving(got_ref, start_ref)
    out_ref[:DK] = (end_ref[:DK] + dot(end_ref[DK:].astype(BF16), state)).astype(BF16)
    out_ref[DK:] = leaving_ref[DK:]


def project_kernel(place_ref, group_ref, local_ref, query_ref, valve_ref, weight_ref, *refs):
    heads = local_ref.shape[1] // DV
    state_refs, out_refs, heads_ref = refs[:heads], refs[heads:-1], refs[-1]
    for k in range(heads):
        at = pl.ds(pl.multiple_of((group_ref[0] ^ k) * DV, DV), DV)
        mixed = local_ref[:, at] + dot_left(query_ref[:, at], state_refs[k][...])
        scaled = mixed * lax.rsqrt(jnp.mean(mixed * mixed, 1, keepdims=True) + 1e-06)
        heads_ref[:, at] = (scaled * silu(valve_ref[:, at].astype(F32))).astype(BF16)
    width = out_refs[0].shape[1]
    for offset in range(len(out_refs) - 1, -1, -1):
        start = pl.multiple_of((place_ref[0] ^ offset) * width, width)
        out_refs[offset][...] = dot(heads_ref[...], weight_ref[:, pl.ds(start, width)]).astype(BF16)


def spread(fields, width):
    rows = lax.broadcasted_iota(jnp.int32, (128, width), 0)
    lanes = lax.broadcasted_iota(jnp.int32, (128, width), 1)
    return jnp.where(lanes // (width // fields) == rows, 1.0, 0.0).astype(BF16)


def own_lane(fields, slots, width):
    rows = lax.broadcasted_iota(jnp.int32, (slots, width), 0)
    lanes = lax.broadcasted_iota(jnp.int32, (slots, width), 1)
    return rows == lanes % (width // fields)


def pack_kernel(capacity, fields, keep_ref, got_ref, row_ref, gain_ref, pick_ref, route_ref, out_ref):
    experts, slots, width = out_ref.shape
    summed = ALPHA * row_ref[...].astype(F32) + (keep_ref[...] + got_ref[...].astype(F32))
    tokens = summed.shape[0]
    mean = jnp.mean(summed, 1, keepdims=True)
    centred = summed - mean
    squares = jnp.sum(centred * centred, 1, keepdims=True)
    gain = gain_ref[...]
    lane = lax.broadcasted_iota(jnp.int32, (tokens, 128), 1)
    notes = jnp.zeros((tokens, 128), F32)
    for value, places in ((mean, (1, 2, 3)), (squares, (4, 5))):
        for place in places:
            piece = value.astype(BF16).astype(F32)
            notes = jnp.where(lane == place, piece, notes)
            value = value - piece
    pick = pick_ref[...]
    body = dot(pick, (centred * gain).astype(BF16))
    notes = dot(pick, notes.astype(BF16))
    routes = dot(pick, route_ref[...], ((1,), (1,)))
    expert = (lax.broadcasted_iota(jnp.int32, (experts * slots, 1), 0) // slots + 1).astype(F32)
    share = jnp.where(routes[:, 2:3] == expert, -routes[:, :1], routes[:, 1:2])
    lane = lax.broadcasted_iota(jnp.int32, (experts * slots, 128), 1)
    notes = jnp.where(lane == 0, share, notes).astype(BF16)
    notes = dot(notes, spread(fields, width))
    mine = own_lane(fields, slots, width)
    gain_high, gain_low = split(gain)
    rows = lax.broadcasted_iota(jnp.int32, (slots, width), 0)
    for e in range(experts):
        here = slice(e * slots, (e + 1) * slots)
        info = jnp.sum(jnp.where(mine, notes[here], 0.0), 0, keepdims=True)
        block = jnp.where(rows == capacity, info, body[here])
        block = jnp.where(rows == capacity + 1, gain_high.astype(F32), block)
        block = jnp.where(rows == capacity + 2, gain_low.astype(F32), block)
        out_ref[e] = block.astype(BF16)


def silu(array):
    return array / (1.0 + jnp.exp(-array))


def read_notes(piece_ref, capacity, slots, fields):
    width = piece_ref.shape[1]
    mine = own_lane(fields, slots, width)
    base = capacity // 8 * 8
    blocks = []
    for source in range(piece_ref.shape[0] // slots):
        info = piece_ref[source * slots + base : source * slots + base + 8, :].astype(F32)
        blocks.append(jnp.where(mine, info[capacity - base : capacity - base + 1], 0.0))
    return dot(jnp.concatenate(blocks, 0).astype(BF16), spread(fields, width), ((1,), (1,)))


def gain_row(array, capacity):
    return array[capacity + 1 : capacity + 2] + array[capacity + 2 : capacity + 3]


def near_kernel(step, slots, capacity, fields, *refs):
    place_ref, piece_refs = refs[0], refs[1:3]
    weight_refs, sum_refs, gain_refs, note_refs = refs[3:7], refs[7:11], refs[11:15], refs[15:17]
    width = piece_refs[0].shape[1]
    at = [pl.ds(pl.multiple_of((place_ref[0] ^ k) * width, width), width) for k in range(2)]

    def product(weight_ref, sum_ref, gain_ref, cut):
        total = None
        for k in range(2):
            weight = weight_ref[at[k], cut] if len(weight_ref.shape) == 2 else weight_ref[0, at[k], cut]
            term = dot(piece_refs[k][...], weight)
            gain_ref[k : k + 1, cut] = gain_row(term, capacity)
            total = term if total is None else total + term
        sum_ref[:, cut] = total

    for i in (2, 3):
        product(weight_refs[i], sum_refs[i], gain_refs[i], slice(None))

    def chunk(i, _):
        cut = pl.ds(pl.multiple_of(i * step, step), step)
        for j in (0, 1):
            product(weight_refs[j], sum_refs[j], gain_refs[j], cut)
        return 0

    lax.fori_loop(0, weight_refs[0].shape[2] // step, chunk, 0)
    for k in range(2):
        note_refs[k][...] = read_notes(piece_refs[k], capacity, slots, fields)


def far_kernel(count, half, step, slots, capacity, fields, *refs):
    place_ref, piece_refs = refs[0], refs[1 : count - 1]
    refs = refs[count - 1 :]
    weight_refs, sum_refs, gain_refs, note_refs = refs[:4], refs[4:8], refs[8:12], refs[12:14]
    own_ref, lower_ref, cl_ref = refs[14:17]
    out_refs = refs[17 : 17 + count]
    hidden_ref, shared_ref = refs[17 + count :]
    height, width = piece_refs[0].shape
    here = slice(half * height, (half + 1) * height)
    at = [pl.ds(pl.multiple_of((place_ref[0] ^ k) * width, width), width) for k in range(2, count)]
    notes = [note_ref[here] for note_ref in note_refs]
    notes = notes + [read_notes(piece_ref, capacity, slots, fields) for piece_ref in piece_refs]
    means = [note[:, 1:2] + note[:, 2:3] + note[:, 3:4] for note in notes]
    mean = sum(means) / count
    offsets = [own_mean - mean for own_mean in means]
    squares = sum(note[:, 4:5] + note[:, 5:6] + width * offset * offset for note, offset in zip(notes, offsets))
    scale = lax.rsqrt(squares / (count * width) + 1e-05)
    share = notes[0][:, :1]
    flag = jnp.where(share < 0.0, 1.0, 0.0)
    share = jnp.abs(share)

    def product(weight_ref, sum_ref, gain_ref, cut):
        total = sum_ref[here, cut]
        for k in range(2):
            total = total + offsets[k] * gain_ref[k : k + 1, cut]
        for k in range(2, count):
            weight = weight_ref[at[k - 2], cut] if len(weight_ref.shape) == 2 else weight_ref[0, at[k - 2], cut]
            term = dot(piece_refs[k - 2][...], weight)
            total = total + term + offsets[k] * gain_row(term, capacity)
        return total * scale

    every = slice(None)
    gate = product(weight_refs[2], sum_refs[2], gain_refs[2], every)
    lift = product(weight_refs[3], sum_refs[3], gain_refs[3], every)
    shared_ref[...] = (silu(gate) * lift * flag).astype(BF16)

    def chunk(i, _):
        cut = pl.ds(pl.multiple_of(i * step, step), step)
        gate = product(weight_refs[0], sum_refs[0], gain_refs[0], cut)
        lift = product(weight_refs[1], sum_refs[1], gain_refs[1], cut)
        hidden_ref[:, cut] = (silu(gate) * lift * share).astype(BF16)
        return 0

    lax.fori_loop(0, weight_refs[0].shape[2] // step, chunk, 0)
    for k in range(count - 1, -1, -1):
        cut = pl.ds(pl.multiple_of((place_ref[0] ^ k) * width, width), width)
        term = dot(hidden_ref[...], lower_ref[0, :, cut]) + dot(shared_ref[...], cl_ref[:, cut])
        if k == 0:
            own = own_ref[here, :].astype(F32)
            term = term + (own + offsets[0] * gain_row(own, capacity)) * (flag * scale * ALPHA)
        out_refs[k][...] = term.astype(out_refs[k].dtype)


def swap(array, axis, bit):
    size = lax.axis_size(axis)
    return lax.ppermute(array, axis, [(i, i ^ bit) for i in range(size)])


def scatter_sum(blocks, axis):
    bit = 1
    while len(blocks) > 1:
        kept = {}
        final = len(blocks) == 2
        for k in range(len(blocks) - 1, 0, -2):
            got = swap(blocks[k].astype(BF16), axis, bit)
            if final:
                return blocks[0].astype(F32), got
            kept[k // 2] = blocks[k - 1].astype(F32) + got.astype(F32)
        blocks = [kept[k] for k in range(len(blocks) // 2)]
        bit *= 2


def sum_all(array, axis):
    bit = 1
    while bit < lax.axis_size(axis):
        array = array + swap(array, axis, bit)
        bit *= 2
    return array


def gather_near(array, axis):
    return [array, swap(array, axis, 1)]


def gather_far(array, axis):
    size = lax.axis_size(axis)
    pieces = {0: array}
    bit = size // 2
    while bit:
        for k, piece in list(pieces.items()):
            if k ^ bit != 1:
                pieces[k ^ bit] = swap(piece, axis, bit)
        bit //= 2
    return [pieces[k] for k in range(2, size)]


def feature_norm(summed, gain):
    width = summed.shape[-1] * lax.axis_size("tp")
    sums = sum_all(jnp.stack([jnp.sum(summed, -1), jnp.sum(summed * summed, -1)]), "tp")
    row_mean = sums[0] / width
    row_var = sums[1] / width - row_mean * row_mean
    return (summed - row_mean[:, None]) * lax.rsqrt(row_var[:, None] + 1e-05) * gain


def call(kernel, outs, *args, in_specs=None, out_specs=None, limit=12, flops=4 * 10**9, **kw):
    shapes = [jax.ShapeDtypeStruct(shape, kind) for shape, kind in outs]
    moved = sum(array.size * array.dtype.itemsize for array in args)
    return pl.pallas_call(
        kernel,
        out_shape=shapes,
        in_specs=in_specs or [vmem()] * len(args),
        out_specs=out_specs or [vmem()] * len(outs),
        compiler_params=pltpu.CompilerParams(vmem_limit_bytes=limit * 1024 * 1024),
        cost_estimate=pl.CostEstimate(flops=flops, bytes_accessed=moved, transcendentals=0),
        **kw,
    )(*args)


def smem():
    return pl.BlockSpec(memory_space=pltpu.SMEM)


def vmem():
    return pl.BlockSpec(memory_space=pltpu.VMEM)


def shards(
    probe_vectors,
    address_vectors,
    content_vectors,
    storage_raw_signal,
    fade_raw_signal,
    channel_fade_exponent,
    extra_fade_amount,
    sequence_label,
    exit_valve_raw_signal,
    final_projection_matrix,
    incoming_rows_matrix,
    initial_rescale_factor,
    specialist_picks,
    picked_specialist_share,
    specialist_valve_matrix,
    specialist_raising_matrix,
    specialist_lowering_matrix,
    common_valve_matrix,
    common_raising_matrix,
    common_lowering_matrix,
    latter_rescale_factor,
):
    tokens, width = incoming_rows_matrix.shape
    heads = storage_raw_signal.shape[0]
    n_sp = lax.axis_size("sp")
    n_tp = lax.axis_size("tp")

    place = lax.axis_index("tp").astype(jnp.int32)[None]

    inputs = (
        probe_vectors,
        address_vectors,
        content_vectors,
        storage_raw_signal,
        fade_raw_signal,
        extra_fade_amount,
        channel_fade_exponent,
        sequence_label[None, :],
    )
    shapes = [((tokens, heads * DV), F32), ((tokens, heads * DK), F32)]

    def one_step(shape):
        return pl.BlockSpec(shape, lambda i: (0,) * len(shape))

    group = (lax.axis_index("sp").astype(jnp.int32) % heads)[None]
    *ms, local, query = call(
        delta_kernel,
        [((DK + DK + 16, DV), BF16)] * heads + shapes,
        group,
        *inputs,
        grid=(1,),
        in_specs=[smem()] + [one_step(array.shape) for array in inputs[:-2]] + [smem(), one_step(inputs[-1].shape)],
        out_specs=[one_step((DK + DK + 16, DV))] * heads + [one_step(shape) for shape, _ in shapes],
        limit=61,
        flops=2 * 10**9,
    )

    def exchange(blocks):
        return [blocks[0]] + [swap(blocks[k], "sp", k) for k in range(1, heads)]

    mine = exchange(ms)
    states, maps, start, leaving, end = call(
        fold_kernel,
        [
            ((heads, DK, DV), F32),
            ((heads, DK, DK), BF16),
            ((16, DV), BF16),
            ((DK + 16, DV), BF16),
            ((DK + DK, DV), F32),
        ],
        group,
        *mine,
        in_specs=[smem()] + [vmem()] * heads,
        scratch_shapes=[pltpu.VMEM((heads, DK + DK + 16, DV), BF16)],
    )
    onward = [(i, i + heads) for i in range(n_sp - heads)]

    def hop(_, leaving):
        got = lax.ppermute(leaving, "sp", onward)
        return call(leave_kernel, [((DK + 16, DV), BF16)], got, start, leaving, end)[0]

    segments = n_sp // heads
    if segments > 2:
        leaving = lax.fori_loop(0, segments - 2, hop, leaving)
    got = lax.ppermute(leaving, "sp", onward)
    entering = exchange(
        call(
            enter_kernel,
            [((DK, DV), BF16)] * heads,
            group,
            got,
            start,
            states,
            maps,
            in_specs=[smem()] + [vmem()] * 4,
        )
    )

    partial = call(
        project_kernel,
        [((tokens, width), BF16)] * n_tp,
        place,
        group,
        local,
        query,
        exit_valve_raw_signal,
        final_projection_matrix,
        *entering,
        in_specs=[smem()] * 2 + [vmem()] * (4 + heads),
        scratch_shapes=[pltpu.VMEM((tokens, heads * DV), BF16)],
    )
    keep, got = scatter_sum(partial, "tp")

    top = specialist_picks.shape[1]
    experts = specialist_valve_matrix.shape[0] * n_sp
    capacity = max(2, 9 * tokens * top // (8 * experts))
    slots = (capacity + 10) // 8 * 8
    named = specialist_picks.T[:, None, :] == jnp.arange(experts, dtype=jnp.int32)[None, :, None]
    taken = jnp.any(named, 0)
    earlier = jnp.arange(tokens)[:, None] < jnp.arange(tokens)[None, :]
    rank = jnp.dot(taken.astype(BF16), earlier.astype(BF16), preferred_element_type=F32)
    slot_index = jnp.arange(slots, dtype=jnp.int32)
    chosen = taken[:, None, :] & (rank.astype(jnp.int32)[:, None, :] == slot_index[None, :, None])
    chosen = chosen & (slot_index < capacity)[None, :, None]
    pick = chosen.astype(BF16).reshape(experts * slots, tokens)
    routes = jnp.concatenate(
        [picked_specialist_share.T.astype(F32), (specialist_picks.T[:1] + 1).astype(F32)], 0
    )
    routes = jnp.pad(routes, ((0, 13), (0, 0))).astype(BF16)
    fields = 8
    (sent,) = call(
        functools.partial(pack_kernel, capacity, fields),
        [((experts, slots, width), BF16)],
        keep,
        got,
        incoming_rows_matrix,
        initial_rescale_factor[None, :],
        pick,
        routes,
    )
    arrived = lax.all_to_all(sent, "sp", 0, 0, tiled=True).reshape(experts * slots, width)

    hidden = specialist_valve_matrix.shape[2]
    shared = common_valve_matrix.shape[1]
    total = experts * slots
    step = min(hidden, 256)
    weights = (specialist_valve_matrix, specialist_raising_matrix, common_valve_matrix, common_raising_matrix)
    work = 4 * total * width * (hidden + shared)
    parts = 2
    height = total // parts
    halves = [gather_far(arrived[i * height : (i + 1) * height], "tp") for i in range(parts)]
    near = gather_near(arrived, "tp")
    common = (step, slots, capacity, fields)
    partial = call(
        functools.partial(near_kernel, *common),
        [((total, hidden), F32)] * 2
        + [((total, shared), F32)] * 2
        + [((8, hidden), F32)] * 2
        + [((8, shared), F32)] * 2
        + [((total, 128), F32)] * 2,
        place,
        *near,
        *weights,
        in_specs=[smem()] + [vmem()] * 6,
        flops=work * 2,
    )
    sums = []
    for i in range(parts):
        results = call(
            functools.partial(far_kernel, n_tp, i, *common),
            [((height, width), F32)] + [((height, width), BF16)] * (n_tp - 1),
            place,
            *halves[i],
            *weights,
            *partial,
            arrived,
            specialist_lowering_matrix,
            common_lowering_matrix,
            in_specs=[smem()] + [vmem()] * (n_tp + 15),
            scratch_shapes=[pltpu.VMEM((height, hidden), BF16), pltpu.VMEM((height, shared), BF16)],
            flops=work * n_tp // parts,
        )
        sums.append(sum(term.astype(F32) for term in scatter_sum(results, "tp")).astype(BF16))
    summed = jnp.concatenate(sums, 0).reshape(experts, slots, width)
    returned = lax.all_to_all(summed, "sp", 0, 0, tiled=True).reshape(total, width)
    second_sum = lax.dot_general(
        pick, returned, (((0,), (0,)), ((), ())), preferred_element_type=F32
    )
    return feature_norm(second_sum, latter_rescale_factor).astype(BF16)


def solution(mesh):
    placed = (
        P("sp", "tp"),
        P("sp", "tp"),
        P("sp", "tp"),
        P("tp", "sp"),
        P("tp", "sp"),
        P("tp"),
        P("tp", "sp"),
        P("sp"),
        P("sp", "tp"),
        P("tp", None),
        P("sp", "tp"),
        P("tp"),
        P("sp", None),
        P("sp", None),
        P("sp", None, "tp"),
        P("sp", None, "tp"),
        P("sp", "tp", None),
        P(None, "tp"),
        P(None, "tp"),
        P("tp", None),
        P("tp"),
    )

    return jax.shard_map(shards, mesh=mesh, in_specs=placed, out_specs=P("sp", "tp"), check_vma=False)
```

time: 109 us -> 106 us (0.972)
  blocking collectives: 41.5 us -> 29.8 us
  starting transfers between devices: 17.1 us -> 22.2 us
  Pallas kernels: 14.1 us -> 17.2 us
    all_to_all x1 -> x0, blocking collectives: 11.4 us -> none  [exchange(): lax.all_to_all(blocks, 'sp', 0, 0, axis_index_groups=groups, tiled=True)]
    ppermute x13 -> x22, starting transfers between devices: 9.16 us -> 17.7 us  [swap(): return lax.ppermute(array, axis, [(i, i ^ bit) for i in range(size)])]
    all_to_all x1 -> x0, waiting for transfers between devices: 4.96 us -> none  [exchange(): lax.all_to_all(blocks, 'sp', 0, 0, axis_index_groups=groups, tiled=True)]
    ppermute x13 -> x22, waiting for transfers between devices: 26.1 us -> 30.2 us  [swap(): return lax.ppermute(array, axis, [(i, i ^ bit) for i in range(size)])]
    all_to_all x1 -> x0, starting transfers between devices: 3.46 us -> none  [exchange(): lax.all_to_all(blocks, 'sp', 0, 0, axis_index_groups=groups, tiled=True)]
    pallas_call x6 -> x8, Pallas kernels: 14.1 us -> 17.2 us  [call(): pl.pallas_call(kernel, out_shape=shapes, in_specs=in_specs or [vmem()] *...]
    all_to_all x1, blocking collectives: 15.4 us -> 13.5 us  [shards(): lax.all_to_all(summed, 'sp', 0, 0, tiled=True).reshape(total, width)]
    all_to_all x1, blocking collectives: 14.7 us -> 16.4 us  [shards(): lax.all_to_all(sent, 'sp', 0, 0, tiled=True).reshape(experts * slots, width)]
  transfers between devices with their start and end apart: 15 -> 23, of which waited for: 11 -> 13; matrix products, arithmetic and copies ran while one was open for 0% -> 2% of each run, Pallas kernels for 2% -> 9%
where the time goes in v1:
time: 106 us; the launch traced here: 105 us
  waiting for transfers between devices  31.7 us (30%)
  blocking collectives  29.8 us (28%)
  starting transfers between devices  22.2 us (21%)
  Pallas kernels  17.2 us (16%)
  other arithmetic  2.54 us (2%)
  local copies, waits for them, and re-layouts  1.15 us (1%)
    ppermute x22, waiting for transfers between devices, swap(): return lax.ppermute(array, axis, [(i, i ^ bit) for i in range(size)])  30.2 us
    ppermute x22, starting transfers between devices, swap(): return lax.ppermute(array, axis, [(i, i ^ bit) for i in range(size)])  17.7 us
    pallas_call x8, Pallas kernels, call(): pl.pallas_call(kernel, out_shape=shapes, in_specs=in_specs or [vmem()] *...  17.2 us
    all_to_all x1, blocking collectives, shards(): lax.all_to_all(sent, 'sp', 0, 0, tiled=True).reshape(experts * slots, width)  16.4 us
    all_to_all x1, blocking collectives, shards(): lax.all_to_all(summed, 'sp', 0, 0, tiled=True).reshape(total, width)  13.5 us
    ppermute x1, starting transfers between devices, shards(): got = lax.ppermute(leaving, 'sp', onward)  4.48 us
  transfers between devices with their start and end apart: 23, of which 13 were waited for; matrix products, arithmetic and copies ran while one was open for 2% of the time, Pallas kernels for 9%

profile of v1, /device:TPU:0, one launch (start us, length us, event | category | flops | bytes accessed | tf_op | source)
XLA Modules:
  0.0 105.4 jit_solution(3292501780381493097)
XLA Ops:
  0.0 4.6 %shard_map.199 = (bf16[272,128]{1,0:T(8,128)(2,1)}, bf16[272,128]{1,0:T(8,128)(2,1)}, bf16[272,128]{1,0:T(8,128)(2,1)}, bf16[272,128]{1,0:T(8,128)(2,1)}, f32[128,512]{1,0:T(8,128)}, /*index=5*/f32[128,512]{1,0:T(8,128)}) custom-call(s32[1]{0:T(128)} %bitcast.2.refs_0_.place_ref.group_ref, bf16[128,512]{1,0:T(8,128)(2,1)} %refs_1_.1, ...), custom_call_target="tpu_custom_call" | custom-call | flops 2000000000 | bytes 399892 | tf_op jit(solution)/shard_map/pallas_call | solution.py:433
  4.6 3.0 %collective-permute-start = (bf16[272,128]{1,0:T(8,128)(2,1)}, bf16[272,128]{1,0:T(8,128)(2,1)S(1)}, u32[]{:S(2)}, u32[]{:S(2)}) collective-permute-start(bf16[272,128]{1,0:T(8,128)(2,1)} %get-tuple-element.44), channel_id=1, source_target_pairs={{0,4},{4,0},{8,12},{12,8},{16,20},{20,16},{24,28},{28,24},{1,5},{5... | collective-permute-start | bytes 208904 | tf_op jit(solution)/shard_map/ppermute | solution.py:381
  7.5 1.6 %collective-permute-start.1 = (bf16[272,128]{1,0:T(8,128)(2,1)}, bf16[272,128]{1,0:T(8,128)(2,1)S(1)}, u32[]{:S(2)}, u32[]{:S(2)}) collective-permute-start(bf16[272,128]{1,0:T(8,128)(2,1)} %get-tuple-element.45), channel_id=1, source_target_pairs={{0,8},{4,12},{8,0},{12,4},{16,24},{20,28},{24,16},{28,20},{1,9},{5... | collective-permute-start | bytes 208904 | tf_op jit(solution)/shard_map/ppermute | solution.py:381
  9.1 0.9 collective-permute-done.refs_1_
  10.0 2.6 %collective-permute-done.1.refs_2_ = bf16[272,128]{1,0:T(8,128)(2,1)S(1)} collective-permute-done((bf16[272,128]{1,0:T(8,128)(2,1)}, bf16[272,128]{1,0:T(8,128)(2,1)S(1)}, u32[]{:S(2)}, u32[]{:S(2)}) %collective-permute-start.1) | collective-permute-done | bytes 69664 | tf_op jit(solution)/shard_map/ppermute | solution.py:381
  12.7 1.9 %collective-permute-done.2.refs_3_ = bf16[272,128]{1,0:T(8,128)(2,1)S(1)} collective-permute-done((bf16[272,128]{1,0:T(8,128)(2,1)}, bf16[272,128]{1,0:T(8,128)(2,1)S(1)}, u32[]{:S(2)}, u32[]{:S(2)}) %collective-permute-start.2) | collective-permute-done | bytes 69664 | tf_op jit(solution)/shard_map/ppermute | solution.py:381
  14.5 0.9 copy-done.12
  15.4 1.2 %shard_map.200 = (f32[4,128,128]{2,1,0:T(8,128)S(1)}, bf16[4,128,128]{2,1,0:T(8,128)(2,1)S(1)}, bf16[16,128]{1,0:T(8,128)(2,1)S(1)}, bf16[144,128]{1,0:T(8,128)(2,1)S(1)}, f32[256,128]{1,0:T(8,128)}) custom-call(s32[1]{0:T(128)} %bitcast.2.refs_0_.place_ref.group_ref, bf16[272,128]{1,0:T(8,128)(2,1)S(1)} %copy-done.12, ...), custom_call_target="tpu_custom_call" | custom-call | flops 4000000000 | bytes 278532 | tf_op jit(solution)/shard_map/pallas_call | solution.py:433
  16.6 4.5 %collective-permute-start.3 = (bf16[144,128]{1,0:T(8,128)(2,1)S(1)}, bf16[144,128]{1,0:T(8,128)(2,1)S(1)}, u32[]{:S(2)}, u32[]{:S(2)}) collective-permute-start(bf16[144,128]{1,0:T(8,128)(2,1)S(1)} %get-tuple-element.47), channel_id=1, source_target_pairs={{0,16},{4,20},{8,24},{12,28},{1,17},{5,21},{9,25},{13,29},{2,18},{... | collective-permute-start | bytes 110600 | tf_op jit(solution)/shard_map/ppermute | solution.py:537
  21.1 0.1 convolution_convert_fusion
  21.2 1.5 %collective-permute-done.3.got_ref = bf16[144,128]{1,0:T(8,128)(2,1)S(1)} collective-permute-done((bf16[144,128]{1,0:T(8,128)(2,1)S(1)}, bf16[144,128]{1,0:T(8,128)(2,1)S(1)}, u32[]{:S(2)}, u32[]{:S(2)}) %collective-permute-start.3) | collective-permute-done | bytes 36896 | tf_op jit(solution)/shard_map/ppermute | solution.py:537
  22.7 0.2 shard_map.201
  22.9 0.6 collective-permute-start.4
  23.5 0.9 collective-permute-start.5
  24.4 2.1 %collective-permute-start.6 = (bf16[128,128]{1,0:T(8,128)(2,1)S(1)}, bf16[128,128]{1,0:T(8,128)(2,1)S(1)}, u32[]{:S(2)}, u32[]{:S(2)}) collective-permute-start(bf16[128,128]{1,0:T(8,128)(2,1)S(1)} %get-tuple-element.54), channel_id=1, source_target_pairs={{0,12},{4,8},{8,4},{12,0},{16,28},{20,24},{24,20},{28,16},{1,13},{... | collective-permute-start | bytes 98312 | tf_op jit(solution)/shard_map/ppermute | solution.py:381
  26.5 0.6 convert_convert_fusion
  27.0 0.0 collective-permute-done.4.refs_1_
  27.0 0.4 collective-permute-done.5.refs_2_
  27.4 1.8 %collective-permute-done.6.refs_3_ = bf16[128,128]{1,0:T(8,128)(2,1)S(1)} collective-permute-done((bf16[128,128]{1,0:T(8,128)(2,1)S(1)}, bf16[128,128]{1,0:T(8,128)(2,1)S(1)}, u32[]{:S(2)}, u32[]{:S(2)}) %collective-permute-start.6) | collective-permute-done | bytes 32800 | tf_op jit(solution)/shard_map/ppermute | solution.py:381
  29.2 0.0 copy-start.15
  29.2 0.0 copy-start.8
  29.2 0.0 copy-start.9
  29.2 0.8 shard_map.202
  30.0 0.1 collective-permute-start.8
  30.1 0.1 and.45
  30.2 0.1 eq.47
  30.3 0.2 fusion.5.pick_ref
  30.5 0.7 fusion.12.route_ref
  31.1 0.5 collective-permute-start.7
  31.7 1.6 %collective-permute-start.9 = (bf16[128,512]{1,0:T(8,128)(2,1)S(1)}, bf16[128,512]{1,0:T(8,128)(2,1)S(1)}, u32[]{:S(2)}, u32[]{:S(2)}) collective-permute-start(bf16[128,512]{1,0:T(8,128)(2,1)S(1)} %add_convert_fusion.4), channel_id=1, source_target_pairs={{0,2},{1,3},{2,0},{3,1},{4,6},{5,7},{6,4},{7,5},{8,10},{9,11},{10,... | collective-permute-start | bytes 393224 | tf_op jit(solution)/shard_map/ppermute | solution.py:381
  33.2 0.0 collective-permute-done.7
  33.3 3.9 %collective-permute-done.9.got_ref = bf16[128,512]{1,0:T(8,128)(2,1)S(1)} collective-permute-done((bf16[128,512]{1,0:T(8,128)(2,1)S(1)}, bf16[128,512]{1,0:T(8,128)(2,1)S(1)}, u32[]{:S(2)}, u32[]{:S(2)}) %collective-permute-start.9) | collective-permute-done | bytes 131104 | tf_op jit(solution)/shard_map/ppermute | solution.py:381
  37.2 0.0 copy-start.3
  37.2 0.0 copy-start.4
  37.2 0.8 shard_map.203
  38.0 16.4 %all_to_all.10 = bf16[8,40,512]{2,1,0:T(8,128)(2,1)S(1)} all-to-all(bf16[8,40,512]{2,1,0:T(8,128)(2,1)S(1)} %shard_map.203), channel_id=1, replica_groups=mesh['sp'=8,'tp'=4] {'sp'}, dimensions={0} | all-to-all | bytes 655360 | tf_op jit(solution)/shard_map/all_to_all | solution.py:593
  54.4 0.0 collective-permute-start.12
  54.4 1.6 %collective-permute-start.10 = (bf16[160,512]{1,0:T(8,128)(2,1)S(1)}, bf16[160,512]{1,0:T(8,128)(2,1)S(1)}, u32[]{:S(2)}, u32[]{:S(2)}) collective-permute-start(bf16[160,512]{1,0:T(8,128)(2,1)S(1)} %bitcast.43), channel_id=1, source_target_pairs={{0,2},{1,3},{2,0},{3,1},{4,6},{5,7},{6,4},{7,5},{8,10},{9,11},{10,... | collective-permute-start | bytes 491528 | tf_op jit(solution)/shard_map/ppermute | solution.py:381
  56.0 0.5 collective-permute-start.16
  56.5 5.0 %collective-permute-done.10.refs_1_ = bf16[160,512]{1,0:T(8,128)(2,1)S(1)} collective-permute-done((bf16[160,512]{1,0:T(8,128)(2,1)S(1)}, bf16[160,512]{1,0:T(8,128)(2,1)S(1)}, u32[]{:S(2)}, u32[]{:S(2)}) %collective-permute-start.10) | collective-permute-done | bytes 163872 | tf_op jit(solution)/shard_map/ppermute | solution.py:381
  61.5 0.0 collective-permute-start.11
  61.5 3.0 %collective-permute-done.16.refs_1_ = bf16[160,512]{1,0:T(8,128)(2,1)S(1)} collective-permute-done((bf16[160,512]{1,0:T(8,128)(2,1)S(1)}, bf16[160,512]{1,0:T(8,128)(2,1)S(1)}, u32[]{:S(2)}, u32[]{:S(2)}) %collective-permute-start.16) | collective-permute-done | bytes 163872 | tf_op jit(solution)/shard_map/ppermute | solution.py:381
  64.6 0.0 collective-permute-start.17
  64.6 2.9 %shard_map.204 = (f32[320,1024]{1,0:T(8,128)S(1)}, f32[320,1024]{1,0:T(8,128)S(1)}, f32[320,128]{1,0:T(8,128)S(1)}, f32[320,128]{1,0:T(8,128)S(1)}, f32[8,1024]{...) custom-call(s32[1]{0:T(128)} %bitcast.1.place_ref.refs_0_, ...), custom_call_target="tpu_custom_call" | custom-call | flops 1509949440 | bytes 10092548 | tf_op jit(solution)/shard_map/pallas_call | solution.py:433
  67.6 3.4 %shard_map.205 = (f32[160,512]{1,0:T(8,128)S(1)}, bf16[160,512]{1,0:T(8,128)(2,1)S(1)}, bf16[160,512]{1,0:T(8,128)(2,1)S(1)}, bf16[160,512]{1,0:T(8,128)(2,1)S(1)}) custom-call(s32[1]{0:T(128)} %bitcast.1.place_ref.refs_0_, bf16[160,512]{1,0:T(8,128)(2,1)S(1)} %collective-permute-done.10.refs_1_, bf16[160,512]{1,0:T(8,128)(2,1)S(1)} %collective-permute-done.11.refs_2_, ...), custom_call_target="tpu_custom_call" | custom-call | flops 1509949440 | bytes 18161668 | tf_op jit(solution)/shard_map/pallas_call | solution.py:433
  71.0 0.6 collective-permute-start.14
  71.5 0.1 collective-permute-start.13
  71.6 3.4 %shard_map.206 = (f32[160,512]{1,0:T(8,128)S(1)}, bf16[160,512]{1,0:T(8,128)(2,1)S(1)}, bf16[160,512]{1,0:T(8,128)(2,1)S(1)}, bf16[160,512]{1,0:T(8,128)(2,1)S(1)}) custom-call(s32[1]{0:T(128)} %bitcast.1.place_ref.refs_0_, bf16[160,512]{1,0:T(8,128)(2,1)S(1)} %collective-permute-done.16.refs_1_, bf16[160,512]{1,0:T(8,128)(2,1)S(1)} %collective-permute-done.17.refs_2_, ...), custom_call_target="tpu_custom_call" | custom-call | flops 1509949440 | bytes 18161668 | tf_op jit(solution)/shard_map/pallas_call | solution.py:433
  75.0 0.0 copy-start.13
  75.0 0.5 collective-permute-start.19
  75.5 0.1 collective-permute-start.18
  75.6 1.6 %collective-permute-start.15 = (bf16[160,512]{1,0:T(8,128)(2,1)S(1)}, bf16[160,512]{1,0:T(8,128)(2,1)S(1)}, u32[]{:S(2)}, u32[]{:S(2)}) collective-permute-start(bf16[160,512]{1,0:T(8,128)(2,1)S(1)} %add_convert_fusion.3), channel_id=1, source_target_pairs={{0,2},{1,3},{2,0},{3,1},{4,6},{5,7},{6,4},{7,5},{8,10},{9,11},{10,... | collective-permute-start | bytes 491528 | tf_op jit(solution)/shard_map/ppermute | solution.py:381
  77.3 0.9 collective-permute-start.20
  78.1 4.6 %collective-permute-done.15 = bf16[160,512]{1,0:T(8,128)(2,1)S(1)} collective-permute-done((bf16[160,512]{1,0:T(8,128)(2,1)S(1)}, bf16[160,512]{1,0:T(8,128)(2,1)S(1)}, u32[]{:S(2)}, u32[]{:S(2)}) %collective-permute-start.15) | collective-permute-done | bytes 163872 | tf_op jit(solution)/shard_map/ppermute | solution.py:381
  82.8 0.1 add_convert_fusion.2
  82.8 2.9 %collective-permute-done.20 = bf16[160,512]{1,0:T(8,128)(2,1)S(1)} collective-permute-done((bf16[160,512]{1,0:T(8,128)(2,1)S(1)}, bf16[160,512]{1,0:T(8,128)(2,1)S(1)}, u32[]{:S(2)}, u32[]{:S(2)}) %collective-permute-start.20) | collective-permute-done | bytes 163872 | tf_op jit(solution)/shard_map/ppermute | solution.py:381
  85.7 0.1 add_convert_fusion
  85.8 13.5 %all_to_all.11 = bf16[8,40,512]{2,1,0:T(8,128)(2,1)S(1)} all-to-all(bf16[8,40,512]{2,1,0:T(8,128)(2,1)S(1)} %bitcast.41), channel_id=1, replica_groups=mesh['sp'=8,'tp'=4] {'sp'}, dimensions={0} | all-to-all | bytes 655360 | tf_op jit(solution)/shard_map/all_to_all | solution.py:637
  99.3 0.4 fusion.16
  99.7 0.1 collective-permute-start.21
  99.8 1.1 %collective-permute-done.21 = f32[2,128]{1,0:T(2,128)S(1)} collective-permute-done((f32[2,128]{1,0:T(2,128)S(1)}, f32[2,128]{1,0:T(2,128)S(1)}, u32[]{:S(2)}, u32[]{:S(2)}) %collective-permute-start.21) | collective-permute-done | bytes 1056 | tf_op jit(solution)/shard_map/ppermute | solution.py:381
  101.0 1.6 %collective-permute-start.22 = (f32[2,128]{1,0:T(2,128)S(1)}, f32[2,128]{1,0:T(2,128)S(1)}, u32[]{:S(2)}, u32[]{:S(2)}) collective-permute-start(f32[2,128]{1,0:T(2,128)S(1)} %fusion.15), channel_id=1, source_target_pairs={{0,2},{1,3},{2,0},{3,1},{4,6},{5,7},{6,4},{7,5},{8,10},{9,11},{10,... | collective-permute-start | bytes 3080 | tf_op jit(solution)/shard_map/ppermute | solution.py:381
  102.5 2.1 %collective-permute-done.22 = f32[2,128]{1,0:T(2,128)S(1)} collective-permute-done((f32[2,128]{1,0:T(2,128)S(1)}, f32[2,128]{1,0:T(2,128)S(1)}, u32[]{:S(2)}, u32[]{:S(2)}) %collective-permute-start.22) | collective-permute-done | bytes 1056 | tf_op jit(solution)/shard_map/ppermute | solution.py:381
  104.7 0.8 multiply_convert_fusion
  (49 shorter events, 0.3 us)
Async XLA Ops:
  0.0 9.1 %copy-start.14 = (s32[128,2]{0,1:T(2,128)S(1)}, s32[128,2]{0,1:T(2,128)}, u32[]{:S(2)}) copy-start(s32[128,2]{0,1:T(2,128)} %param.33) | copy-start | bytes 3076
  4.6 5.5 %collective-permute-start = (bf16[272,128]{1,0:T(8,128)(2,1)}, bf16[272,128]{1,0:T(8,128)(2,1)S(1)}, u32[]{:S(2)}, u32[]{:S(2)}) collective-permute-start(bf16[272,128]{1,0:T(8,128)(2,1)} %get-tuple-element.44), channel_id=1, source_target_pairs={{0,4},{4,0},{8,12},{12,8},{16,20},{20,16},{24,28},{28,24},{1,5},{5... | collective-permute-start | bytes 208904 | tf_op jit(solution)/shard_map/ppermute | solution.py:381
  7.5 5.1 %collective-permute-start.1 = (bf16[272,128]{1,0:T(8,128)(2,1)}, bf16[272,128]{1,0:T(8,128)(2,1)S(1)}, u32[]{:S(2)}, u32[]{:S(2)}) collective-permute-start(bf16[272,128]{1,0:T(8,128)(2,1)} %get-tuple-element.45), channel_id=1, source_target_pairs={{0,8},{4,12},{8,0},{12,4},{16,24},{20,28},{24,16},{28,20},{1,9},{5... | collective-permute-start | bytes 208904 | tf_op jit(solution)/shard_map/ppermute | solution.py:381
  9.1 5.4 %collective-permute-start.2 = (bf16[272,128]{1,0:T(8,128)(2,1)}, bf16[272,128]{1,0:T(8,128)(2,1)S(1)}, u32[]{:S(2)}, u32[]{:S(2)}) collective-permute-start(bf16[272,128]{1,0:T(8,128)(2,1)} %get-tuple-element.46), channel_id=1, source_target_pairs={{0,12},{4,8},{8,4},{12,0},{16,28},{20,24},{24,20},{28,16},{1,13},{... | collective-permute-start | bytes 208904 | tf_op jit(solution)/shard_map/ppermute | solution.py:381
  14.5 0.9 copy-start.12
  16.6 6.1 %collective-permute-start.3 = (bf16[144,128]{1,0:T(8,128)(2,1)S(1)}, bf16[144,128]{1,0:T(8,128)(2,1)S(1)}, u32[]{:S(2)}, u32[]{:S(2)}) collective-permute-start(bf16[144,128]{1,0:T(8,128)(2,1)S(1)} %get-tuple-element.47), channel_id=1, source_target_pairs={{0,16},{4,20},{8,24},{12,28},{1,17},{5,21},{9,25},{13,29},{2,18},{... | collective-permute-start | bytes 110600 | tf_op jit(solution)/shard_map/ppermute | solution.py:537
  22.7 6.5 %copy-start.6 = (bf16[512,2048]{1,0:T(8,128)(2,1)S(1)}, bf16[512,2048]{1,0:T(8,128)(2,1)}, u32[]{:S(2)}) copy-start(bf16[512,2048]{1,0:T(8,128)(2,1)} %weight_ref.1) | copy-start | bytes 6291460
  22.7 6.5 %copy-start.7 = (bf16[128,512]{1,0:T(8,128)(2,1)S(1)}, bf16[128,512]{1,0:T(8,128)(2,1)}, u32[]{:S(2)}) copy-start(bf16[128,512]{1,0:T(8,128)(2,1)} %valve_ref.1) | copy-start | bytes 393220
  22.7 6.5 %copy-start.10 = (f32[128,512]{1,0:T(8,128)S(1)}, f32[128,512]{1,0:T(8,128)}, u32[]{:S(2)}) copy-start(f32[128,512]{1,0:T(8,128)} %get-tuple-element.41.local_ref) | copy-start | bytes 786436
  22.7 6.5 %copy-start.11 = (f32[128,512]{1,0:T(8,128)S(1)}, f32[128,512]{1,0:T(8,128)}, u32[]{:S(2)}) copy-start(f32[128,512]{1,0:T(8,128)} %get-tuple-element.42.query_ref) | copy-start | bytes 786436
  22.9 4.1 %collective-permute-start.4 = (bf16[128,128]{1,0:T(8,128)(2,1)S(1)}, bf16[128,128]{1,0:T(8,128)(2,1)S(1)}, u32[]{:S(2)}, u32[]{:S(2)}) collective-permute-start(bf16[128,128]{1,0:T(8,128)(2,1)S(1)} %get-tuple-element.52), channel_id=1, source_target_pairs={{0,4},{4,0},{8,12},{12,8},{16,20},{20,16},{24,28},{28,24},{1,5},{5... | collective-permute-start | bytes 98312 | tf_op jit(solution)/shard_map/ppermute | solution.py:381
  23.5 3.9 %collective-permute-start.5 = (bf16[128,128]{1,0:T(8,128)(2,1)S(1)}, bf16[128,128]{1,0:T(8,128)(2,1)S(1)}, u32[]{:S(2)}, u32[]{:S(2)}) collective-permute-start(bf16[128,128]{1,0:T(8,128)(2,1)S(1)} %get-tuple-element.53), channel_id=1, source_target_pairs={{0,8},{4,12},{8,0},{12,4},{16,24},{20,28},{24,16},{28,20},{1,9},{5... | collective-permute-start | bytes 98312 | tf_op jit(solution)/shard_map/ppermute | solution.py:381
  24.4 4.8 %collective-permute-start.6 = (bf16[128,128]{1,0:T(8,128)(2,1)S(1)}, bf16[128,128]{1,0:T(8,128)(2,1)S(1)}, u32[]{:S(2)}, u32[]{:S(2)}) collective-permute-start(bf16[128,128]{1,0:T(8,128)(2,1)S(1)} %get-tuple-element.54), channel_id=1, source_target_pairs={{0,12},{4,8},{8,4},{12,0},{16,28},{20,24},{24,20},{28,16},{1,13},{... | collective-permute-start | bytes 98312 | tf_op jit(solution)/shard_map/ppermute | solution.py:381
  29.2 1.3 %copy-start.15 = (bf16[128,2]{0,1:T(2,128)(2,1)S(1)}, bf16[128,2]{0,1:T(2,128)(2,1)}, u32[]{:S(2)}) copy-start(bf16[128,2]{0,1:T(2,128)(2,1)} %param.34) | copy-start | bytes 1540
  29.2 7.9 %copy-start.8 = (bf16[128,512]{1,0:T(8,128)(2,1)S(1)}, bf16[128,512]{1,0:T(8,128)(2,1)}, u32[]{:S(2)}) copy-start(bf16[128,512]{1,0:T(8,128)(2,1)} %row_ref.1) | copy-start | bytes 393220
  29.2 7.9 %copy-start.9 = (f32[512]{0:T(512)S(1)}, f32[512]{0:T(512)}, u32[]{:S(2)}) copy-start(f32[512]{0:T(512)} %param.32) | copy-start | bytes 6148
  30.0 1.6 %collective-permute-start.8 = (bf16[128,512]{1,0:T(8,128)(2,1)S(1)}, bf16[128,512]{1,0:T(8,128)(2,1)S(1)}, u32[]{:S(2)}, u32[]{:S(2)}) collective-permute-start(bf16[128,512]{1,0:T(8,128)(2,1)S(1)} %get-tuple-element.58), channel_id=1, source_target_pairs={{0,1},{1,0},{2,3},{3,2},{4,5},{5,4},{6,7},{7,6},{8,9},{9,8},{10,11... | collective-permute-start | bytes 393224 | tf_op jit(solution)/shard_map/ppermute | solution.py:381
  31.1 2.1 %collective-permute-start.7 = (bf16[128,512]{1,0:T(8,128)(2,1)S(1)}, bf16[128,512]{1,0:T(8,128)(2,1)S(1)}, u32[]{:S(2)}, u32[]{:S(2)}) collective-permute-start(bf16[128,512]{1,0:T(8,128)(2,1)S(1)} %get-tuple-element.56), channel_id=1, source_target_pairs={{0,1},{1,0},{2,3},{3,2},{4,5},{5,4},{6,7},{7,6},{8,9},{9,8},{10,11... | collective-permute-start | bytes 393224 | tf_op jit(solution)/shard_map/ppermute | solution.py:381
  31.7 5.5 %collective-permute-start.9 = (bf16[128,512]{1,0:T(8,128)(2,1)S(1)}, bf16[128,512]{1,0:T(8,128)(2,1)S(1)}, u32[]{:S(2)}, u32[]{:S(2)}) collective-permute-start(bf16[128,512]{1,0:T(8,128)(2,1)S(1)} %add_convert_fusion.4), channel_id=1, source_target_pairs={{0,2},{1,3},{2,0},{3,1},{4,6},{5,7},{6,4},{7,5},{8,10},{9,11},{10,... | collective-permute-start | bytes 393224 | tf_op jit(solution)/shard_map/ppermute | solution.py:381
  37.2 27.4 %copy-start = (bf16[1,2048,1024]{2,1,0:T(8,128)(2,1)S(1)}, bf16[1,2048,1024]{2,1,0:T(8,128)(2,1)}, u32[]{:S(2)}) copy-start(bf16[1,2048,1024]{2,1,0:T(8,128)(2,1)} %refs_3_.7) | copy-start | bytes 12582916
  37.2 27.4 %copy-start.1 = (bf16[1,2048,1024]{2,1,0:T(8,128)(2,1)S(1)}, bf16[1,2048,1024]{2,1,0:T(8,128)(2,1)}, u32[]{:S(2)}) copy-start(bf16[1,2048,1024]{2,1,0:T(8,128)(2,1)} %refs_4_.7) | copy-start | bytes 12582916
  37.2 27.4 %copy-start.3 = (bf16[2048,128]{1,0:T(8,128)(2,1)S(1)}, bf16[2048,128]{1,0:T(8,128)(2,1)}, u32[]{:S(2)}) copy-start(bf16[2048,128]{1,0:T(8,128)(2,1)} %refs_5_.7) | copy-start | bytes 1572868
  37.2 27.4 %copy-start.4 = (bf16[2048,128]{1,0:T(8,128)(2,1)S(1)}, bf16[2048,128]{1,0:T(8,128)(2,1)}, u32[]{:S(2)}) copy-start(bf16[2048,128]{1,0:T(8,128)(2,1)} %refs_6_.7) | copy-start | bytes 1572868
  54.4 10.2 %collective-permute-start.12 = (bf16[320,512]{1,0:T(8,128)(2,1)S(1)}, bf16[320,512]{1,0:T(8,128)(2,1)S(1)}, u32[]{:S(2)}, u32[]{:S(2)}) collective-permute-start(bf16[320,512]{1,0:T(8,128)(2,1)S(1)} %bitcast.36), channel_id=1, source_target_pairs={{0,1},{1,0},{2,3},{3,2},{4,5},{5,4},{6,7},{7,6},{8,9},{9,8},{10,11... | collective-permute-start | bytes 983048 | tf_op jit(solution)/shard_map/ppermute | solution.py:381
  54.4 7.1 %collective-permute-start.10 = (bf16[160,512]{1,0:T(8,128)(2,1)S(1)}, bf16[160,512]{1,0:T(8,128)(2,1)S(1)}, u32[]{:S(2)}, u32[]{:S(2)}) collective-permute-start(bf16[160,512]{1,0:T(8,128)(2,1)S(1)} %bitcast.43), channel_id=1, source_target_pairs={{0,2},{1,3},{2,0},{3,1},{4,6},{5,7},{6,4},{7,5},{8,10},{9,11},{10,... | collective-permute-start | bytes 491528 | tf_op jit(solution)/shard_map/ppermute | solution.py:381
  56.0 11.6 %copy-start.2 = (bf16[1,1024,2048]{2,1,0:T(8,128)(2,1)S(1)}, bf16[1,1024,2048]{2,1,0:T(8,128)(2,1)}, u32[]{:S(2)}) copy-start(bf16[1,1024,2048]{2,1,0:T(8,128)(2,1)} %refs_18_.3) | copy-start | bytes 12582916
  56.0 11.6 %copy-start.5 = (bf16[128,2048]{1,0:T(8,128)(2,1)S(1)}, bf16[128,2048]{1,0:T(8,128)(2,1)}, u32[]{:S(2)}) copy-start(bf16[128,2048]{1,0:T(8,128)(2,1)} %refs_19_.3) | copy-start | bytes 1572868
  56.0 8.6 %collective-permute-start.16 = (bf16[160,512]{1,0:T(8,128)(2,1)S(1)}, bf16[160,512]{1,0:T(8,128)(2,1)S(1)}, u32[]{:S(2)}, u32[]{:S(2)}) collective-permute-start(bf16[160,512]{1,0:T(8,128)(2,1)S(1)} %bitcast.42), channel_id=1, source_target_pairs={{0,2},{1,3},{2,0},{3,1},{4,6},{5,7},{6,4},{7,5},{8,10},{9,11},{10,... | collective-permute-start | bytes 491528 | tf_op jit(solution)/shard_map/ppermute | solution.py:381
  61.5 6.0 %collective-permute-start.11 = (bf16[160,512]{1,0:T(8,128)(2,1)S(1)}, bf16[160,512]{1,0:T(8,128)(2,1)S(1)}, u32[]{:S(2)}, u32[]{:S(2)}) collective-permute-start(bf16[160,512]{1,0:T(8,128)(2,1)S(1)} %collective-permute-done.10.refs_1_), channel_id=1, source_target_pairs={{0,1},{1,0},{2,3},{3,2},{4,5},{5,4},{6,7},{7,6},{8,9},{9,8},{10,11... | collective-permute-start | bytes 491528 | tf_op jit(solution)/shard_map/ppermute | solution.py:381
  64.6 7.0 %collective-permute-start.17 = (bf16[160,512]{1,0:T(8,128)(2,1)S(1)}, bf16[160,512]{1,0:T(8,128)(2,1)S(1)}, u32[]{:S(2)}, u32[]{:S(2)}) collective-permute-start(bf16[160,512]{1,0:T(8,128)(2,1)S(1)} %collective-permute-done.16.refs_1_), channel_id=1, source_target_pairs={{0,1},{1,0},{2,3},{3,2},{4,5},{5,4},{6,7},{7,6},{8,9},{9,8},{10,11... | collective-permute-start | bytes 491528 | tf_op jit(solution)/shard_map/ppermute | solution.py:381
  71.0 4.6 %collective-permute-start.14 = (bf16[160,512]{1,0:T(8,128)(2,1)S(1)}, bf16[160,512]{1,0:T(8,128)(2,1)S(1)}, u32[]{:S(2)}, u32[]{:S(2)}) collective-permute-start(bf16[160,512]{1,0:T(8,128)(2,1)S(1)} %get-tuple-element.72), channel_id=1, source_target_pairs={{0,1},{1,0},{2,3},{3,2},{4,5},{5,4},{6,7},{7,6},{8,9},{9,8},{10,11... | collective-permute-start | bytes 491528 | tf_op jit(solution)/shard_map/ppermute | solution.py:381
  71.5 6.6 %collective-permute-start.13 = (bf16[160,512]{1,0:T(8,128)(2,1)S(1)}, bf16[160,512]{1,0:T(8,128)(2,1)S(1)}, u32[]{:S(2)}, u32[]{:S(2)}) collective-permute-start(bf16[160,512]{1,0:T(8,128)(2,1)S(1)} %get-tuple-element.70), channel_id=1, source_target_pairs={{0,1},{1,0},{2,3},{3,2},{4,5},{5,4},{6,7},{7,6},{8,9},{9,8},{10,11... | collective-permute-start | bytes 491528 | tf_op jit(solution)/shard_map/ppermute | solution.py:381
  75.0 29.7 %copy-start.13 = (f32[512]{0:T(512)S(1)}, f32[512]{0:T(512)}, u32[]{:S(2)}) copy-start(f32[512]{0:T(512)} %param.41) | copy-start | bytes 6148
  75.0 2.2 %collective-permute-start.19 = (bf16[160,512]{1,0:T(8,128)(2,1)S(1)}, bf16[160,512]{1,0:T(8,128)(2,1)S(1)}, u32[]{:S(2)}, u32[]{:S(2)}) collective-permute-start(bf16[160,512]{1,0:T(8,128)(2,1)S(1)} %get-tuple-element.76), channel_id=1, source_target_pairs={{0,1},{1,0},{2,3},{3,2},{4,5},{5,4},{6,7},{7,6},{8,9},{9,8},{10,11... | collective-permute-start | bytes 491528 | tf_op jit(solution)/shard_map/ppermute | solution.py:381
  75.5 7.3 %collective-permute-start.18 = (bf16[160,512]{1,0:T(8,128)(2,1)S(1)}, bf16[160,512]{1,0:T(8,128)(2,1)S(1)}, u32[]{:S(2)}, u32[]{:S(2)}) collective-permute-start(bf16[160,512]{1,0:T(8,128)(2,1)S(1)} %get-tuple-element.74), channel_id=1, source_target_pairs={{0,1},{1,0},{2,3},{3,2},{4,5},{5,4},{6,7},{7,6},{8,9},{9,8},{10,11... | collective-permute-start | bytes 491528 | tf_op jit(solution)/shard_map/ppermute | solution.py:381
  75.6 7.1 %collective-permute-start.15 = (bf16[160,512]{1,0:T(8,128)(2,1)S(1)}, bf16[160,512]{1,0:T(8,128)(2,1)S(1)}, u32[]{:S(2)}, u32[]{:S(2)}) collective-permute-start(bf16[160,512]{1,0:T(8,128)(2,1)S(1)} %add_convert_fusion.3), channel_id=1, source_target_pairs={{0,2},{1,3},{2,0},{3,1},{4,6},{5,7},{6,4},{7,5},{8,10},{9,11},{10,... | collective-permute-start | bytes 491528 | tf_op jit(solution)/shard_map/ppermute | solution.py:381
  77.3 8.5 %collective-permute-start.20 = (bf16[160,512]{1,0:T(8,128)(2,1)S(1)}, bf16[160,512]{1,0:T(8,128)(2,1)S(1)}, u32[]{:S(2)}, u32[]{:S(2)}) collective-permute-start(bf16[160,512]{1,0:T(8,128)(2,1)S(1)} %add_convert_fusion.1), channel_id=1, source_target_pairs={{0,2},{1,3},{2,0},{3,1},{4,6},{5,7},{6,4},{7,5},{8,10},{9,11},{10,... | collective-permute-start | bytes 491528 | tf_op jit(solution)/shard_map/ppermute | solution.py:381
  99.7 1.2 %collective-permute-start.21 = (f32[2,128]{1,0:T(2,128)S(1)}, f32[2,128]{1,0:T(2,128)S(1)}, u32[]{:S(2)}, u32[]{:S(2)}) collective-permute-start(f32[2,128]{1,0:T(2,128)S(1)} %pad_maximum_fusion.1), channel_id=1, source_target_pairs={{0,1},{1,0},{2,3},{3,2},{4,5},{5,4},{6,7},{7,6},{8,9},{9,8},{10,11... | collective-permute-start | bytes 3080 | tf_op jit(solution)/shard_map/ppermute | solution.py:381
  101.0 3.6 %collective-permute-start.22 = (f32[2,128]{1,0:T(2,128)S(1)}, f32[2,128]{1,0:T(2,128)S(1)}, u32[]{:S(2)}, u32[]{:S(2)}) collective-permute-start(f32[2,128]{1,0:T(2,128)S(1)} %fusion.15), channel_id=1, source_target_pairs={{0,2},{1,3},{2,0},{3,1},{4,6},{5,7},{6,4},{7,5},{8,10},{9,11},{10,... | collective-permute-start | bytes 3080 | tf_op jit(solution)/shard_map/ppermute | solution.py:381

commit v2 on v1

--- a/solution.py
+++ b/solution.py
@@ -159,6 +159,12 @@
     return ms_ref[j, DK + DK + 8 :].astype(F32)[:1]
 
 
+def hold_kernel(array_ref, out_ref, done_ref):
+    copy = pltpu.make_async_copy(array_ref, out_ref, done_ref)
+    copy.start()
+    copy.wait()
+
+
 def fold_kernel(place_ref, *refs):
     ms_refs = refs[:-6]
     state_ref, map_ref, start_ref, leaving_ref, end_ref, ms_ref = refs[-6:]
@@ -239,8 +245,31 @@
     return rows == lanes % (width // fields)
 
 
-def pack_kernel(capacity, fields, keep_ref, got_ref, row_ref, gain_ref, pick_ref, route_ref, out_ref):
-    experts, slots, width = out_ref.shape
+def route_kernel(capacity, slots, place_ref, named_ref, share_ref, pick_ref, note_ref):
+    top, tokens = named_ref.shape
+    experts = pick_ref.shape[0] // slots
+    named, share = named_ref[...], share_ref[...].astype(F32)
+    taken, signed = [], []
+    for k in range(experts):
+        hit = jnp.where(named == (place_ref[0] ^ k), 1.0, 0.0)
+        taken.append(sum(hit[j : j + 1] for j in range(top)))
+        signed.append(sum(hit[j : j + 1] * share[j : j + 1] * (1.0 if j else -1.0) for j in range(top)))
+    before = lax.broadcasted_iota(jnp.int32, (tokens, tokens), 0)
+    after = lax.broadcasted_iota(jnp.int32, (tokens, tokens), 1)
+    earlier = jnp.where(before < after, 1.0, 0.0).astype(BF16)
+    rank = dot(jnp.concatenate(taken, 0).astype(BF16), earlier)
+    slot = lax.broadcasted_iota(jnp.int32, (slots, tokens), 0).astype(F32)
+    for k in range(experts):
+        chosen = jnp.where(rank[k : k + 1] == slot, taken[k], 0.0)
+        chosen = jnp.where(slot < capacity, chosen, 0.0)
+        here = slice(k * slots, (k + 1) * slots)
+        pick_ref[here] = chosen.astype(BF16)
+        note_ref[here] = jnp.sum(chosen * signed[k], 1, keepdims=True)
+
+
+def pack_kernel(capacity, fields, keep_ref, got_ref, row_ref, gain_ref, pick_ref, share_ref, *out_refs):
+    experts = len(out_refs)
+    slots, width = out_refs[0].shape
     summed = ALPHA * row_ref[...].astype(F32) + (keep_ref[...] + got_ref[...].astype(F32))
     tokens = summed.shape[0]
     mean = jnp.mean(summed, 1, keepdims=True)
@@ -257,11 +286,8 @@
     pick = pick_ref[...]
     body = dot(pick, (centred * gain).astype(BF16))
     notes = dot(pick, notes.astype(BF16))
-    routes = dot(pick, route_ref[...], ((1,), (1,)))
-    expert = (lax.broadcasted_iota(jnp.int32, (experts * slots, 1), 0) // slots + 1).astype(F32)
-    share = jnp.where(routes[:, 2:3] == expert, -routes[:, :1], routes[:, 1:2])
     lane = lax.broadcasted_iota(jnp.int32, (experts * slots, 128), 1)
-    notes = jnp.where(lane == 0, share, notes).astype(BF16)
+    notes = jnp.where(lane == 0, share_ref[...], notes).astype(BF16)
     notes = dot(notes, spread(fields, width))
     mine = own_lane(fields, slots, width)
     gain_high, gain_low = split(gain)
@@ -272,7 +298,7 @@
         block = jnp.where(rows == capacity, info, body[here])
         block = jnp.where(rows == capacity + 1, gain_high.astype(F32), block)
         block = jnp.where(rows == capacity + 2, gain_low.astype(F32), block)
-        out_ref[e] = block.astype(BF16)
+        out_refs[e][...] = block.astype(BF16)
 
 
 def silu(array):
@@ -323,17 +349,16 @@
         note_refs[k][...] = read_notes(piece_refs[k], capacity, slots, fields)
 
 
-def far_kernel(count, half, step, slots, capacity, fields, *refs):
+def far_kernel(count, step, slots, capacity, fields, *refs):
     place_ref, piece_refs = refs[0], refs[1 : count - 1]
     refs = refs[count - 1 :]
     weight_refs, sum_refs, gain_refs, note_refs = refs[:4], refs[4:8], refs[8:12], refs[12:14]
     own_ref, lower_ref, cl_ref = refs[14:17]
     out_refs = refs[17 : 17 + count]
     hidden_ref, shared_ref = refs[17 + count :]
-    height, width = piece_refs[0].shape
-    here = slice(half * height, (half + 1) * height)
+    _, width = piece_refs[0].shape
     at = [pl.ds(pl.multiple_of((place_ref[0] ^ k) * width, width), width) for k in range(2, count)]
-    notes = [note_ref[here] for note_ref in note_refs]
+    notes = [note_ref[...] for note_ref in note_refs]
     notes = notes + [read_notes(piece_ref, capacity, slots, fields) for piece_ref in piece_refs]
     means = [note[:, 1:2] + note[:, 2:3] + note[:, 3:4] for note in notes]
     mean = sum(means) / count
@@ -345,7 +370,7 @@
     share = jnp.abs(share)
 
     def product(weight_ref, sum_ref, gain_ref, cut):
-        total = sum_ref[here, cut]
+        total = sum_ref[:, cut]
         for k in range(2):
             total = total + offsets[k] * gain_ref[k : k + 1, cut]
         for k in range(2, count):
@@ -371,7 +396,7 @@
         cut = pl.ds(pl.multiple_of((place_ref[0] ^ k) * width, width), width)
         term = dot(hidden_ref[...], lower_ref[0, :, cut]) + dot(shared_ref[...], cl_ref[:, cut])
         if k == 0:
-            own = own_ref[here, :].astype(F32)
+            own = own_ref[...].astype(F32)
             term = term + (own + offsets[0] * gain_row(own, capacity)) * (flag * scale * ALPHA)
         out_refs[k][...] = term.astype(out_refs[k].dtype)
 
@@ -508,9 +533,20 @@
     )
 
     def exchange(blocks):
-        return [blocks[0]] + [swap(blocks[k], "sp", k) for k in range(1, heads)]
-
-    mine = exchange(ms)
+        moved = []
+        for k in range(1, heads):
+            moved.append(swap(blocks[k], "sp", k))
+        return [blocks[0]] + moved
+
+    _, *others = exchange(ms)
+    own = call(
+        hold_kernel,
+        [((DK + DK + 16, DV), BF16)],
+        ms[0],
+        in_specs=[pl.BlockSpec(memory_space=pl.ANY)],
+        scratch_shapes=[pltpu.SemaphoreType.DMA(())],
+    )
+    mine = list(own) + others
     states, maps, start, leaving, end = call(
         fold_kernel,
         [
@@ -545,7 +581,7 @@
             states,
             maps,
             in_specs=[smem()] + [vmem()] * 4,
-        )
+        ),
     )
 
     partial = call(
@@ -567,74 +603,80 @@
     experts = specialist_valve_matrix.shape[0] * n_sp
     capacity = max(2, 9 * tokens * top // (8 * experts))
     slots = (capacity + 10) // 8 * 8
-    named = specialist_picks.T[:, None, :] == jnp.arange(experts, dtype=jnp.int32)[None, :, None]
-    taken = jnp.any(named, 0)
-    earlier = jnp.arange(tokens)[:, None] < jnp.arange(tokens)[None, :]
-    rank = jnp.dot(taken.astype(BF16), earlier.astype(BF16), preferred_element_type=F32)
-    slot_index = jnp.arange(slots, dtype=jnp.int32)
-    chosen = taken[:, None, :] & (rank.astype(jnp.int32)[:, None, :] == slot_index[None, :, None])
-    chosen = chosen & (slot_index < capacity)[None, :, None]
-    pick = chosen.astype(BF16).reshape(experts * slots, tokens)
-    routes = jnp.concatenate(
-        [picked_specialist_share.T.astype(F32), (specialist_picks.T[:1] + 1).astype(F32)], 0
-    )
-    routes = jnp.pad(routes, ((0, 13), (0, 0))).astype(BF16)
+    total = experts * slots
+    pick, share = call(
+        functools.partial(route_kernel, capacity, slots),
+        [((total, tokens), BF16), ((total, 1), F32)],
+        lax.axis_index("sp").astype(jnp.int32)[None],
+        specialist_picks.T,
+        picked_specialist_share.T,
+        in_specs=[smem()] + [vmem()] * 2,
+    )
     fields = 8
-    (sent,) = call(
+    sent = call(
         functools.partial(pack_kernel, capacity, fields),
-        [((experts, slots, width), BF16)],
+        [((slots, width), BF16)] * experts,
         keep,
         got,
         incoming_rows_matrix,
         initial_rescale_factor[None, :],
         pick,
-        routes,
-    )
-    arrived = lax.all_to_all(sent, "sp", 0, 0, tiled=True).reshape(experts * slots, width)
-
+        share,
+    )
+
+    def trade(blocks, ks):
+        moved = []
+        for k in ks:
+            moved.append(swap(blocks[k], "sp", k) if k else blocks[k])
+        return moved
+
+    parts = [range(experts // 2, experts), range(experts // 2)]
+    arrived = []
+    for ks in parts:
+        moved = trade(sent, ks)
+        arrived.append(jnp.concatenate(moved, 0))
     hidden = specialist_valve_matrix.shape[2]
     shared = common_valve_matrix.shape[1]
-    total = experts * slots
     step = min(hidden, 256)
     weights = (specialist_valve_matrix, specialist_raising_matrix, common_valve_matrix, common_raising_matrix)
     work = 4 * total * width * (hidden + shared)
-    parts = 2
-    height = total // parts
-    halves = [gather_far(arrived[i * height : (i + 1) * height], "tp") for i in range(parts)]
-    near = gather_near(arrived, "tp")
+    height = total // len(parts)
     common = (step, slots, capacity, fields)
-    partial = call(
-        functools.partial(near_kernel, *common),
-        [((total, hidden), F32)] * 2
-        + [((total, shared), F32)] * 2
-        + [((8, hidden), F32)] * 2
-        + [((8, shared), F32)] * 2
-        + [((total, 128), F32)] * 2,
-        place,
-        *near,
-        *weights,
-        in_specs=[smem()] + [vmem()] * 6,
-        flops=work * 2,
-    )
-    sums = []
-    for i in range(parts):
+    back = {}
+    for i, ks in enumerate(parts):
+        far = gather_far(arrived[i], "tp")
+        near = gather_near(arrived[i], "tp")
+        partial = call(
+            functools.partial(near_kernel, *common),
+            [((height, hidden), F32)] * 2
+            + [((height, shared), F32)] * 2
+            + [((8, hidden), F32)] * 2
+            + [((8, shared), F32)] * 2
+            + [((height, 128), F32)] * 2,
+            place,
+            *near,
+            *weights,
+            in_specs=[smem()] + [vmem()] * 6,
+            flops=work,
+        )
         results = call(
-            functools.partial(far_kernel, n_tp, i, *common),
+            functools.partial(far_kernel, n_tp, *common),
             [((height, width), F32)] + [((height, width), BF16)] * (n_tp - 1),
             place,
-            *halves[i],
+            *far,
             *weights,
             *partial,
-            arrived,
+            arrived[i],
             specialist_lowering_matrix,
             common_lowering_matrix,
             in_specs=[smem()] + [vmem()] * (n_tp + 15),
             scratch_shapes=[pltpu.VMEM((height, hidden), BF16), pltpu.VMEM((height, shared), BF16)],
-            flops=work * n_tp // parts,
+            flops=work * n_tp // 2,
         )
-        sums.append(sum(term.astype(F32) for term in scatter_sum(results, "tp")).astype(BF16))
-    summed = jnp.concatenate(sums, 0).reshape(experts, slots, width)
-    returned = lax.all_to_all(summed, "sp", 0, 0, tiled=True).reshape(total, width)
+        keep, got = scatter_sum(results, "tp")
+        blocks = (keep + got.astype(F32)).astype(BF16).reshape(len(ks), slots, width)
+        back.update(zip(ks, trade({k: blocks[j] for j, k in enumerate(ks)}, ks)))
+    returned = jnp.concatenate([back[k] for k in range(experts)], 0)
     second_sum = lax.dot_general(
         pick, returned, (((0,), (0,)), ((), ())), preferred_element_type=F32
     )

time: 106 us -> 110 us (1.038)
  blocking collectives: 29.8 us -> 0 us
  starting transfers between devices: 22.2 us -> 42.8 us
  waiting for transfers between devices: 31.7 us -> 45.8 us
  other arithmetic: 2.54 us -> 1.08 us
  Pallas kernels: 17.2 us -> 18.3 us
    all_to_all x2 -> x0, blocking collectives: 29.8 us -> none  [the longest x1 16.4 us: shards(): lax.all_to_all(sent, 'sp', 0, 0, tiled=True).reshape(experts * slots, width)]
    ppermute x22 -> x37, starting transfers between devices: 17.7 us -> 38.1 us  [swap(): return lax.ppermute(array, axis, [(i, i ^ bit) for i in range(size)])]
    ppermute x22 -> x37, waiting for transfers between devices: 30.2 us -> 44.4 us  [swap(): return lax.ppermute(array, axis, [(i, i ^ bit) for i in range(size)])]
    pallas_call x8 -> x11, Pallas kernels: 17.2 us -> 18.3 us  [call(): pl.pallas_call(kernel, out_shape=shapes, in_specs=in_specs or [vmem()] *...]
  transfers between devices with their start and end apart: 23 -> 38, of which waited for: 13 -> 20; matrix products, arithmetic and copies ran while one was open for 2% -> 0% of each run, Pallas kernels for 9% -> 10%
where the time goes in v2:
time: 110 us
  waiting for transfers between devices  45.8 us (42%)
  starting transfers between devices  42.8 us (39%)
  Pallas kernels  18.3 us (17%)
    ppermute x37, waiting for transfers between devices, swap(): return lax.ppermute(array, axis, [(i, i ^ bit) for i in range(size)])  44.4 us
    ppermute x37, starting transfers between devices, swap(): return lax.ppermute(array, axis, [(i, i ^ bit) for i in range(size)])  38.1 us
    pallas_call x11, Pallas kernels, call(): pl.pallas_call(kernel, out_shape=shapes, in_specs=in_specs or [vmem()] *...  18.3 us
    ppermute x1, starting transfers between devices, shards(): got = lax.ppermute(leaving, 'sp', onward)  4.66 us
  transfers between devices with their start and end apart: 38, of which 20 were waited for; matrix products, arithmetic and copies ran while one was open for 0% of the time, Pallas kernels for 10%

profile of v2, /device:TPU:0, one launch (start us, length us, event | category | flops | bytes accessed | tf_op | source)
XLA Modules:
  0.0 109.8 jit_solution(9586906551243554475)
XLA Ops:
  0.0 4.6 %shard_map.200 = (bf16[272,128]{1,0:T(8,128)(2,1)}, bf16[272,128]{1,0:T(8,128)(2,1)}, bf16[272,128]{1,0:T(8,128)(2,1)}, bf16[272,128]{1,0:T(8,128)(2,1)}, f32[128,512]{1,0:T(8,128)}, /*index=5*/f32[128,512]{1,0:T(8,128)}) custom-call(s32[1]{0:T(128)} %bitcast.4.refs_0_.place_ref.group_ref, bf16[128,512]{1,0:T(8,128)(2,1)} %refs_1_.1, ...), custom_call_target="tpu_custom_call" | custom-call | flops 2000000000 | bytes 399892 | tf_op jit(solution)/shard_map/pallas_call | solution.py:458
  4.6 3.0 %collective-permute-start = (bf16[272,128]{1,0:T(8,128)(2,1)}, bf16[272,128]{1,0:T(8,128)(2,1)S(1)}, u32[]{:S(2)}, u32[]{:S(2)}) collective-permute-start(bf16[272,128]{1,0:T(8,128)(2,1)} %get-tuple-element.65), channel_id=1, source_target_pairs={{0,4},{4,0},{8,12},{12,8},{16,20},{20,16},{24,28},{28,24},{1,5},{5... | collective-permute-start | bytes 208904 | tf_op jit(solution)/shard_map/ppermute | solution.py:406
  7.6 1.6 %collective-permute-start.1 = (bf16[272,128]{1,0:T(8,128)(2,1)}, bf16[272,128]{1,0:T(8,128)(2,1)S(1)}, u32[]{:S(2)}, u32[]{:S(2)}) collective-permute-start(bf16[272,128]{1,0:T(8,128)(2,1)} %get-tuple-element.66), channel_id=1, source_target_pairs={{0,8},{4,12},{8,0},{12,4},{16,24},{20,28},{24,16},{28,20},{1,9},{5... | collective-permute-start | bytes 208904 | tf_op jit(solution)/shard_map/ppermute | solution.py:406
  9.1 0.9 copy-done.14
  10.1 2.6 %collective-permute-done.1.refs_2_ = bf16[272,128]{1,0:T(8,128)(2,1)S(1)} collective-permute-done((bf16[272,128]{1,0:T(8,128)(2,1)}, bf16[272,128]{1,0:T(8,128)(2,1)S(1)}, u32[]{:S(2)}, u32[]{:S(2)}) %collective-permute-start.1) | collective-permute-done | bytes 69664 | tf_op jit(solution)/shard_map/ppermute | solution.py:406
  12.7 1.9 %collective-permute-done.2.refs_3_ = bf16[272,128]{1,0:T(8,128)(2,1)S(1)} collective-permute-done((bf16[272,128]{1,0:T(8,128)(2,1)}, bf16[272,128]{1,0:T(8,128)(2,1)S(1)}, u32[]{:S(2)}, u32[]{:S(2)}) %collective-permute-start.2) | collective-permute-done | bytes 69664 | tf_op jit(solution)/shard_map/ppermute | solution.py:406
  14.5 1.2 %shard_map.202 = (f32[4,128,128]{2,1,0:T(8,128)S(1)}, bf16[4,128,128]{2,1,0:T(8,128)(2,1)S(1)}, bf16[16,128]{1,0:T(8,128)(2,1)S(1)}, bf16[144,128]{1,0:T(8,128)(2,1)S(1)}, f32[256,128]{1,0:T(8,128)}) custom-call(s32[1]{0:T(128)} %bitcast.4.refs_0_.place_ref.group_ref, bf16[272,128]{1,0:T(8,128)(2,1)S(1)} %shard_map.201.refs_0_, ...), custom_call_target="tpu_custom_call" | custom-call | flops 4000000000 | bytes 278532 | tf_op jit(solution)/shard_map/pallas_call | solution.py:458
  15.7 4.7 %collective-permute-start.3 = (bf16[144,128]{1,0:T(8,128)(2,1)S(1)}, bf16[144,128]{1,0:T(8,128)(2,1)S(1)}, u32[]{:S(2)}, u32[]{:S(2)}) collective-permute-start(bf16[144,128]{1,0:T(8,128)(2,1)S(1)} %get-tuple-element.68), channel_id=1, source_target_pairs={{0,16},{4,20},{8,24},{12,28},{1,17},{5,21},{9,25},{13,29},{2,18},{... | collective-permute-start | bytes 110600 | tf_op jit(solution)/shard_map/ppermute | solution.py:573
  20.4 1.4 %collective-permute-done.3.got_ref = bf16[144,128]{1,0:T(8,128)(2,1)S(1)} collective-permute-done((bf16[144,128]{1,0:T(8,128)(2,1)S(1)}, bf16[144,128]{1,0:T(8,128)(2,1)S(1)}, u32[]{:S(2)}, u32[]{:S(2)}) %collective-permute-start.3) | collective-permute-done | bytes 36896 | tf_op jit(solution)/shard_map/ppermute | solution.py:573
  21.8 0.2 shard_map.203
  22.0 0.6 collective-permute-start.4
  22.6 0.9 collective-permute-start.5
  23.5 2.1 %collective-permute-start.6 = (bf16[128,128]{1,0:T(8,128)(2,1)S(1)}, bf16[128,128]{1,0:T(8,128)(2,1)S(1)}, u32[]{:S(2)}, u32[]{:S(2)}) collective-permute-start(bf16[128,128]{1,0:T(8,128)(2,1)S(1)} %get-tuple-element.75), channel_id=1, source_target_pairs={{0,12},{4,8},{8,4},{12,0},{16,28},{20,24},{24,20},{28,16},{1,13},{... | collective-permute-start | bytes 98312 | tf_op jit(solution)/shard_map/ppermute | solution.py:406
  25.6 0.4 collective-permute-done.4.refs_1_
  26.0 0.5 collective-permute-done.5.refs_2_
  26.5 1.8 %collective-permute-done.6.refs_3_ = bf16[128,128]{1,0:T(8,128)(2,1)S(1)} collective-permute-done((bf16[128,128]{1,0:T(8,128)(2,1)S(1)}, bf16[128,128]{1,0:T(8,128)(2,1)S(1)}, u32[]{:S(2)}, u32[]{:S(2)}) %collective-permute-start.6) | collective-permute-done | bytes 32800 | tf_op jit(solution)/shard_map/ppermute | solution.py:406
  28.3 0.8 shard_map.204
  29.1 0.1 collective-permute-start.8
  29.2 0.2 shard_map.199
  29.5 0.5 collective-permute-start.7
  30.0 0.5 collective-permute-done.8
  30.6 1.6 %collective-permute-start.9 = (bf16[128,512]{1,0:T(8,128)(2,1)S(1)}, bf16[128,512]{1,0:T(8,128)(2,1)S(1)}, u32[]{:S(2)}, u32[]{:S(2)}) collective-permute-start(bf16[128,512]{1,0:T(8,128)(2,1)S(1)} %add_convert_fusion.4), channel_id=1, source_target_pairs={{0,2},{1,3},{2,0},{3,1},{4,6},{5,7},{6,4},{7,5},{8,10},{9,11},{10,... | collective-permute-start | bytes 393224 | tf_op jit(solution)/shard_map/ppermute | solution.py:406
  32.2 4.0 %collective-permute-done.9.got_ref = bf16[128,512]{1,0:T(8,128)(2,1)S(1)} collective-permute-done((bf16[128,512]{1,0:T(8,128)(2,1)S(1)}, bf16[128,512]{1,0:T(8,128)(2,1)S(1)}, u32[]{:S(2)}, u32[]{:S(2)}) %collective-permute-start.9) | collective-permute-done | bytes 131104 | tf_op jit(solution)/shard_map/ppermute | solution.py:406
  36.2 0.6 shard_map.205
  36.9 3.3 %collective-permute-start.22 = (bf16[40,512]{1,0:T(8,128)(2,1)S(1)}, bf16[40,512]{1,0:T(8,128)(2,1)S(1)}, u32[]{:S(2)}, u32[]{:S(2)}) collective-permute-start(bf16[40,512]{1,0:T(8,128)(2,1)S(1)} %get-tuple-element.99), channel_id=1, source_target_pairs={{0,16},{4,20},{8,24},{12,28},{16,0},{20,4},{24,8},{28,12},{1,17},{... | collective-permute-start | bytes 122888 | tf_op jit(solution)/shard_map/ppermute | solution.py:406
  40.1 0.6 collective-permute-start.23
  40.7 3.9 %collective-permute-start.24 = (bf16[40,512]{1,0:T(8,128)(2,1)S(1)}, bf16[40,512]{1,0:T(8,128)(2,1)S(1)}, u32[]{:S(2)}, u32[]{:S(2)}) collective-permute-start(bf16[40,512]{1,0:T(8,128)(2,1)S(1)} %get-tuple-element.101), channel_id=1, source_target_pairs={{0,24},{4,28},{8,16},{12,20},{16,8},{20,12},{24,0},{28,4},{1,25},{... | collective-permute-start | bytes 122888 | tf_op jit(solution)/shard_map/ppermute | solution.py:406
  44.6 0.3 collective-permute-start.25
  45.0 1.1 %collective-permute-start.10 = (bf16[40,512]{1,0:T(8,128)(2,1)S(1)}, bf16[40,512]{1,0:T(8,128)(2,1)S(1)}, u32[]{:S(2)}, u32[]{:S(2)}) collective-permute-start(bf16[40,512]{1,0:T(8,128)(2,1)S(1)} %get-tuple-element.82), channel_id=1, source_target_pairs={{0,4},{4,0},{8,12},{12,8},{16,20},{20,16},{24,28},{28,24},{1,5},{5... | collective-permute-start | bytes 122888 | tf_op jit(solution)/shard_map/ppermute | solution.py:406
  46.1 3.3 %collective-permute-done.10 = bf16[40,512]{1,0:T(8,128)(2,1)S(1)} collective-permute-done((bf16[40,512]{1,0:T(8,128)(2,1)S(1)}, bf16[40,512]{1,0:T(8,128)(2,1)S(1)}, u32[]{:S(2)}, u32[]{:S(2)}) %collective-permute-start.10) | collective-permute-done | bytes 40992 | tf_op jit(solution)/shard_map/ppermute | solution.py:406
  49.3 4.4 %collective-permute-done.11 = bf16[40,512]{1,0:T(8,128)(2,1)S(1)} collective-permute-done((bf16[40,512]{1,0:T(8,128)(2,1)S(1)}, bf16[40,512]{1,0:T(8,128)(2,1)S(1)}, u32[]{:S(2)}, u32[]{:S(2)}) %collective-permute-start.11) | collective-permute-done | bytes 40992 | tf_op jit(solution)/shard_map/ppermute | solution.py:406
  53.7 4.9 %collective-permute-done.12 = bf16[40,512]{1,0:T(8,128)(2,1)S(1)} collective-permute-done((bf16[40,512]{1,0:T(8,128)(2,1)S(1)}, bf16[40,512]{1,0:T(8,128)(2,1)S(1)}, u32[]{:S(2)}, u32[]{:S(2)}) %collective-permute-start.12) | collective-permute-done | bytes 40992 | tf_op jit(solution)/shard_map/ppermute | solution.py:406
  58.6 1.5 %collective-permute-start.13 = (bf16[160,512]{1,0:T(8,128)(2,1)S(1)}, bf16[160,512]{1,0:T(8,128)(2,1)S(1)}, u32[]{:S(2)}, u32[]{:S(2)}) collective-permute-start(bf16[160,512]{1,0:T(8,128)(2,1)S(1)} %constant_dynamic-update-slice_fusion.refs_1_.refs_17_), channel_id=1, source_target_pairs={{0,2},{1,3},{2,0},{3,1},{4,6},{5,7},{6,4},{7,5},{8,10},{9,11},{10,... | collective-permute-start | bytes 491528 | tf_op jit(solution)/shard_map/ppermute | solution.py:406
  60.2 0.6 collective-permute-start.26
  60.8 3.1 %collective-permute-done.13.refs_1_ = bf16[160,512]{1,0:T(8,128)(2,1)S(1)} collective-permute-done((bf16[160,512]{1,0:T(8,128)(2,1)S(1)}, bf16[160,512]{1,0:T(8,128)(2,1)S(1)}, u32[]{:S(2)}, u32[]{:S(2)}) %collective-permute-start.13) | collective-permute-done | bytes 163872 | tf_op jit(solution)/shard_map/ppermute | solution.py:406
  64.0 0.5 collective-permute-start.28
  64.5 1.2 %collective-permute-done.26.refs_1_ = bf16[160,512]{1,0:T(8,128)(2,1)S(1)} collective-permute-done((bf16[160,512]{1,0:T(8,128)(2,1)S(1)}, bf16[160,512]{1,0:T(8,128)(2,1)S(1)}, u32[]{:S(2)}, u32[]{:S(2)}) %collective-permute-start.26) | collective-permute-done | bytes 163872 | tf_op jit(solution)/shard_map/ppermute | solution.py:406
  65.7 2.0 %shard_map.206 = (f32[160,1024]{1,0:T(8,128)S(1)}, f32[160,1024]{1,0:T(8,128)S(1)}, f32[160,128]{1,0:T(8,128)S(1)}, f32[160,128]{1,0:T(8,128)S(1)}, f32[8,1024]{...) custom-call(s32[1]{0:T(128)} %bitcast.3.place_ref.refs_0_, ...), custom_call_target="tpu_custom_call" | custom-call | flops 754974720 | bytes 9764868 | tf_op jit(solution)/shard_map/pallas_call | solution.py:458
  67.8 3.4 %shard_map.207 = (f32[160,512]{1,0:T(8,128)S(1)}, bf16[160,512]{1,0:T(8,128)(2,1)S(1)}, bf16[160,512]{1,0:T(8,128)(2,1)S(1)}, bf16[160,512]{1,0:T(8,128)(2,1)S(1)}) custom-call(s32[1]{0:T(128)} %bitcast.3.place_ref.refs_0_, bf16[160,512]{1,0:T(8,128)(2,1)S(1)} %collective-permute-done.13.refs_1_, bf16[160,512]{1,0:T(8,128)(2,1)S(1)} %collective-permute-done.14.refs_2_, ...), custom_call_target="tpu_custom_call" | custom-call | flops 1509949440 | bytes 16359428 | tf_op jit(solution)/shard_map/pallas_call | solution.py:458
  71.1 0.6 collective-permute-start.17
  71.7 2.0 %shard_map.208 = (f32[160,1024]{1,0:T(8,128)S(1)}, f32[160,1024]{1,0:T(8,128)S(1)}, f32[160,128]{1,0:T(8,128)S(1)}, f32[160,128]{1,0:T(8,128)S(1)}, f32[8,1024]{...) custom-call(s32[1]{0:T(128)} %bitcast.3.place_ref.refs_0_, ...), custom_call_target="tpu_custom_call" | custom-call | flops 754974720 | bytes 9764868 | tf_op jit(solution)/shard_map/pallas_call | solution.py:458
  73.7 3.4 %shard_map.209 = (f32[160,512]{1,0:T(8,128)S(1)}, bf16[160,512]{1,0:T(8,128)(2,1)S(1)}, bf16[160,512]{1,0:T(8,128)(2,1)S(1)}, bf16[160,512]{1,0:T(8,128)(2,1)S(1)}) custom-call(s32[1]{0:T(128)} %bitcast.3.place_ref.refs_0_, bf16[160,512]{1,0:T(8,128)(2,1)S(1)} %collective-permute-done.26.refs_1_, bf16[160,512]{1,0:T(8,128)(2,1)S(1)} %collective-permute-done.27.refs_2_, ...), custom_call_target="tpu_custom_call" | custom-call | flops 1509949440 | bytes 16359428 | tf_op jit(solution)/shard_map/pallas_call | solution.py:458
  77.1 0.1 collective-permute-start.30
  77.2 0.5 collective-permute-start.29
  77.7 0.1 collective-permute-start.16
  77.8 1.5 %collective-permute-start.18 = (bf16[160,512]{1,0:T(8,128)(2,1)S(1)}, bf16[160,512]{1,0:T(8,128)(2,1)S(1)}, u32[]{:S(2)}, u32[]{:S(2)}) collective-permute-start(bf16[160,512]{1,0:T(8,128)(2,1)S(1)} %add_convert_fusion.3), channel_id=1, source_target_pairs={{0,2},{1,3},{2,0},{3,1},{4,6},{5,7},{6,4},{7,5},{8,10},{9,11},{10,... | collective-permute-start | bytes 491528 | tf_op jit(solution)/shard_map/ppermute | solution.py:406
  79.4 0.7 collective-permute-start.31
  80.1 4.8 %collective-permute-done.18 = bf16[160,512]{1,0:T(8,128)(2,1)S(1)} collective-permute-done((bf16[160,512]{1,0:T(8,128)(2,1)S(1)}, bf16[160,512]{1,0:T(8,128)(2,1)S(1)}, u32[]{:S(2)}, u32[]{:S(2)}) %collective-permute-start.18) | collective-permute-done | bytes 163872 | tf_op jit(solution)/shard_map/ppermute | solution.py:406
  85.0 0.8 collective-permute-start.19
  85.9 2.1 %collective-permute-done.31 = bf16[160,512]{1,0:T(8,128)(2,1)S(1)} collective-permute-done((bf16[160,512]{1,0:T(8,128)(2,1)S(1)}, bf16[160,512]{1,0:T(8,128)(2,1)S(1)}, u32[]{:S(2)}, u32[]{:S(2)}) %collective-permute-start.31) | collective-permute-done | bytes 163872 | tf_op jit(solution)/shard_map/ppermute | solution.py:406
  88.0 1.5 %collective-permute-start.32 = (bf16[40,512]{1,0:T(8,128)(2,1)S(1)}, bf16[40,512]{1,0:T(8,128)(2,1)S(1)}, u32[]{:S(2)}, u32[]{:S(2)}) collective-permute-start(bf16[40,512]{1,0:T(8,128)(2,1)S(1)} %get-tuple-element.122), channel_id=1, source_target_pairs={{0,16},{4,20},{8,24},{12,28},{16,0},{20,4},{24,8},{28,12},{1,17},{... | collective-permute-start | bytes 122888 | tf_op jit(solution)/shard_map/ppermute | solution.py:406
  89.5 2.3 %collective-permute-start.20 = (bf16[40,512]{1,0:T(8,128)(2,1)S(1)}, bf16[40,512]{1,0:T(8,128)(2,1)S(1)}, u32[]{:S(2)}, u32[]{:S(2)}) collective-permute-start(bf16[40,512]{1,0:T(8,128)(2,1)S(1)} %get-tuple-element.124), channel_id=1, source_target_pairs={{0,8},{4,12},{8,0},{12,4},{16,24},{20,28},{24,16},{28,20},{1,9},{5... | collective-permute-start | bytes 122888 | tf_op jit(solution)/shard_map/ppermute | solution.py:406
  91.8 0.6 collective-permute-start.21
  92.4 1.5 %collective-permute-start.33 = (bf16[40,512]{1,0:T(8,128)(2,1)S(1)}, bf16[40,512]{1,0:T(8,128)(2,1)S(1)}, u32[]{:S(2)}, u32[]{:S(2)}) collective-permute-start(bf16[40,512]{1,0:T(8,128)(2,1)S(1)} %get-tuple-element.121), channel_id=1, source_target_pairs={{0,20},{4,16},{8,28},{12,24},{16,4},{20,0},{24,12},{28,8},{1,21},{... | collective-permute-start | bytes 122888 | tf_op jit(solution)/shard_map/ppermute | solution.py:406
  93.9 3.2 %collective-permute-start.34 = (bf16[40,512]{1,0:T(8,128)(2,1)S(1)}, bf16[40,512]{1,0:T(8,128)(2,1)S(1)}, u32[]{:S(2)}, u32[]{:S(2)}) collective-permute-start(bf16[40,512]{1,0:T(8,128)(2,1)S(1)} %get-tuple-element.120), channel_id=1, source_target_pairs={{0,24},{4,28},{8,16},{12,20},{16,8},{20,12},{24,0},{28,4},{1,25},{... | collective-permute-start | bytes 122888 | tf_op jit(solution)/shard_map/ppermute | solution.py:406
  97.1 0.9 collective-permute-start.35
  98.0 0.6 collective-permute-done.33
  98.6 1.1 %collective-permute-done.34 = bf16[40,512]{1,0:T(8,128)(2,1)S(1)} collective-permute-done((bf16[40,512]{1,0:T(8,128)(2,1)S(1)}, bf16[40,512]{1,0:T(8,128)(2,1)S(1)}, u32[]{:S(2)}, u32[]{:S(2)}) %collective-permute-start.34) | collective-permute-done | bytes 40992 | tf_op jit(solution)/shard_map/ppermute | solution.py:406
  99.7 4.1 %collective-permute-done.35 = bf16[40,512]{1,0:T(8,128)(2,1)S(1)} collective-permute-done((bf16[40,512]{1,0:T(8,128)(2,1)S(1)}, bf16[40,512]{1,0:T(8,128)(2,1)S(1)}, u32[]{:S(2)}, u32[]{:S(2)}) %collective-permute-start.35) | collective-permute-done | bytes 40992 | tf_op jit(solution)/shard_map/ppermute | solution.py:406
  103.8 0.3 fusion.3
  104.2 1.1 %collective-permute-done.36 = f32[2,128]{1,0:T(2,128)S(1)} collective-permute-done((f32[2,128]{1,0:T(2,128)S(1)}, f32[2,128]{1,0:T(2,128)S(1)}, u32[]{:S(2)}, u32[]{:S(2)}) %collective-permute-start.36) | collective-permute-done | bytes 1056 | tf_op jit(solution)/shard_map/ppermute | solution.py:406
  105.4 1.7 %collective-permute-start.37 = (f32[2,128]{1,0:T(2,128)S(1)}, f32[2,128]{1,0:T(2,128)S(1)}, u32[]{:S(2)}, u32[]{:S(2)}) collective-permute-start(f32[2,128]{1,0:T(2,128)S(1)} %fusion.2), channel_id=1, source_target_pairs={{0,2},{1,3},{2,0},{3,1},{4,6},{5,7},{6,4},{7,5},{8,10},{9,11},{10,... | collective-permute-start | bytes 3080 | tf_op jit(solution)/shard_map/ppermute | solution.py:406
  107.0 2.0 %collective-permute-done.37 = f32[2,128]{1,0:T(2,128)S(1)} collective-permute-done((f32[2,128]{1,0:T(2,128)S(1)}, f32[2,128]{1,0:T(2,128)S(1)}, u32[]{:S(2)}, u32[]{:S(2)}) %collective-permute-start.37) | collective-permute-done | bytes 1056 | tf_op jit(solution)/shard_map/ppermute | solution.py:406
  109.1 0.8 multiply_convert_fusion
  (85 shorter events, 0.7 us)
Async XLA Ops:
  4.6 5.5 %collective-permute-start = (bf16[272,128]{1,0:T(8,128)(2,1)}, bf16[272,128]{1,0:T(8,128)(2,1)S(1)}, u32[]{:S(2)}, u32[]{:S(2)}) collective-permute-start(bf16[272,128]{1,0:T(8,128)(2,1)} %get-tuple-element.65), channel_id=1, source_target_pairs={{0,4},{4,0},{8,12},{12,8},{16,20},{20,16},{24,28},{28,24},{1,5},{5... | collective-permute-start | bytes 208904 | tf_op jit(solution)/shard_map/ppermute | solution.py:406
  7.6 5.1 %collective-permute-start.1 = (bf16[272,128]{1,0:T(8,128)(2,1)}, bf16[272,128]{1,0:T(8,128)(2,1)S(1)}, u32[]{:S(2)}, u32[]{:S(2)}) collective-permute-start(bf16[272,128]{1,0:T(8,128)(2,1)} %get-tuple-element.66), channel_id=1, source_target_pairs={{0,8},{4,12},{8,0},{12,4},{16,24},{20,28},{24,16},{28,20},{1,9},{5... | collective-permute-start | bytes 208904 | tf_op jit(solution)/shard_map/ppermute | solution.py:406
  9.1 5.4 %collective-permute-start.2 = (bf16[272,128]{1,0:T(8,128)(2,1)}, bf16[272,128]{1,0:T(8,128)(2,1)S(1)}, u32[]{:S(2)}, u32[]{:S(2)}) collective-permute-start(bf16[272,128]{1,0:T(8,128)(2,1)} %get-tuple-element.67), channel_id=1, source_target_pairs={{0,12},{4,8},{8,4},{12,0},{16,28},{20,24},{24,20},{28,16},{1,13},{... | collective-permute-start | bytes 208904 | tf_op jit(solution)/shard_map/ppermute | solution.py:406
  9.1 0.9 copy-start.14
  15.7 6.1 %collective-permute-start.3 = (bf16[144,128]{1,0:T(8,128)(2,1)S(1)}, bf16[144,128]{1,0:T(8,128)(2,1)S(1)}, u32[]{:S(2)}, u32[]{:S(2)}) collective-permute-start(bf16[144,128]{1,0:T(8,128)(2,1)S(1)} %get-tuple-element.68), channel_id=1, source_target_pairs={{0,16},{4,20},{8,24},{12,28},{1,17},{5,21},{9,25},{13,29},{2,18},{... | collective-permute-start | bytes 110600 | tf_op jit(solution)/shard_map/ppermute | solution.py:573
  21.8 6.5 %copy-start.6 = (bf16[512,2048]{1,0:T(8,128)(2,1)S(1)}, bf16[512,2048]{1,0:T(8,128)(2,1)}, u32[]{:S(2)}) copy-start(bf16[512,2048]{1,0:T(8,128)(2,1)} %weight_ref.1) | copy-start | bytes 6291460
  21.8 6.5 %copy-start.7 = (bf16[128,512]{1,0:T(8,128)(2,1)S(1)}, bf16[128,512]{1,0:T(8,128)(2,1)}, u32[]{:S(2)}) copy-start(bf16[128,512]{1,0:T(8,128)(2,1)} %valve_ref.1) | copy-start | bytes 393220
  21.8 6.5 %copy-start.12 = (f32[128,512]{1,0:T(8,128)S(1)}, f32[128,512]{1,0:T(8,128)}, u32[]{:S(2)}) copy-start(f32[128,512]{1,0:T(8,128)} %get-tuple-element.62.local_ref) | copy-start | bytes 786436
  21.8 6.5 %copy-start.13 = (f32[128,512]{1,0:T(8,128)S(1)}, f32[128,512]{1,0:T(8,128)}, u32[]{:S(2)}) copy-start(f32[128,512]{1,0:T(8,128)} %get-tuple-element.63.query_ref) | copy-start | bytes 786436
  22.0 4.0 %collective-permute-start.4 = (bf16[128,128]{1,0:T(8,128)(2,1)S(1)}, bf16[128,128]{1,0:T(8,128)(2,1)S(1)}, u32[]{:S(2)}, u32[]{:S(2)}) collective-permute-start(bf16[128,128]{1,0:T(8,128)(2,1)S(1)} %get-tuple-element.73), channel_id=1, source_target_pairs={{0,4},{4,0},{8,12},{12,8},{16,20},{20,16},{24,28},{28,24},{1,5},{5... | collective-permute-start | bytes 98312 | tf_op jit(solution)/shard_map/ppermute | solution.py:406
  22.6 3.9 %collective-permute-start.5 = (bf16[128,128]{1,0:T(8,128)(2,1)S(1)}, bf16[128,128]{1,0:T(8,128)(2,1)S(1)}, u32[]{:S(2)}, u32[]{:S(2)}) collective-permute-start(bf16[128,128]{1,0:T(8,128)(2,1)S(1)} %get-tuple-element.74), channel_id=1, source_target_pairs={{0,8},{4,12},{8,0},{12,4},{16,24},{20,28},{24,16},{28,20},{1,9},{5... | collective-permute-start | bytes 98312 | tf_op jit(solution)/shard_map/ppermute | solution.py:406
  23.5 4.8 %collective-permute-start.6 = (bf16[128,128]{1,0:T(8,128)(2,1)S(1)}, bf16[128,128]{1,0:T(8,128)(2,1)S(1)}, u32[]{:S(2)}, u32[]{:S(2)}) collective-permute-start(bf16[128,128]{1,0:T(8,128)(2,1)S(1)} %get-tuple-element.75), channel_id=1, source_target_pairs={{0,12},{4,8},{8,4},{12,0},{16,28},{20,24},{24,20},{28,16},{1,13},{... | collective-permute-start | bytes 98312 | tf_op jit(solution)/shard_map/ppermute | solution.py:406
  28.3 0.9 copy-start.10
  28.3 0.9 copy-start.11
  29.1 1.4 %collective-permute-start.8 = (bf16[128,512]{1,0:T(8,128)(2,1)S(1)}, bf16[128,512]{1,0:T(8,128)(2,1)S(1)}, u32[]{:S(2)}, u32[]{:S(2)}) collective-permute-start(bf16[128,512]{1,0:T(8,128)(2,1)S(1)} %get-tuple-element.79), channel_id=1, source_target_pairs={{0,1},{1,0},{2,3},{3,2},{4,5},{5,4},{6,7},{7,6},{8,9},{9,8},{10,11... | collective-permute-start | bytes 393224 | tf_op jit(solution)/shard_map/ppermute | solution.py:406
  29.2 7.0 %copy-start.8 = (bf16[128,512]{1,0:T(8,128)(2,1)S(1)}, bf16[128,512]{1,0:T(8,128)(2,1)}, u32[]{:S(2)}) copy-start(bf16[128,512]{1,0:T(8,128)(2,1)} %row_ref.1) | copy-start | bytes 393220
  29.2 7.0 %copy-start.9 = (f32[512]{0:T(512)S(1)}, f32[512]{0:T(512)}, u32[]{:S(2)}) copy-start(f32[512]{0:T(512)} %param.32) | copy-start | bytes 6148
  29.5 2.7 %collective-permute-start.7 = (bf16[128,512]{1,0:T(8,128)(2,1)S(1)}, bf16[128,512]{1,0:T(8,128)(2,1)S(1)}, u32[]{:S(2)}, u32[]{:S(2)}) collective-permute-start(bf16[128,512]{1,0:T(8,128)(2,1)S(1)} %get-tuple-element.77), channel_id=1, source_target_pairs={{0,1},{1,0},{2,3},{3,2},{4,5},{5,4},{6,7},{7,6},{8,9},{9,8},{10,11... | collective-permute-start | bytes 393224 | tf_op jit(solution)/shard_map/ppermute | solution.py:406
  30.6 5.6 %collective-permute-start.9 = (bf16[128,512]{1,0:T(8,128)(2,1)S(1)}, bf16[128,512]{1,0:T(8,128)(2,1)S(1)}, u32[]{:S(2)}, u32[]{:S(2)}) collective-permute-start(bf16[128,512]{1,0:T(8,128)(2,1)S(1)} %add_convert_fusion.4), channel_id=1, source_target_pairs={{0,2},{1,3},{2,0},{3,1},{4,6},{5,7},{6,4},{7,5},{8,10},{9,11},{10,... | collective-permute-start | bytes 393224 | tf_op jit(solution)/shard_map/ppermute | solution.py:406
  36.2 29.5 %copy-start = (bf16[1,2048,1024]{2,1,0:T(8,128)(2,1)S(1)}, bf16[1,2048,1024]{2,1,0:T(8,128)(2,1)}, u32[]{:S(2)}) copy-start(bf16[1,2048,1024]{2,1,0:T(8,128)(2,1)} %refs_3_.9) | copy-start | bytes 12582916
  36.2 29.5 %copy-start.1 = (bf16[1,2048,1024]{2,1,0:T(8,128)(2,1)S(1)}, bf16[1,2048,1024]{2,1,0:T(8,128)(2,1)}, u32[]{:S(2)}) copy-start(bf16[1,2048,1024]{2,1,0:T(8,128)(2,1)} %refs_4_.9) | copy-start | bytes 12582916
  36.2 29.5 %copy-start.3 = (bf16[2048,128]{1,0:T(8,128)(2,1)S(1)}, bf16[2048,128]{1,0:T(8,128)(2,1)}, u32[]{:S(2)}) copy-start(bf16[2048,128]{1,0:T(8,128)(2,1)} %refs_5_.9) | copy-start | bytes 1572868
  36.2 29.5 %copy-start.4 = (bf16[2048,128]{1,0:T(8,128)(2,1)S(1)}, bf16[2048,128]{1,0:T(8,128)(2,1)}, u32[]{:S(2)}) copy-start(bf16[2048,128]{1,0:T(8,128)(2,1)} %refs_6_.9) | copy-start | bytes 1572868
  36.9 23.3 %collective-permute-start.22 = (bf16[40,512]{1,0:T(8,128)(2,1)S(1)}, bf16[40,512]{1,0:T(8,128)(2,1)S(1)}, u32[]{:S(2)}, u32[]{:S(2)}) collective-permute-start(bf16[40,512]{1,0:T(8,128)(2,1)S(1)} %get-tuple-element.99), channel_id=1, source_target_pairs={{0,16},{4,20},{8,24},{12,28},{16,0},{20,4},{24,8},{28,12},{1,17},{... | collective-permute-start | bytes 122888 | tf_op jit(solution)/shard_map/ppermute | solution.py:406
  40.1 20.0 %collective-permute-start.23 = (bf16[40,512]{1,0:T(8,128)(2,1)S(1)}, bf16[40,512]{1,0:T(8,128)(2,1)S(1)}, u32[]{:S(2)}, u32[]{:S(2)}) collective-permute-start(bf16[40,512]{1,0:T(8,128)(2,1)S(1)} %get-tuple-element.100), channel_id=1, source_target_pairs={{0,20},{4,16},{8,28},{12,24},{16,4},{20,0},{24,12},{28,8},{1,21},{... | collective-permute-start | bytes 122888 | tf_op jit(solution)/shard_map/ppermute | solution.py:406
  40.7 19.4 %collective-permute-start.24 = (bf16[40,512]{1,0:T(8,128)(2,1)S(1)}, bf16[40,512]{1,0:T(8,128)(2,1)S(1)}, u32[]{:S(2)}, u32[]{:S(2)}) collective-permute-start(bf16[40,512]{1,0:T(8,128)(2,1)S(1)} %get-tuple-element.101), channel_id=1, source_target_pairs={{0,24},{4,28},{8,16},{12,20},{16,8},{20,12},{24,0},{28,4},{1,25},{... | collective-permute-start | bytes 122888 | tf_op jit(solution)/shard_map/ppermute | solution.py:406
  44.6 15.6 %collective-permute-start.25 = (bf16[40,512]{1,0:T(8,128)(2,1)S(1)}, bf16[40,512]{1,0:T(8,128)(2,1)S(1)}, u32[]{:S(2)}, u32[]{:S(2)}) collective-permute-start(bf16[40,512]{1,0:T(8,128)(2,1)S(1)} %get-tuple-element.102), channel_id=1, source_target_pairs={{0,28},{4,24},{8,20},{12,16},{16,12},{20,8},{24,4},{28,0},{1,29},{... | collective-permute-start | bytes 122888 | tf_op jit(solution)/shard_map/ppermute | solution.py:406
  45.0 4.4 %collective-permute-start.10 = (bf16[40,512]{1,0:T(8,128)(2,1)S(1)}, bf16[40,512]{1,0:T(8,128)(2,1)S(1)}, u32[]{:S(2)}, u32[]{:S(2)}) collective-permute-start(bf16[40,512]{1,0:T(8,128)(2,1)S(1)} %get-tuple-element.82), channel_id=1, source_target_pairs={{0,4},{4,0},{8,12},{12,8},{16,20},{20,16},{24,28},{28,24},{1,5},{5... | collective-permute-start | bytes 122888 | tf_op jit(solution)/shard_map/ppermute | solution.py:406
  49.3 4.4 %collective-permute-start.11 = (bf16[40,512]{1,0:T(8,128)(2,1)S(1)}, bf16[40,512]{1,0:T(8,128)(2,1)S(1)}, u32[]{:S(2)}, u32[]{:S(2)}) collective-permute-start(bf16[40,512]{1,0:T(8,128)(2,1)S(1)} %get-tuple-element.83), channel_id=1, source_target_pairs={{0,8},{4,12},{8,0},{12,4},{16,24},{20,28},{24,16},{28,20},{1,9},{5... | collective-permute-start | bytes 122888 | tf_op jit(solution)/shard_map/ppermute | solution.py:406
  53.7 4.9 %collective-permute-start.12 = (bf16[40,512]{1,0:T(8,128)(2,1)S(1)}, bf16[40,512]{1,0:T(8,128)(2,1)S(1)}, u32[]{:S(2)}, u32[]{:S(2)}) collective-permute-start(bf16[40,512]{1,0:T(8,128)(2,1)S(1)} %get-tuple-element.84), channel_id=1, source_target_pairs={{0,12},{4,8},{8,4},{12,0},{16,28},{20,24},{24,20},{28,16},{1,13},{... | collective-permute-start | bytes 122888 | tf_op jit(solution)/shard_map/ppermute | solution.py:406
  58.6 5.3 %collective-permute-start.13 = (bf16[160,512]{1,0:T(8,128)(2,1)S(1)}, bf16[160,512]{1,0:T(8,128)(2,1)S(1)}, u32[]{:S(2)}, u32[]{:S(2)}) collective-permute-start(bf16[160,512]{1,0:T(8,128)(2,1)S(1)} %constant_dynamic-update-slice_fusion.refs_1_.refs_17_), channel_id=1, source_target_pairs={{0,2},{1,3},{2,0},{3,1},{4,6},{5,7},{6,4},{7,5},{8,10},{9,11},{10,... | collective-permute-start | bytes 491528 | tf_op jit(solution)/shard_map/ppermute | solution.py:406
  60.2 7.6 %copy-start.2 = (bf16[1,1024,2048]{2,1,0:T(8,128)(2,1)S(1)}, bf16[1,1024,2048]{2,1,0:T(8,128)(2,1)}, u32[]{:S(2)}) copy-start(bf16[1,1024,2048]{2,1,0:T(8,128)(2,1)} %refs_18_.3) | copy-start | bytes 12582916
  60.2 7.6 %copy-start.5 = (bf16[128,2048]{1,0:T(8,128)(2,1)S(1)}, bf16[128,2048]{1,0:T(8,128)(2,1)}, u32[]{:S(2)}) copy-start(bf16[128,2048]{1,0:T(8,128)(2,1)} %refs_19_.3) | copy-start | bytes 1572868
  60.2 5.5 %collective-permute-start.26 = (bf16[160,512]{1,0:T(8,128)(2,1)S(1)}, bf16[160,512]{1,0:T(8,128)(2,1)S(1)}, u32[]{:S(2)}, u32[]{:S(2)}) collective-permute-start(bf16[160,512]{1,0:T(8,128)(2,1)S(1)} %constant_dynamic-update-slice_fusion.4.refs_1_.refs_17_), channel_id=1, source_target_pairs={{0,2},{1,3},{2,0},{3,1},{4,6},{5,7},{6,4},{7,5},{8,10},{9,11},{10,... | collective-permute-start | bytes 491528 | tf_op jit(solution)/shard_map/ppermute | solution.py:406
  60.8 4.9 %collective-permute-start.15 = (bf16[160,512]{1,0:T(8,128)(2,1)S(1)}, bf16[160,512]{1,0:T(8,128)(2,1)S(1)}, u32[]{:S(2)}, u32[]{:S(2)}) collective-permute-start(bf16[160,512]{1,0:T(8,128)(2,1)S(1)} %constant_dynamic-update-slice_fusion.refs_1_.refs_17_), channel_id=1, source_target_pairs={{0,1},{1,0},{2,3},{3,2},{4,5},{5,4},{6,7},{7,6},{8,9},{9,8},{10,11... | collective-permute-start | bytes 491528 | tf_op jit(solution)/shard_map/ppermute | solution.py:406
  63.9 3.8 %collective-permute-start.14 = (bf16[160,512]{1,0:T(8,128)(2,1)S(1)}, bf16[160,512]{1,0:T(8,128)(2,1)S(1)}, u32[]{:S(2)}, u32[]{:S(2)}) collective-permute-start(bf16[160,512]{1,0:T(8,128)(2,1)S(1)} %collective-permute-done.13.refs_1_), channel_id=1, source_target_pairs={{0,1},{1,0},{2,3},{3,2},{4,5},{5,4},{6,7},{7,6},{8,9},{9,8},{10,11... | collective-permute-start | bytes 491528 | tf_op jit(solution)/shard_map/ppermute | solution.py:406
  64.0 7.8 %collective-permute-start.28 = (bf16[160,512]{1,0:T(8,128)(2,1)S(1)}, bf16[160,512]{1,0:T(8,128)(2,1)S(1)}, u32[]{:S(2)}, u32[]{:S(2)}) collective-permute-start(bf16[160,512]{1,0:T(8,128)(2,1)S(1)} %constant_dynamic-update-slice_fusion.4.refs_1_.refs_17_), channel_id=1, source_target_pairs={{0,1},{1,0},{2,3},{3,2},{4,5},{5,4},{6,7},{7,6},{8,9},{9,8},{10,11... | collective-permute-start | bytes 491528 | tf_op jit(solution)/shard_map/ppermute | solution.py:406
  65.7 8.0 %collective-permute-start.27 = (bf16[160,512]{1,0:T(8,128)(2,1)S(1)}, bf16[160,512]{1,0:T(8,128)(2,1)S(1)}, u32[]{:S(2)}, u32[]{:S(2)}) collective-permute-start(bf16[160,512]{1,0:T(8,128)(2,1)S(1)} %collective-permute-done.26.refs_1_), channel_id=1, source_target_pairs={{0,1},{1,0},{2,3},{3,2},{4,5},{5,4},{6,7},{7,6},{8,9},{9,8},{10,11... | collective-permute-start | bytes 491528 | tf_op jit(solution)/shard_map/ppermute | solution.py:406
  71.1 6.6 %collective-permute-start.17 = (bf16[160,512]{1,0:T(8,128)(2,1)S(1)}, bf16[160,512]{1,0:T(8,128)(2,1)S(1)}, u32[]{:S(2)}, u32[]{:S(2)}) collective-permute-start(bf16[160,512]{1,0:T(8,128)(2,1)S(1)} %get-tuple-element.98), channel_id=1, source_target_pairs={{0,1},{1,0},{2,3},{3,2},{4,5},{5,4},{6,7},{7,6},{8,9},{9,8},{10,11... | collective-permute-start | bytes 491528 | tf_op jit(solution)/shard_map/ppermute | solution.py:406
  77.1 32.0 %copy-start.15 = (f32[512]{0:T(512)S(1)}, f32[512]{0:T(512)}, u32[]{:S(2)}) copy-start(f32[512]{0:T(512)} %param.41) | copy-start | bytes 6148
  77.1 2.3 %collective-permute-start.30 = (bf16[160,512]{1,0:T(8,128)(2,1)S(1)}, bf16[160,512]{1,0:T(8,128)(2,1)S(1)}, u32[]{:S(2)}, u32[]{:S(2)}) collective-permute-start(bf16[160,512]{1,0:T(8,128)(2,1)S(1)} %get-tuple-element.116), channel_id=1, source_target_pairs={{0,1},{1,0},{2,3},{3,2},{4,5},{5,4},{6,7},{7,6},{8,9},{9,8},{10,11... | collective-permute-start | bytes 491528 | tf_op jit(solution)/shard_map/ppermute | solution.py:406
  77.2 8.7 %collective-permute-start.29 = (bf16[160,512]{1,0:T(8,128)(2,1)S(1)}, bf16[160,512]{1,0:T(8,128)(2,1)S(1)}, u32[]{:S(2)}, u32[]{:S(2)}) collective-permute-start(bf16[160,512]{1,0:T(8,128)(2,1)S(1)} %get-tuple-element.114), channel_id=1, source_target_pairs={{0,1},{1,0},{2,3},{3,2},{4,5},{5,4},{6,7},{7,6},{8,9},{9,8},{10,11... | collective-permute-start | bytes 491528 | tf_op jit(solution)/shard_map/ppermute | solution.py:406
  77.7 2.5 %collective-permute-start.16 = (bf16[160,512]{1,0:T(8,128)(2,1)S(1)}, bf16[160,512]{1,0:T(8,128)(2,1)S(1)}, u32[]{:S(2)}, u32[]{:S(2)}) collective-permute-start(bf16[160,512]{1,0:T(8,128)(2,1)S(1)} %get-tuple-element.96), channel_id=1, source_target_pairs={{0,1},{1,0},{2,3},{3,2},{4,5},{5,4},{6,7},{7,6},{8,9},{9,8},{10,11... | collective-permute-start | bytes 491528 | tf_op jit(solution)/shard_map/ppermute | solution.py:406
  77.8 7.1 %collective-permute-start.18 = (bf16[160,512]{1,0:T(8,128)(2,1)S(1)}, bf16[160,512]{1,0:T(8,128)(2,1)S(1)}, u32[]{:S(2)}, u32[]{:S(2)}) collective-permute-start(bf16[160,512]{1,0:T(8,128)(2,1)S(1)} %add_convert_fusion.3), channel_id=1, source_target_pairs={{0,2},{1,3},{2,0},{3,1},{4,6},{5,7},{6,4},{7,5},{8,10},{9,11},{10,... | collective-permute-start | bytes 491528 | tf_op jit(solution)/shard_map/ppermute | solution.py:406
  79.4 8.5 %collective-permute-start.31 = (bf16[160,512]{1,0:T(8,128)(2,1)S(1)}, bf16[160,512]{1,0:T(8,128)(2,1)S(1)}, u32[]{:S(2)}, u32[]{:S(2)}) collective-permute-start(bf16[160,512]{1,0:T(8,128)(2,1)S(1)} %add_convert_fusion.1), channel_id=1, source_target_pairs={{0,2},{1,3},{2,0},{3,1},{4,6},{5,7},{6,4},{7,5},{8,10},{9,11},{10,... | collective-permute-start | bytes 491528 | tf_op jit(solution)/shard_map/ppermute | solution.py:406
  85.0 8.9 %collective-permute-start.19 = (bf16[40,512]{1,0:T(8,128)(2,1)S(1)}, bf16[40,512]{1,0:T(8,128)(2,1)S(1)}, u32[]{:S(2)}, u32[]{:S(2)}) collective-permute-start(bf16[40,512]{1,0:T(8,128)(2,1)S(1)} %get-tuple-element.125), channel_id=1, source_target_pairs={{0,4},{4,0},{8,12},{12,8},{16,20},{20,16},{24,28},{28,24},{1,5},{5... | collective-permute-start | bytes 122888 | tf_op jit(solution)/shard_map/ppermute | solution.py:406
  88.0 10.0 %collective-permute-start.32 = (bf16[40,512]{1,0:T(8,128)(2,1)S(1)}, bf16[40,512]{1,0:T(8,128)(2,1)S(1)}, u32[]{:S(2)}, u32[]{:S(2)}) collective-permute-start(bf16[40,512]{1,0:T(8,128)(2,1)S(1)} %get-tuple-element.122), channel_id=1, source_target_pairs={{0,16},{4,20},{8,24},{12,28},{16,0},{20,4},{24,8},{28,12},{1,17},{... | collective-permute-start | bytes 122888 | tf_op jit(solution)/shard_map/ppermute | solution.py:406
  89.5 7.6 %collective-permute-start.20 = (bf16[40,512]{1,0:T(8,128)(2,1)S(1)}, bf16[40,512]{1,0:T(8,128)(2,1)S(1)}, u32[]{:S(2)}, u32[]{:S(2)}) collective-permute-start(bf16[40,512]{1,0:T(8,128)(2,1)S(1)} %get-tuple-element.124), channel_id=1, source_target_pairs={{0,8},{4,12},{8,0},{12,4},{16,24},{20,28},{24,16},{28,20},{1,9},{5... | collective-permute-start | bytes 122888 | tf_op jit(solution)/shard_map/ppermute | solution.py:406
  91.8 6.2 %collective-permute-start.21 = (bf16[40,512]{1,0:T(8,128)(2,1)S(1)}, bf16[40,512]{1,0:T(8,128)(2,1)S(1)}, u32[]{:S(2)}, u32[]{:S(2)}) collective-permute-start(bf16[40,512]{1,0:T(8,128)(2,1)S(1)} %get-tuple-element.123), channel_id=1, source_target_pairs={{0,12},{4,8},{8,4},{12,0},{16,28},{20,24},{24,20},{28,16},{1,13},{... | collective-permute-start | bytes 122888 | tf_op jit(solution)/shard_map/ppermute | solution.py:406
  92.4 6.2 %collective-permute-start.33 = (bf16[40,512]{1,0:T(8,128)(2,1)S(1)}, bf16[40,512]{1,0:T(8,128)(2,1)S(1)}, u32[]{:S(2)}, u32[]{:S(2)}) collective-permute-start(bf16[40,512]{1,0:T(8,128)(2,1)S(1)} %get-tuple-element.121), channel_id=1, source_target_pairs={{0,20},{4,16},{8,28},{12,24},{16,4},{20,0},{24,12},{28,8},{1,21},{... | collective-permute-start | bytes 122888 | tf_op jit(solution)/shard_map/ppermute | solution.py:406
  93.9 5.8 %collective-permute-start.34 = (bf16[40,512]{1,0:T(8,128)(2,1)S(1)}, bf16[40,512]{1,0:T(8,128)(2,1)S(1)}, u32[]{:S(2)}, u32[]{:S(2)}) collective-permute-start(bf16[40,512]{1,0:T(8,128)(2,1)S(1)} %get-tuple-element.120), channel_id=1, source_target_pairs={{0,24},{4,28},{8,16},{12,20},{16,8},{20,12},{24,0},{28,4},{1,25},{... | collective-permute-start | bytes 122888 | tf_op jit(solution)/shard_map/ppermute | solution.py:406
  97.1 6.7 %collective-permute-start.35 = (bf16[40,512]{1,0:T(8,128)(2,1)S(1)}, bf16[40,512]{1,0:T(8,128)(2,1)S(1)}, u32[]{:S(2)}, u32[]{:S(2)}) collective-permute-start(bf16[40,512]{1,0:T(8,128)(2,1)S(1)} %get-tuple-element.119), channel_id=1, source_target_pairs={{0,28},{4,24},{8,20},{12,16},{16,12},{20,8},{24,4},{28,0},{1,29},{... | collective-permute-start | bytes 122888 | tf_op jit(solution)/shard_map/ppermute | solution.py:406
  104.1 1.2 %collective-permute-start.36 = (f32[2,128]{1,0:T(2,128)S(1)}, f32[2,128]{1,0:T(2,128)S(1)}, u32[]{:S(2)}, u32[]{:S(2)}) collective-permute-start(f32[2,128]{1,0:T(2,128)S(1)} %pad_maximum_fusion), channel_id=1, source_target_pairs={{0,1},{1,0},{2,3},{3,2},{4,5},{5,4},{6,7},{7,6},{8,9},{9,8},{10,11... | collective-permute-start | bytes 3080 | tf_op jit(solution)/shard_map/ppermute | solution.py:406
  105.4 3.6 %collective-permute-start.37 = (f32[2,128]{1,0:T(2,128)S(1)}, f32[2,128]{1,0:T(2,128)S(1)}, u32[]{:S(2)}, u32[]{:S(2)}) collective-permute-start(f32[2,128]{1,0:T(2,128)S(1)} %fusion.2), channel_id=1, source_target_pairs={{0,2},{1,3},{2,0},{3,1},{4,6},{5,7},{6,4},{7,5},{8,10},{9,11},{10,... | collective-permute-start | bytes 3080 | tf_op jit(solution)/shard_map/ppermute | solution.py:406

commit v3 on v2

--- a/solution.py
+++ b/solution.py
@@ -353,10 +353,10 @@
     place_ref, piece_refs = refs[0], refs[1 : count - 1]
     refs = refs[count - 1 :]
     weight_refs, sum_refs, gain_refs, note_refs = refs[:4], refs[4:8], refs[8:12], refs[12:14]
-    own_ref, lower_ref, cl_ref = refs[14:17]
-    out_refs = refs[17 : 17 + count]
-    hidden_ref, shared_ref = refs[17 + count :]
-    _, width = piece_refs[0].shape
+    lower_ref, cl_ref = refs[14:16]
+    out_refs = refs[16 : 16 + count // 2]
+    hidden_ref, shared_ref, row_ref = refs[16 + count // 2 :]
+    height, width = piece_refs[0].shape
     at = [pl.ds(pl.multiple_of((place_ref[0] ^ k) * width, width), width) for k in range(2, count)]
     notes = [note_ref[...] for note_ref in note_refs]
     notes = notes + [read_notes(piece_ref, capacity, slots, fields) for piece_ref in piece_refs]
@@ -392,13 +392,25 @@
         return 0
 
     lax.fori_loop(0, weight_refs[0].shape[2] // step, chunk, 0)
-    for k in range(count - 1, -1, -1):
-        cut = pl.ds(pl.multiple_of((place_ref[0] ^ k) * width, width), width)
-        term = dot(hidden_ref[...], lower_ref[0, :, cut]) + dot(shared_ref[...], cl_ref[:, cut])
+    lane = lax.broadcasted_iota(jnp.int32, (height, 128), 1)
+    row_ref[...] = jnp.where(lane == 0, offsets[0], flag * scale * ALPHA)
+    for k in range(count - 1, 0, -2):
+        out_refs[k // 2][...] = lowered(place_ref, k, width, hidden_ref, shared_ref, lower_ref, cl_ref).astype(BF16)
+
+
+def lowered(place_ref, k, width, hidden_ref, shared_ref, lower_ref, cl_ref):
+    cut = pl.ds(pl.multiple_of((place_ref[0] ^ k) * width, width), width)
+    return dot(hidden_ref[...], lower_ref[0, :, cut]) + dot(shared_ref[...], cl_ref[:, cut])
+
+
+def tail_kernel(capacity, place_ref, own_ref, hidden_ref, shared_ref, row_ref, lower_ref, cl_ref, *out_refs):
+    width = own_ref.shape[1]
+    for k in range(2 * len(out_refs) - 2, -1, -2):
+        term = lowered(place_ref, k, width, hidden_ref, shared_ref, lower_ref, cl_ref)
         if k == 0:
             own = own_ref[...].astype(F32)
-            term = term + (own + offsets[0] * gain_row(own, capacity)) * (flag * scale * ALPHA)
-        out_refs[k][...] = term.astype(out_refs[k].dtype)
+            term = term + (own + row_ref[:, :1] * gain_row(own, capacity)) * row_ref[:, 1:2]
+        out_refs[k // 2][...] = term.astype(out_refs[k // 2].dtype)
 
 
 def swap(array, axis, bit):
@@ -659,20 +671,32 @@
             in_specs=[smem()] + [vmem()] * 6,
             flops=work,
         )
-        results = call(
+        lowering = (specialist_lowering_matrix, common_lowering_matrix)
+        *sends, inner, outer, notes = call(
             functools.partial(far_kernel, n_tp, *common),
-            [((height, width), F32)] + [((height, width), BF16)] * (n_tp - 1),
+            [((height, width), BF16)] * (n_tp // 2)
+            + [((height, hidden), BF16), ((height, shared), BF16), ((height, 128), F32)],
             place,
             *far,
             *weights,
             *partial,
-            arrived[i],
-            specialist_lowering_matrix,
-            common_lowering_matrix,
-            in_specs=[smem()] + [vmem()] * (n_tp + 15),
-            scratch_shapes=[pltpu.VMEM((height, hidden), BF16), pltpu.VMEM((height, shared), BF16)],
+            *lowering,
+            in_specs=[smem()] + [vmem()] * (n_tp + 14),
             flops=work * n_tp // 2,
         )
+        keeps = call(
+            functools.partial(tail_kernel, capacity),
+            [((height, width), F32)] + [((height, width), BF16)] * (n_tp // 2 - 1),
+            place,
+            arrived[i],
+            inner,
+            outer,
+            notes,
+            *lowering,
+            in_specs=[smem()] + [vmem()] * 6,
+            flops=work // 2,
+        )
+        results = [(sends if k % 2 else keeps)[k // 2] for k in range(n_tp)]
         keep, got = scatter_sum(results, "tp")
         blocks = (keep + got.astype(F32)).astype(BF16).reshape(len(ks), slots, width)
         back.update(zip(ks, trade({k: blocks[j] for j, k in enumerate(ks)}, ks)))

time: 110 us -> 111 us (level)
    pallas_call x11 -> x13, Pallas kernels: 18.3 us -> 18.6 us  [call(): pl.pallas_call(kernel, out_shape=shapes, in_specs=in_specs or [vmem()] *...]
where the time goes in v3:
time: 111 us; the launch traced here: 110 us
  waiting for transfers between devices  46 us (41%)
  starting transfers between devices  42.6 us (38%)
  Pallas kernels  18.6 us (17%)
  local copies, waits for them, and re-layouts  1.29 us (1%)
  other arithmetic  1.11 us (1%)
    ppermute x37, waiting for transfers between devices, swap(): return lax.ppermute(array, axis, [(i, i ^ bit) for i in range(size)])  44.5 us
    ppermute x37, starting transfers between devices, swap(): return lax.ppermute(array, axis, [(i, i ^ bit) for i in range(size)])  38 us
    pallas_call x13, Pallas kernels, call(): pl.pallas_call(kernel, out_shape=shapes, in_specs=in_specs or [vmem()] *...  18.6 us
    ppermute x1, starting transfers between devices, shards(): got = lax.ppermute(leaving, 'sp', onward)  4.66 us
  transfers between devices with their start and end apart: 38, of which 20 were waited for; matrix products, arithmetic and copies ran while one was open for 0% of the time, Pallas kernels for 10%

profile of v3, /device:TPU:0, one launch (start us, length us, event | category | flops | bytes accessed | tf_op | source)
XLA Modules:
  0.0 110.4 jit_solution(5708744863508807791)
XLA Ops:
  0.0 4.6 %shard_map.200 = (bf16[272,128]{1,0:T(8,128)(2,1)}, bf16[272,128]{1,0:T(8,128)(2,1)}, bf16[272,128]{1,0:T(8,128)(2,1)}, bf16[272,128]{1,0:T(8,128)(2,1)}, f32[128,512]{1,0:T(8,128)}, /*index=5*/f32[128,512]{1,0:T(8,128)}) custom-call(s32[1]{0:T(128)} %bitcast.4.refs_0_.place_ref.group_ref, bf16[128,512]{1,0:T(8,128)(2,1)} %refs_1_.1, ...), custom_call_target="tpu_custom_call" | custom-call | flops 2000000000 | bytes 399892 | tf_op jit(solution)/shard_map/pallas_call | solution.py:470
  4.6 3.0 %collective-permute-start = (bf16[272,128]{1,0:T(8,128)(2,1)}, bf16[272,128]{1,0:T(8,128)(2,1)S(1)}, u32[]{:S(2)}, u32[]{:S(2)}) collective-permute-start(bf16[272,128]{1,0:T(8,128)(2,1)} %get-tuple-element.71), channel_id=1, source_target_pairs={{0,4},{4,0},{8,12},{12,8},{16,20},{20,16},{24,28},{28,24},{1,5},{5... | collective-permute-start | bytes 208904 | tf_op jit(solution)/shard_map/ppermute | solution.py:418
  7.5 1.6 %collective-permute-start.1 = (bf16[272,128]{1,0:T(8,128)(2,1)}, bf16[272,128]{1,0:T(8,128)(2,1)S(1)}, u32[]{:S(2)}, u32[]{:S(2)}) collective-permute-start(bf16[272,128]{1,0:T(8,128)(2,1)} %get-tuple-element.72), channel_id=1, source_target_pairs={{0,8},{4,12},{8,0},{12,4},{16,24},{20,28},{24,16},{28,20},{1,9},{5... | collective-permute-start | bytes 208904 | tf_op jit(solution)/shard_map/ppermute | solution.py:418
  9.1 0.9 copy-done.14
  10.1 2.6 %collective-permute-done.1.refs_2_ = bf16[272,128]{1,0:T(8,128)(2,1)S(1)} collective-permute-done((bf16[272,128]{1,0:T(8,128)(2,1)}, bf16[272,128]{1,0:T(8,128)(2,1)S(1)}, u32[]{:S(2)}, u32[]{:S(2)}) %collective-permute-start.1) | collective-permute-done | bytes 69664 | tf_op jit(solution)/shard_map/ppermute | solution.py:418
  12.7 1.9 %collective-permute-done.2.refs_3_ = bf16[272,128]{1,0:T(8,128)(2,1)S(1)} collective-permute-done((bf16[272,128]{1,0:T(8,128)(2,1)}, bf16[272,128]{1,0:T(8,128)(2,1)S(1)}, u32[]{:S(2)}, u32[]{:S(2)}) %collective-permute-start.2) | collective-permute-done | bytes 69664 | tf_op jit(solution)/shard_map/ppermute | solution.py:418
  14.5 1.2 %shard_map.202 = (f32[4,128,128]{2,1,0:T(8,128)S(1)}, bf16[4,128,128]{2,1,0:T(8,128)(2,1)S(1)}, bf16[16,128]{1,0:T(8,128)(2,1)S(1)}, bf16[144,128]{1,0:T(8,128)(2,1)S(1)}, f32[256,128]{1,0:T(8,128)}) custom-call(s32[1]{0:T(128)} %bitcast.4.refs_0_.place_ref.group_ref, bf16[272,128]{1,0:T(8,128)(2,1)S(1)} %shard_map.201.refs_0_, ...), custom_call_target="tpu_custom_call" | custom-call | flops 4000000000 | bytes 278532 | tf_op jit(solution)/shard_map/pallas_call | solution.py:470
  15.7 4.7 %collective-permute-start.3 = (bf16[144,128]{1,0:T(8,128)(2,1)S(1)}, bf16[144,128]{1,0:T(8,128)(2,1)S(1)}, u32[]{:S(2)}, u32[]{:S(2)}) collective-permute-start(bf16[144,128]{1,0:T(8,128)(2,1)S(1)} %get-tuple-element.74), channel_id=1, source_target_pairs={{0,16},{4,20},{8,24},{12,28},{1,17},{5,21},{9,25},{13,29},{2,18},{... | collective-permute-start | bytes 110600 | tf_op jit(solution)/shard_map/ppermute | solution.py:585
  20.4 1.4 %collective-permute-done.3.got_ref = bf16[144,128]{1,0:T(8,128)(2,1)S(1)} collective-permute-done((bf16[144,128]{1,0:T(8,128)(2,1)S(1)}, bf16[144,128]{1,0:T(8,128)(2,1)S(1)}, u32[]{:S(2)}, u32[]{:S(2)}) %collective-permute-start.3) | collective-permute-done | bytes 36896 | tf_op jit(solution)/shard_map/ppermute | solution.py:585
  21.8 0.2 shard_map.203
  22.0 0.6 collective-permute-start.4
  22.6 0.9 collective-permute-start.5
  23.5 2.1 %collective-permute-start.6 = (bf16[128,128]{1,0:T(8,128)(2,1)S(1)}, bf16[128,128]{1,0:T(8,128)(2,1)S(1)}, u32[]{:S(2)}, u32[]{:S(2)}) collective-permute-start(bf16[128,128]{1,0:T(8,128)(2,1)S(1)} %get-tuple-element.81), channel_id=1, source_target_pairs={{0,12},{4,8},{8,4},{12,0},{16,28},{20,24},{24,20},{28,16},{1,13},{... | collective-permute-start | bytes 98312 | tf_op jit(solution)/shard_map/ppermute | solution.py:418
  25.6 0.4 collective-permute-done.4.refs_1_
  26.0 0.5 collective-permute-done.5.refs_2_
  26.5 1.8 %collective-permute-done.6.refs_3_ = bf16[128,128]{1,0:T(8,128)(2,1)S(1)} collective-permute-done((bf16[128,128]{1,0:T(8,128)(2,1)S(1)}, bf16[128,128]{1,0:T(8,128)(2,1)S(1)}, u32[]{:S(2)}, u32[]{:S(2)}) %collective-permute-start.6) | collective-permute-done | bytes 32800 | tf_op jit(solution)/shard_map/ppermute | solution.py:418
  28.3 0.8 shard_map.204
  29.2 0.2 shard_map.199
  29.5 0.5 collective-permute-start.7
  30.0 0.5 collective-permute-done.8
  30.6 1.6 %collective-permute-start.9 = (bf16[128,512]{1,0:T(8,128)(2,1)S(1)}, bf16[128,512]{1,0:T(8,128)(2,1)S(1)}, u32[]{:S(2)}, u32[]{:S(2)}) collective-permute-start(bf16[128,512]{1,0:T(8,128)(2,1)S(1)} %add_convert_fusion.4), channel_id=1, source_target_pairs={{0,2},{1,3},{2,0},{3,1},{4,6},{5,7},{6,4},{7,5},{8,10},{9,11},{10,... | collective-permute-start | bytes 393224 | tf_op jit(solution)/shard_map/ppermute | solution.py:418
  32.2 4.0 %collective-permute-done.9.got_ref = bf16[128,512]{1,0:T(8,128)(2,1)S(1)} collective-permute-done((bf16[128,512]{1,0:T(8,128)(2,1)S(1)}, bf16[128,512]{1,0:T(8,128)(2,1)S(1)}, u32[]{:S(2)}, u32[]{:S(2)}) %collective-permute-start.9) | collective-permute-done | bytes 131104 | tf_op jit(solution)/shard_map/ppermute | solution.py:418
  36.2 0.6 shard_map.205
  36.9 3.3 %collective-permute-start.22 = (bf16[40,512]{1,0:T(8,128)(2,1)S(1)}, bf16[40,512]{1,0:T(8,128)(2,1)S(1)}, u32[]{:S(2)}, u32[]{:S(2)}) collective-permute-start(bf16[40,512]{1,0:T(8,128)(2,1)S(1)} %get-tuple-element.108), channel_id=1, source_target_pairs={{0,16},{4,20},{8,24},{12,28},{16,0},{20,4},{24,8},{28,12},{1,17},{... | collective-permute-start | bytes 122888 | tf_op jit(solution)/shard_map/ppermute | solution.py:418
  40.1 0.6 collective-permute-start.23
  40.7 3.9 %collective-permute-start.24 = (bf16[40,512]{1,0:T(8,128)(2,1)S(1)}, bf16[40,512]{1,0:T(8,128)(2,1)S(1)}, u32[]{:S(2)}, u32[]{:S(2)}) collective-permute-start(bf16[40,512]{1,0:T(8,128)(2,1)S(1)} %get-tuple-element.110), channel_id=1, source_target_pairs={{0,24},{4,28},{8,16},{12,20},{16,8},{20,12},{24,0},{28,4},{1,25},{... | collective-permute-start | bytes 122888 | tf_op jit(solution)/shard_map/ppermute | solution.py:418
  44.6 0.4 collective-permute-start.25
  45.0 1.1 %collective-permute-start.10 = (bf16[40,512]{1,0:T(8,128)(2,1)S(1)}, bf16[40,512]{1,0:T(8,128)(2,1)S(1)}, u32[]{:S(2)}, u32[]{:S(2)}) collective-permute-start(bf16[40,512]{1,0:T(8,128)(2,1)S(1)} %get-tuple-element.88), channel_id=1, source_target_pairs={{0,4},{4,0},{8,12},{12,8},{16,20},{20,16},{24,28},{28,24},{1,5},{5... | collective-permute-start | bytes 122888 | tf_op jit(solution)/shard_map/ppermute | solution.py:418
  46.1 3.3 %collective-permute-done.10 = bf16[40,512]{1,0:T(8,128)(2,1)S(1)} collective-permute-done((bf16[40,512]{1,0:T(8,128)(2,1)S(1)}, bf16[40,512]{1,0:T(8,128)(2,1)S(1)}, u32[]{:S(2)}, u32[]{:S(2)}) %collective-permute-start.10) | collective-permute-done | bytes 40992 | tf_op jit(solution)/shard_map/ppermute | solution.py:418
  49.3 4.4 %collective-permute-done.11 = bf16[40,512]{1,0:T(8,128)(2,1)S(1)} collective-permute-done((bf16[40,512]{1,0:T(8,128)(2,1)S(1)}, bf16[40,512]{1,0:T(8,128)(2,1)S(1)}, u32[]{:S(2)}, u32[]{:S(2)}) %collective-permute-start.11) | collective-permute-done | bytes 40992 | tf_op jit(solution)/shard_map/ppermute | solution.py:418
  53.7 4.9 %collective-permute-done.12 = bf16[40,512]{1,0:T(8,128)(2,1)S(1)} collective-permute-done((bf16[40,512]{1,0:T(8,128)(2,1)S(1)}, bf16[40,512]{1,0:T(8,128)(2,1)S(1)}, u32[]{:S(2)}, u32[]{:S(2)}) %collective-permute-start.12) | collective-permute-done | bytes 40992 | tf_op jit(solution)/shard_map/ppermute | solution.py:418
  58.6 1.5 %collective-permute-start.13 = (bf16[160,512]{1,0:T(8,128)(2,1)S(1)}, bf16[160,512]{1,0:T(8,128)(2,1)S(1)}, u32[]{:S(2)}, u32[]{:S(2)}) collective-permute-start(bf16[160,512]{1,0:T(8,128)(2,1)S(1)} %constant_dynamic-update-slice_fusion.refs_1_.own_ref), channel_id=1, source_target_pairs={{0,2},{1,3},{2,0},{3,1},{4,6},{5,7},{6,4},{7,5},{8,10},{9,11},{10,... | collective-permute-start | bytes 491528 | tf_op jit(solution)/shard_map/ppermute | solution.py:418
  60.2 0.6 collective-permute-start.26
  60.8 0.5 collective-permute-start.15
  61.3 2.6 %collective-permute-done.13.refs_1_ = bf16[160,512]{1,0:T(8,128)(2,1)S(1)} collective-permute-done((bf16[160,512]{1,0:T(8,128)(2,1)S(1)}, bf16[160,512]{1,0:T(8,128)(2,1)S(1)}, u32[]{:S(2)}, u32[]{:S(2)}) %collective-permute-start.13) | collective-permute-done | bytes 163872 | tf_op jit(solution)/shard_map/ppermute | solution.py:418
  64.0 1.8 %collective-permute-done.26.refs_1_ = bf16[160,512]{1,0:T(8,128)(2,1)S(1)} collective-permute-done((bf16[160,512]{1,0:T(8,128)(2,1)S(1)}, bf16[160,512]{1,0:T(8,128)(2,1)S(1)}, u32[]{:S(2)}, u32[]{:S(2)}) %collective-permute-start.26) | collective-permute-done | bytes 163872 | tf_op jit(solution)/shard_map/ppermute | solution.py:418
  65.7 2.0 %shard_map.209 = (f32[160,1024]{1,0:T(8,128)S(1)}, f32[160,1024]{1,0:T(8,128)S(1)}, f32[160,128]{1,0:T(8,128)S(1)}, f32[160,128]{1,0:T(8,128)S(1)}, f32[8,1024]{...) custom-call(s32[1]{0:T(128)} %bitcast.3.place_ref.refs_0_, ...), custom_call_target="tpu_custom_call" | custom-call | flops 754974720 | bytes 9764868 | tf_op jit(solution)/shard_map/pallas_call | solution.py:470
  67.8 2.0 %shard_map.206 = (f32[160,1024]{1,0:T(8,128)S(1)}, f32[160,1024]{1,0:T(8,128)S(1)}, f32[160,128]{1,0:T(8,128)S(1)}, f32[160,128]{1,0:T(8,128)S(1)}, f32[8,1024]{...) custom-call(s32[1]{0:T(128)} %bitcast.3.place_ref.refs_0_, ...), custom_call_target="tpu_custom_call" | custom-call | flops 754974720 | bytes 9764868 | tf_op jit(solution)/shard_map/pallas_call | solution.py:470
  69.8 0.1 copy-done.2
  70.0 2.9 %shard_map.207 = (bf16[160,512]{1,0:T(8,128)(2,1)S(1)}, bf16[160,512]{1,0:T(8,128)(2,1)S(1)}, bf16[160,1024]{1,0:T(8,128)(2,1)S(1)}, bf16[160,128]{1,0:T(8,128)(2,1)S(1)}, f32[160,128]{1,0:T(8,128)S(1)}) custom-call(s32[1]{0:T(128)} %bitcast.3.place_ref.refs_0_, bf16[160,512]{1,0:T(8,128)(2,1)S(1)} %collective-permute-done.13.refs_1_, ...), custom_call_target="tpu_custom_call" | custom-call | flops 1509949440 | bytes 16195588 | tf_op jit(solution)/shard_map/pallas_call | solution.py:470
  73.0 0.6 collective-permute-start.17
  73.5 2.9 %shard_map.210 = (bf16[160,512]{1,0:T(8,128)(2,1)S(1)}, bf16[160,512]{1,0:T(8,128)(2,1)S(1)}, bf16[160,1024]{1,0:T(8,128)(2,1)S(1)}, bf16[160,128]{1,0:T(8,128)(2,1)S(1)}, f32[160,128]{1,0:T(8,128)S(1)}) custom-call(s32[1]{0:T(128)} %bitcast.3.place_ref.refs_0_, bf16[160,512]{1,0:T(8,128)(2,1)S(1)} %collective-permute-done.26.refs_1_, ...), custom_call_target="tpu_custom_call" | custom-call | flops 1509949440 | bytes 16195588 | tf_op jit(solution)/shard_map/pallas_call | solution.py:470
  76.6 0.5 collective-permute-start.29
  77.1 0.6 shard_map.211
  77.7 0.6 shard_map.208
  78.4 1.6 %collective-permute-start.18 = (bf16[160,512]{1,0:T(8,128)(2,1)S(1)}, bf16[160,512]{1,0:T(8,128)(2,1)S(1)}, u32[]{:S(2)}, u32[]{:S(2)}) collective-permute-start(bf16[160,512]{1,0:T(8,128)(2,1)S(1)} %add_convert_fusion.3), channel_id=1, source_target_pairs={{0,2},{1,3},{2,0},{3,1},{4,6},{5,7},{6,4},{7,5},{8,10},{9,11},{10,... | collective-permute-start | bytes 491528 | tf_op jit(solution)/shard_map/ppermute | solution.py:418
  80.0 0.6 collective-permute-start.31
  80.6 4.9 %collective-permute-done.18 = bf16[160,512]{1,0:T(8,128)(2,1)S(1)} collective-permute-done((bf16[160,512]{1,0:T(8,128)(2,1)S(1)}, bf16[160,512]{1,0:T(8,128)(2,1)S(1)}, u32[]{:S(2)}, u32[]{:S(2)}) %collective-permute-start.18) | collective-permute-done | bytes 163872 | tf_op jit(solution)/shard_map/ppermute | solution.py:418
  85.6 0.8 collective-permute-start.19
  86.5 2.0 %collective-permute-done.31 = bf16[160,512]{1,0:T(8,128)(2,1)S(1)} collective-permute-done((bf16[160,512]{1,0:T(8,128)(2,1)S(1)}, bf16[160,512]{1,0:T(8,128)(2,1)S(1)}, u32[]{:S(2)}, u32[]{:S(2)}) %collective-permute-start.31) | collective-permute-done | bytes 163872 | tf_op jit(solution)/shard_map/ppermute | solution.py:418
  88.6 1.5 %collective-permute-start.32 = (bf16[40,512]{1,0:T(8,128)(2,1)S(1)}, bf16[40,512]{1,0:T(8,128)(2,1)S(1)}, u32[]{:S(2)}, u32[]{:S(2)}) collective-permute-start(bf16[40,512]{1,0:T(8,128)(2,1)S(1)} %get-tuple-element.134), channel_id=1, source_target_pairs={{0,16},{4,20},{8,24},{12,28},{16,0},{20,4},{24,8},{28,12},{1,17},{... | collective-permute-start | bytes 122888 | tf_op jit(solution)/shard_map/ppermute | solution.py:418
  90.1 2.3 %collective-permute-start.20 = (bf16[40,512]{1,0:T(8,128)(2,1)S(1)}, bf16[40,512]{1,0:T(8,128)(2,1)S(1)}, u32[]{:S(2)}, u32[]{:S(2)}) collective-permute-start(bf16[40,512]{1,0:T(8,128)(2,1)S(1)} %get-tuple-element.136), channel_id=1, source_target_pairs={{0,8},{4,12},{8,0},{12,4},{16,24},{20,28},{24,16},{28,20},{1,9},{5... | collective-permute-start | bytes 122888 | tf_op jit(solution)/shard_map/ppermute | solution.py:418
  92.4 0.6 collective-permute-start.21
  93.0 1.5 %collective-permute-start.33 = (bf16[40,512]{1,0:T(8,128)(2,1)S(1)}, bf16[40,512]{1,0:T(8,128)(2,1)S(1)}, u32[]{:S(2)}, u32[]{:S(2)}) collective-permute-start(bf16[40,512]{1,0:T(8,128)(2,1)S(1)} %get-tuple-element.133), channel_id=1, source_target_pairs={{0,20},{4,16},{8,28},{12,24},{16,4},{20,0},{24,12},{28,8},{1,21},{... | collective-permute-start | bytes 122888 | tf_op jit(solution)/shard_map/ppermute | solution.py:418
  94.5 3.2 %collective-permute-start.34 = (bf16[40,512]{1,0:T(8,128)(2,1)S(1)}, bf16[40,512]{1,0:T(8,128)(2,1)S(1)}, u32[]{:S(2)}, u32[]{:S(2)}) collective-permute-start(bf16[40,512]{1,0:T(8,128)(2,1)S(1)} %get-tuple-element.132), channel_id=1, source_target_pairs={{0,24},{4,28},{8,16},{12,20},{16,8},{20,12},{24,0},{28,4},{1,25},{... | collective-permute-start | bytes 122888 | tf_op jit(solution)/shard_map/ppermute | solution.py:418
  97.7 0.9 collective-permute-start.35
  98.6 0.6 collective-permute-done.33
  99.1 1.2 %collective-permute-done.34 = bf16[40,512]{1,0:T(8,128)(2,1)S(1)} collective-permute-done((bf16[40,512]{1,0:T(8,128)(2,1)S(1)}, bf16[40,512]{1,0:T(8,128)(2,1)S(1)}, u32[]{:S(2)}, u32[]{:S(2)}) %collective-permute-start.34) | collective-permute-done | bytes 40992 | tf_op jit(solution)/shard_map/ppermute | solution.py:418
  100.3 4.1 %collective-permute-done.35 = bf16[40,512]{1,0:T(8,128)(2,1)S(1)} collective-permute-done((bf16[40,512]{1,0:T(8,128)(2,1)S(1)}, bf16[40,512]{1,0:T(8,128)(2,1)S(1)}, u32[]{:S(2)}, u32[]{:S(2)}) %collective-permute-start.35) | collective-permute-done | bytes 40992 | tf_op jit(solution)/shard_map/ppermute | solution.py:418
  104.4 0.3 fusion.3
  104.8 1.1 %collective-permute-done.36 = f32[2,128]{1,0:T(2,128)S(1)} collective-permute-done((f32[2,128]{1,0:T(2,128)S(1)}, f32[2,128]{1,0:T(2,128)S(1)}, u32[]{:S(2)}, u32[]{:S(2)}) %collective-permute-start.36) | collective-permute-done | bytes 1056 | tf_op jit(solution)/shard_map/ppermute | solution.py:418
  106.0 1.7 %collective-permute-start.37 = (f32[2,128]{1,0:T(2,128)S(1)}, f32[2,128]{1,0:T(2,128)S(1)}, u32[]{:S(2)}, u32[]{:S(2)}) collective-permute-start(f32[2,128]{1,0:T(2,128)S(1)} %fusion.2), channel_id=1, source_target_pairs={{0,2},{1,3},{2,0},{3,1},{4,6},{5,7},{6,4},{7,5},{8,10},{9,11},{10,... | collective-permute-start | bytes 3080 | tf_op jit(solution)/shard_map/ppermute | solution.py:418
  107.6 2.0 %collective-permute-done.37 = f32[2,128]{1,0:T(2,128)S(1)} collective-permute-done((f32[2,128]{1,0:T(2,128)S(1)}, f32[2,128]{1,0:T(2,128)S(1)}, u32[]{:S(2)}, u32[]{:S(2)}) %collective-permute-start.37) | collective-permute-done | bytes 1056 | tf_op jit(solution)/shard_map/ppermute | solution.py:418
  109.6 0.8 multiply_convert_fusion
  (87 shorter events, 1.1 us)
Async XLA Ops:
  4.6 5.5 %collective-permute-start = (bf16[272,128]{1,0:T(8,128)(2,1)}, bf16[272,128]{1,0:T(8,128)(2,1)S(1)}, u32[]{:S(2)}, u32[]{:S(2)}) collective-permute-start(bf16[272,128]{1,0:T(8,128)(2,1)} %get-tuple-element.71), channel_id=1, source_target_pairs={{0,4},{4,0},{8,12},{12,8},{16,20},{20,16},{24,28},{28,24},{1,5},{5... | collective-permute-start | bytes 208904 | tf_op jit(solution)/shard_map/ppermute | solution.py:418
  7.5 5.1 %collective-permute-start.1 = (bf16[272,128]{1,0:T(8,128)(2,1)}, bf16[272,128]{1,0:T(8,128)(2,1)S(1)}, u32[]{:S(2)}, u32[]{:S(2)}) collective-permute-start(bf16[272,128]{1,0:T(8,128)(2,1)} %get-tuple-element.72), channel_id=1, source_target_pairs={{0,8},{4,12},{8,0},{12,4},{16,24},{20,28},{24,16},{28,20},{1,9},{5... | collective-permute-start | bytes 208904 | tf_op jit(solution)/shard_map/ppermute | solution.py:418
  9.1 5.4 %collective-permute-start.2 = (bf16[272,128]{1,0:T(8,128)(2,1)}, bf16[272,128]{1,0:T(8,128)(2,1)S(1)}, u32[]{:S(2)}, u32[]{:S(2)}) collective-permute-start(bf16[272,128]{1,0:T(8,128)(2,1)} %get-tuple-element.73), channel_id=1, source_target_pairs={{0,12},{4,8},{8,4},{12,0},{16,28},{20,24},{24,20},{28,16},{1,13},{... | collective-permute-start | bytes 208904 | tf_op jit(solution)/shard_map/ppermute | solution.py:418
  9.1 0.9 copy-start.14
  15.7 6.1 %collective-permute-start.3 = (bf16[144,128]{1,0:T(8,128)(2,1)S(1)}, bf16[144,128]{1,0:T(8,128)(2,1)S(1)}, u32[]{:S(2)}, u32[]{:S(2)}) collective-permute-start(bf16[144,128]{1,0:T(8,128)(2,1)S(1)} %get-tuple-element.74), channel_id=1, source_target_pairs={{0,16},{4,20},{8,24},{12,28},{1,17},{5,21},{9,25},{13,29},{2,18},{... | collective-permute-start | bytes 110600 | tf_op jit(solution)/shard_map/ppermute | solution.py:585
  21.8 6.5 %copy-start.6 = (bf16[512,2048]{1,0:T(8,128)(2,1)S(1)}, bf16[512,2048]{1,0:T(8,128)(2,1)}, u32[]{:S(2)}) copy-start(bf16[512,2048]{1,0:T(8,128)(2,1)} %weight_ref.1) | copy-start | bytes 6291460
  21.8 6.5 %copy-start.7 = (bf16[128,512]{1,0:T(8,128)(2,1)S(1)}, bf16[128,512]{1,0:T(8,128)(2,1)}, u32[]{:S(2)}) copy-start(bf16[128,512]{1,0:T(8,128)(2,1)} %valve_ref.1) | copy-start | bytes 393220
  21.8 6.5 %copy-start.12 = (f32[128,512]{1,0:T(8,128)S(1)}, f32[128,512]{1,0:T(8,128)}, u32[]{:S(2)}) copy-start(f32[128,512]{1,0:T(8,128)} %get-tuple-element.68.local_ref) | copy-start | bytes 786436
  21.8 6.5 %copy-start.13 = (f32[128,512]{1,0:T(8,128)S(1)}, f32[128,512]{1,0:T(8,128)}, u32[]{:S(2)}) copy-start(f32[128,512]{1,0:T(8,128)} %get-tuple-element.69.query_ref) | copy-start | bytes 786436
  22.0 4.0 %collective-permute-start.4 = (bf16[128,128]{1,0:T(8,128)(2,1)S(1)}, bf16[128,128]{1,0:T(8,128)(2,1)S(1)}, u32[]{:S(2)}, u32[]{:S(2)}) collective-permute-start(bf16[128,128]{1,0:T(8,128)(2,1)S(1)} %get-tuple-element.79), channel_id=1, source_target_pairs={{0,4},{4,0},{8,12},{12,8},{16,20},{20,16},{24,28},{28,24},{1,5},{5... | collective-permute-start | bytes 98312 | tf_op jit(solution)/shard_map/ppermute | solution.py:418
  22.6 3.9 %collective-permute-start.5 = (bf16[128,128]{1,0:T(8,128)(2,1)S(1)}, bf16[128,128]{1,0:T(8,128)(2,1)S(1)}, u32[]{:S(2)}, u32[]{:S(2)}) collective-permute-start(bf16[128,128]{1,0:T(8,128)(2,1)S(1)} %get-tuple-element.80), channel_id=1, source_target_pairs={{0,8},{4,12},{8,0},{12,4},{16,24},{20,28},{24,16},{28,20},{1,9},{5... | collective-permute-start | bytes 98312 | tf_op jit(solution)/shard_map/ppermute | solution.py:418
  23.5 4.8 %collective-permute-start.6 = (bf16[128,128]{1,0:T(8,128)(2,1)S(1)}, bf16[128,128]{1,0:T(8,128)(2,1)S(1)}, u32[]{:S(2)}, u32[]{:S(2)}) collective-permute-start(bf16[128,128]{1,0:T(8,128)(2,1)S(1)} %get-tuple-element.81), channel_id=1, source_target_pairs={{0,12},{4,8},{8,4},{12,0},{16,28},{20,24},{24,20},{28,16},{1,13},{... | collective-permute-start | bytes 98312 | tf_op jit(solution)/shard_map/ppermute | solution.py:418
  28.3 0.9 copy-start.10
  28.3 0.9 copy-start.11
  29.1 1.4 %collective-permute-start.8 = (bf16[128,512]{1,0:T(8,128)(2,1)S(1)}, bf16[128,512]{1,0:T(8,128)(2,1)S(1)}, u32[]{:S(2)}, u32[]{:S(2)}) collective-permute-start(bf16[128,512]{1,0:T(8,128)(2,1)S(1)} %get-tuple-element.85), channel_id=1, source_target_pairs={{0,1},{1,0},{2,3},{3,2},{4,5},{5,4},{6,7},{7,6},{8,9},{9,8},{10,11... | collective-permute-start | bytes 393224 | tf_op jit(solution)/shard_map/ppermute | solution.py:418
  29.2 7.0 %copy-start.8 = (bf16[128,512]{1,0:T(8,128)(2,1)S(1)}, bf16[128,512]{1,0:T(8,128)(2,1)}, u32[]{:S(2)}) copy-start(bf16[128,512]{1,0:T(8,128)(2,1)} %row_ref.1) | copy-start | bytes 393220
  29.2 7.0 %copy-start.9 = (f32[512]{0:T(512)S(1)}, f32[512]{0:T(512)}, u32[]{:S(2)}) copy-start(f32[512]{0:T(512)} %param.32) | copy-start | bytes 6148
  29.5 2.7 %collective-permute-start.7 = (bf16[128,512]{1,0:T(8,128)(2,1)S(1)}, bf16[128,512]{1,0:T(8,128)(2,1)S(1)}, u32[]{:S(2)}, u32[]{:S(2)}) collective-permute-start(bf16[128,512]{1,0:T(8,128)(2,1)S(1)} %get-tuple-element.83), channel_id=1, source_target_pairs={{0,1},{1,0},{2,3},{3,2},{4,5},{5,4},{6,7},{7,6},{8,9},{9,8},{10,11... | collective-permute-start | bytes 393224 | tf_op jit(solution)/shard_map/ppermute | solution.py:418
  30.6 5.6 %collective-permute-start.9 = (bf16[128,512]{1,0:T(8,128)(2,1)S(1)}, bf16[128,512]{1,0:T(8,128)(2,1)S(1)}, u32[]{:S(2)}, u32[]{:S(2)}) collective-permute-start(bf16[128,512]{1,0:T(8,128)(2,1)S(1)} %add_convert_fusion.4), channel_id=1, source_target_pairs={{0,2},{1,3},{2,0},{3,1},{4,6},{5,7},{6,4},{7,5},{8,10},{9,11},{10,... | collective-permute-start | bytes 393224 | tf_op jit(solution)/shard_map/ppermute | solution.py:418
  36.2 29.5 %copy-start = (bf16[1,2048,1024]{2,1,0:T(8,128)(2,1)S(1)}, bf16[1,2048,1024]{2,1,0:T(8,128)(2,1)}, u32[]{:S(2)}) copy-start(bf16[1,2048,1024]{2,1,0:T(8,128)(2,1)} %refs_3_.9) | copy-start | bytes 12582916
  36.2 29.5 %copy-start.1 = (bf16[1,2048,1024]{2,1,0:T(8,128)(2,1)S(1)}, bf16[1,2048,1024]{2,1,0:T(8,128)(2,1)}, u32[]{:S(2)}) copy-start(bf16[1,2048,1024]{2,1,0:T(8,128)(2,1)} %refs_4_.9) | copy-start | bytes 12582916
  36.2 29.5 %copy-start.3 = (bf16[2048,128]{1,0:T(8,128)(2,1)S(1)}, bf16[2048,128]{1,0:T(8,128)(2,1)}, u32[]{:S(2)}) copy-start(bf16[2048,128]{1,0:T(8,128)(2,1)} %refs_5_.9) | copy-start | bytes 1572868
  36.2 29.5 %copy-start.4 = (bf16[2048,128]{1,0:T(8,128)(2,1)S(1)}, bf16[2048,128]{1,0:T(8,128)(2,1)}, u32[]{:S(2)}) copy-start(bf16[2048,128]{1,0:T(8,128)(2,1)} %refs_6_.9) | copy-start | bytes 1572868
  36.9 23.3 %collective-permute-start.22 = (bf16[40,512]{1,0:T(8,128)(2,1)S(1)}, bf16[40,512]{1,0:T(8,128)(2,1)S(1)}, u32[]{:S(2)}, u32[]{:S(2)}) collective-permute-start(bf16[40,512]{1,0:T(8,128)(2,1)S(1)} %get-tuple-element.108), channel_id=1, source_target_pairs={{0,16},{4,20},{8,24},{12,28},{16,0},{20,4},{24,8},{28,12},{1,17},{... | collective-permute-start | bytes 122888 | tf_op jit(solution)/shard_map/ppermute | solution.py:418
  40.1 20.0 %collective-permute-start.23 = (bf16[40,512]{1,0:T(8,128)(2,1)S(1)}, bf16[40,512]{1,0:T(8,128)(2,1)S(1)}, u32[]{:S(2)}, u32[]{:S(2)}) collective-permute-start(bf16[40,512]{1,0:T(8,128)(2,1)S(1)} %get-tuple-element.109), channel_id=1, source_target_pairs={{0,20},{4,16},{8,28},{12,24},{16,4},{20,0},{24,12},{28,8},{1,21},{... | collective-permute-start | bytes 122888 | tf_op jit(solution)/shard_map/ppermute | solution.py:418
  40.7 19.4 %collective-permute-start.24 = (bf16[40,512]{1,0:T(8,128)(2,1)S(1)}, bf16[40,512]{1,0:T(8,128)(2,1)S(1)}, u32[]{:S(2)}, u32[]{:S(2)}) collective-permute-start(bf16[40,512]{1,0:T(8,128)(2,1)S(1)} %get-tuple-element.110), channel_id=1, source_target_pairs={{0,24},{4,28},{8,16},{12,20},{16,8},{20,12},{24,0},{28,4},{1,25},{... | collective-permute-start | bytes 122888 | tf_op jit(solution)/shard_map/ppermute | solution.py:418
  44.6 15.6 %collective-permute-start.25 = (bf16[40,512]{1,0:T(8,128)(2,1)S(1)}, bf16[40,512]{1,0:T(8,128)(2,1)S(1)}, u32[]{:S(2)}, u32[]{:S(2)}) collective-permute-start(bf16[40,512]{1,0:T(8,128)(2,1)S(1)} %get-tuple-element.111), channel_id=1, source_target_pairs={{0,28},{4,24},{8,20},{12,16},{16,12},{20,8},{24,4},{28,0},{1,29},{... | collective-permute-start | bytes 122888 | tf_op jit(solution)/shard_map/ppermute | solution.py:418
  45.0 4.4 %collective-permute-start.10 = (bf16[40,512]{1,0:T(8,128)(2,1)S(1)}, bf16[40,512]{1,0:T(8,128)(2,1)S(1)}, u32[]{:S(2)}, u32[]{:S(2)}) collective-permute-start(bf16[40,512]{1,0:T(8,128)(2,1)S(1)} %get-tuple-element.88), channel_id=1, source_target_pairs={{0,4},{4,0},{8,12},{12,8},{16,20},{20,16},{24,28},{28,24},{1,5},{5... | collective-permute-start | bytes 122888 | tf_op jit(solution)/shard_map/ppermute | solution.py:418
  49.3 4.4 %collective-permute-start.11 = (bf16[40,512]{1,0:T(8,128)(2,1)S(1)}, bf16[40,512]{1,0:T(8,128)(2,1)S(1)}, u32[]{:S(2)}, u32[]{:S(2)}) collective-permute-start(bf16[40,512]{1,0:T(8,128)(2,1)S(1)} %get-tuple-element.89), channel_id=1, source_target_pairs={{0,8},{4,12},{8,0},{12,4},{16,24},{20,28},{24,16},{28,20},{1,9},{5... | collective-permute-start | bytes 122888 | tf_op jit(solution)/shard_map/ppermute | solution.py:418
  53.7 4.9 %collective-permute-start.12 = (bf16[40,512]{1,0:T(8,128)(2,1)S(1)}, bf16[40,512]{1,0:T(8,128)(2,1)S(1)}, u32[]{:S(2)}, u32[]{:S(2)}) collective-permute-start(bf16[40,512]{1,0:T(8,128)(2,1)S(1)} %get-tuple-element.90), channel_id=1, source_target_pairs={{0,12},{4,8},{8,4},{12,0},{16,28},{20,24},{24,20},{28,16},{1,13},{... | collective-permute-start | bytes 122888 | tf_op jit(solution)/shard_map/ppermute | solution.py:418
  58.6 5.3 %collective-permute-start.13 = (bf16[160,512]{1,0:T(8,128)(2,1)S(1)}, bf16[160,512]{1,0:T(8,128)(2,1)S(1)}, u32[]{:S(2)}, u32[]{:S(2)}) collective-permute-start(bf16[160,512]{1,0:T(8,128)(2,1)S(1)} %constant_dynamic-update-slice_fusion.refs_1_.own_ref), channel_id=1, source_target_pairs={{0,2},{1,3},{2,0},{3,1},{4,6},{5,7},{6,4},{7,5},{8,10},{9,11},{10,... | collective-permute-start | bytes 491528 | tf_op jit(solution)/shard_map/ppermute | solution.py:418
  60.2 5.5 %collective-permute-start.26 = (bf16[160,512]{1,0:T(8,128)(2,1)S(1)}, bf16[160,512]{1,0:T(8,128)(2,1)S(1)}, u32[]{:S(2)}, u32[]{:S(2)}) collective-permute-start(bf16[160,512]{1,0:T(8,128)(2,1)S(1)} %constant_dynamic-update-slice_fusion.4.refs_1_.own_ref), channel_id=1, source_target_pairs={{0,2},{1,3},{2,0},{3,1},{4,6},{5,7},{6,4},{7,5},{8,10},{9,11},{10,... | collective-permute-start | bytes 491528 | tf_op jit(solution)/shard_map/ppermute | solution.py:418
  60.8 4.9 %collective-permute-start.28 = (bf16[160,512]{1,0:T(8,128)(2,1)S(1)}, bf16[160,512]{1,0:T(8,128)(2,1)S(1)}, u32[]{:S(2)}, u32[]{:S(2)}) collective-permute-start(bf16[160,512]{1,0:T(8,128)(2,1)S(1)} %constant_dynamic-update-slice_fusion.4.refs_1_.own_ref), channel_id=1, source_target_pairs={{0,1},{1,0},{2,3},{3,2},{4,5},{5,4},{6,7},{7,6},{8,9},{9,8},{10,11... | collective-permute-start | bytes 491528 | tf_op jit(solution)/shard_map/ppermute | solution.py:418
  60.8 7.0 %collective-permute-start.15 = (bf16[160,512]{1,0:T(8,128)(2,1)S(1)}, bf16[160,512]{1,0:T(8,128)(2,1)S(1)}, u32[]{:S(2)}, u32[]{:S(2)}) collective-permute-start(bf16[160,512]{1,0:T(8,128)(2,1)S(1)} %constant_dynamic-update-slice_fusion.refs_1_.own_ref), channel_id=1, source_target_pairs={{0,1},{1,0},{2,3},{3,2},{4,5},{5,4},{6,7},{7,6},{8,9},{9,8},{10,11... | collective-permute-start | bytes 491528 | tf_op jit(solution)/shard_map/ppermute | solution.py:418
  63.9 5.8 %collective-permute-start.14 = (bf16[160,512]{1,0:T(8,128)(2,1)S(1)}, bf16[160,512]{1,0:T(8,128)(2,1)S(1)}, u32[]{:S(2)}, u32[]{:S(2)}) collective-permute-start(bf16[160,512]{1,0:T(8,128)(2,1)S(1)} %collective-permute-done.13.refs_1_), channel_id=1, source_target_pairs={{0,1},{1,0},{2,3},{3,2},{4,5},{5,4},{6,7},{7,6},{8,9},{9,8},{10,11... | collective-permute-start | bytes 491528 | tf_op jit(solution)/shard_map/ppermute | solution.py:418
  65.7 7.8 %collective-permute-start.27 = (bf16[160,512]{1,0:T(8,128)(2,1)S(1)}, bf16[160,512]{1,0:T(8,128)(2,1)S(1)}, u32[]{:S(2)}, u32[]{:S(2)}) collective-permute-start(bf16[160,512]{1,0:T(8,128)(2,1)S(1)} %collective-permute-done.26.refs_1_), channel_id=1, source_target_pairs={{0,1},{1,0},{2,3},{3,2},{4,5},{5,4},{6,7},{7,6},{8,9},{9,8},{10,11... | collective-permute-start | bytes 491528 | tf_op jit(solution)/shard_map/ppermute | solution.py:418
  67.7 2.2 %copy-start.2 = (bf16[1,1024,2048]{2,1,0:T(8,128)(2,1)S(1)}, bf16[1,1024,2048]{2,1,0:T(8,128)(2,1)}, u32[]{:S(2)}) copy-start(bf16[1,1024,2048]{2,1,0:T(8,128)(2,1)} %lower_ref.3) | copy-start | bytes 12582916
  67.8 2.3 %copy-start.5 = (bf16[128,2048]{1,0:T(8,128)(2,1)S(1)}, bf16[128,2048]{1,0:T(8,128)(2,1)}, u32[]{:S(2)}) copy-start(bf16[128,2048]{1,0:T(8,128)(2,1)} %cl_ref.3) | copy-start | bytes 1572868
  73.0 5.4 %collective-permute-start.17 = (bf16[160,512]{1,0:T(8,128)(2,1)S(1)}, bf16[160,512]{1,0:T(8,128)(2,1)S(1)}, u32[]{:S(2)}, u32[]{:S(2)}) collective-permute-start(bf16[160,512]{1,0:T(8,128)(2,1)S(1)} %get-tuple-element.107), channel_id=1, source_target_pairs={{0,1},{1,0},{2,3},{3,2},{4,5},{5,4},{6,7},{7,6},{8,9},{9,8},{10,11... | collective-permute-start | bytes 491528 | tf_op jit(solution)/shard_map/ppermute | solution.py:418
  76.5 3.5 %collective-permute-start.30 = (bf16[160,512]{1,0:T(8,128)(2,1)S(1)}, bf16[160,512]{1,0:T(8,128)(2,1)S(1)}, u32[]{:S(2)}, u32[]{:S(2)}) collective-permute-start(bf16[160,512]{1,0:T(8,128)(2,1)S(1)} %get-tuple-element.128), channel_id=1, source_target_pairs={{0,1},{1,0},{2,3},{3,2},{4,5},{5,4},{6,7},{7,6},{8,9},{9,8},{10,11... | collective-permute-start | bytes 491528 | tf_op jit(solution)/shard_map/ppermute | solution.py:418
  76.6 9.9 %collective-permute-start.29 = (bf16[160,512]{1,0:T(8,128)(2,1)S(1)}, bf16[160,512]{1,0:T(8,128)(2,1)S(1)}, u32[]{:S(2)}, u32[]{:S(2)}) collective-permute-start(bf16[160,512]{1,0:T(8,128)(2,1)S(1)} %get-tuple-element.126), channel_id=1, source_target_pairs={{0,1},{1,0},{2,3},{3,2},{4,5},{5,4},{6,7},{7,6},{8,9},{9,8},{10,11... | collective-permute-start | bytes 491528 | tf_op jit(solution)/shard_map/ppermute | solution.py:418
  77.0 3.6 %collective-permute-start.16 = (bf16[160,512]{1,0:T(8,128)(2,1)S(1)}, bf16[160,512]{1,0:T(8,128)(2,1)S(1)}, u32[]{:S(2)}, u32[]{:S(2)}) collective-permute-start(bf16[160,512]{1,0:T(8,128)(2,1)S(1)} %get-tuple-element.105), channel_id=1, source_target_pairs={{0,1},{1,0},{2,3},{3,2},{4,5},{5,4},{6,7},{7,6},{8,9},{9,8},{10,11... | collective-permute-start | bytes 491528 | tf_op jit(solution)/shard_map/ppermute | solution.py:418
  77.7 31.9 %copy-start.15 = (f32[512]{0:T(512)S(1)}, f32[512]{0:T(512)}, u32[]{:S(2)}) copy-start(f32[512]{0:T(512)} %param.41) | copy-start | bytes 6148
  78.4 7.1 %collective-permute-start.18 = (bf16[160,512]{1,0:T(8,128)(2,1)S(1)}, bf16[160,512]{1,0:T(8,128)(2,1)S(1)}, u32[]{:S(2)}, u32[]{:S(2)}) collective-permute-start(bf16[160,512]{1,0:T(8,128)(2,1)S(1)} %add_convert_fusion.3), channel_id=1, source_target_pairs={{0,2},{1,3},{2,0},{3,1},{4,6},{5,7},{6,4},{7,5},{8,10},{9,11},{10,... | collective-permute-start | bytes 491528 | tf_op jit(solution)/shard_map/ppermute | solution.py:418
  80.0 8.5 %collective-permute-start.31 = (bf16[160,512]{1,0:T(8,128)(2,1)S(1)}, bf16[160,512]{1,0:T(8,128)(2,1)S(1)}, u32[]{:S(2)}, u32[]{:S(2)}) collective-permute-start(bf16[160,512]{1,0:T(8,128)(2,1)S(1)} %add_convert_fusion.1), channel_id=1, source_target_pairs={{0,2},{1,3},{2,0},{3,1},{4,6},{5,7},{6,4},{7,5},{8,10},{9,11},{10,... | collective-permute-start | bytes 491528 | tf_op jit(solution)/shard_map/ppermute | solution.py:418
  85.6 8.9 %collective-permute-start.19 = (bf16[40,512]{1,0:T(8,128)(2,1)S(1)}, bf16[40,512]{1,0:T(8,128)(2,1)S(1)}, u32[]{:S(2)}, u32[]{:S(2)}) collective-permute-start(bf16[40,512]{1,0:T(8,128)(2,1)S(1)} %get-tuple-element.137), channel_id=1, source_target_pairs={{0,4},{4,0},{8,12},{12,8},{16,20},{20,16},{24,28},{28,24},{1,5},{5... | collective-permute-start | bytes 122888 | tf_op jit(solution)/shard_map/ppermute | solution.py:418
  88.6 10.0 %collective-permute-start.32 = (bf16[40,512]{1,0:T(8,128)(2,1)S(1)}, bf16[40,512]{1,0:T(8,128)(2,1)S(1)}, u32[]{:S(2)}, u32[]{:S(2)}) collective-permute-start(bf16[40,512]{1,0:T(8,128)(2,1)S(1)} %get-tuple-element.134), channel_id=1, source_target_pairs={{0,16},{4,20},{8,24},{12,28},{16,0},{20,4},{24,8},{28,12},{1,17},{... | collective-permute-start | bytes 122888 | tf_op jit(solution)/shard_map/ppermute | solution.py:418
  90.1 7.6 %collective-permute-start.20 = (bf16[40,512]{1,0:T(8,128)(2,1)S(1)}, bf16[40,512]{1,0:T(8,128)(2,1)S(1)}, u32[]{:S(2)}, u32[]{:S(2)}) collective-permute-start(bf16[40,512]{1,0:T(8,128)(2,1)S(1)} %get-tuple-element.136), channel_id=1, source_target_pairs={{0,8},{4,12},{8,0},{12,4},{16,24},{20,28},{24,16},{28,20},{1,9},{5... | collective-permute-start | bytes 122888 | tf_op jit(solution)/shard_map/ppermute | solution.py:418
  92.4 6.2 %collective-permute-start.21 = (bf16[40,512]{1,0:T(8,128)(2,1)S(1)}, bf16[40,512]{1,0:T(8,128)(2,1)S(1)}, u32[]{:S(2)}, u32[]{:S(2)}) collective-permute-start(bf16[40,512]{1,0:T(8,128)(2,1)S(1)} %get-tuple-element.135), channel_id=1, source_target_pairs={{0,12},{4,8},{8,4},{12,0},{16,28},{20,24},{24,20},{28,16},{1,13},{... | collective-permute-start | bytes 122888 | tf_op jit(solution)/shard_map/ppermute | solution.py:418
  93.0 6.2 %collective-permute-start.33 = (bf16[40,512]{1,0:T(8,128)(2,1)S(1)}, bf16[40,512]{1,0:T(8,128)(2,1)S(1)}, u32[]{:S(2)}, u32[]{:S(2)}) collective-permute-start(bf16[40,512]{1,0:T(8,128)(2,1)S(1)} %get-tuple-element.133), channel_id=1, source_target_pairs={{0,20},{4,16},{8,28},{12,24},{16,4},{20,0},{24,12},{28,8},{1,21},{... | collective-permute-start | bytes 122888 | tf_op jit(solution)/shard_map/ppermute | solution.py:418
  94.5 5.8 %collective-permute-start.34 = (bf16[40,512]{1,0:T(8,128)(2,1)S(1)}, bf16[40,512]{1,0:T(8,128)(2,1)S(1)}, u32[]{:S(2)}, u32[]{:S(2)}) collective-permute-start(bf16[40,512]{1,0:T(8,128)(2,1)S(1)} %get-tuple-element.132), channel_id=1, source_target_pairs={{0,24},{4,28},{8,16},{12,20},{16,8},{20,12},{24,0},{28,4},{1,25},{... | collective-permute-start | bytes 122888 | tf_op jit(solution)/shard_map/ppermute | solution.py:418
  97.7 6.7 %collective-permute-start.35 = (bf16[40,512]{1,0:T(8,128)(2,1)S(1)}, bf16[40,512]{1,0:T(8,128)(2,1)S(1)}, u32[]{:S(2)}, u32[]{:S(2)}) collective-permute-start(bf16[40,512]{1,0:T(8,128)(2,1)S(1)} %get-tuple-element.131), channel_id=1, source_target_pairs={{0,28},{4,24},{8,20},{12,16},{16,12},{20,8},{24,4},{28,0},{1,29},{... | collective-permute-start | bytes 122888 | tf_op jit(solution)/shard_map/ppermute | solution.py:418
  104.7 1.2 %collective-permute-start.36 = (f32[2,128]{1,0:T(2,128)S(1)}, f32[2,128]{1,0:T(2,128)S(1)}, u32[]{:S(2)}, u32[]{:S(2)}) collective-permute-start(f32[2,128]{1,0:T(2,128)S(1)} %pad_maximum_fusion), channel_id=1, source_target_pairs={{0,1},{1,0},{2,3},{3,2},{4,5},{5,4},{6,7},{7,6},{8,9},{9,8},{10,11... | collective-permute-start | bytes 3080 | tf_op jit(solution)/shard_map/ppermute | solution.py:418
  106.0 3.6 %collective-permute-start.37 = (f32[2,128]{1,0:T(2,128)S(1)}, f32[2,128]{1,0:T(2,128)S(1)}, u32[]{:S(2)}, u32[]{:S(2)}) collective-permute-start(f32[2,128]{1,0:T(2,128)S(1)} %fusion.2), channel_id=1, source_target_pairs={{0,2},{1,3},{2,0},{3,1},{4,6},{5,7},{6,4},{7,5},{8,10},{9,11},{10,... | collective-permute-start | bytes 3080 | tf_op jit(solution)/shard_map/ppermute | solution.py:418

commit v4 on v3

--- a/solution.py
+++ b/solution.py
@@ -221,16 +221,20 @@
 
 def project_kernel(place_ref, group_ref, local_ref, query_ref, valve_ref, weight_ref, *refs):
     heads = local_ref.shape[1] // DV
-    state_refs, out_refs, heads_ref = refs[:heads], refs[heads:-1], refs[-1]
+    state_refs, heads_ref, out_refs = refs[:heads], refs[heads], refs[heads + 1 :]
     for k in range(heads):
         at = pl.ds(pl.multiple_of((group_ref[0] ^ k) * DV, DV), DV)
         mixed = local_ref[:, at] + dot_left(query_ref[:, at], state_refs[k][...])
         scaled = mixed * lax.rsqrt(jnp.mean(mixed * mixed, 1, keepdims=True) + 1e-06)
         heads_ref[:, at] = (scaled * silu(valve_ref[:, at].astype(F32))).astype(BF16)
+    project_blocks(1, place_ref, heads_ref, weight_ref, *out_refs)
+
+
+def project_blocks(odd, place_ref, heads_ref, weight_ref, *out_refs):
     width = out_refs[0].shape[1]
-    for offset in range(len(out_refs) - 1, -1, -1):
-        start = pl.multiple_of((place_ref[0] ^ offset) * width, width)
-        out_refs[offset][...] = dot(heads_ref[...], weight_ref[:, pl.ds(start, width)]).astype(BF16)
+    for i in range(len(out_refs) - 1, -1, -1):
+        start = pl.multiple_of((place_ref[0] ^ (2 * i + odd)) * width, width)
+        out_refs[i][...] = dot(heads_ref[...], weight_ref[:, pl.ds(start, width)]).astype(out_refs[i].dtype)
 
 
 def spread(fields, width):
@@ -433,6 +437,9 @@
 
 
 def sum_all(array, axis):
+    size = lax.axis_size(axis)
+    if size <= 4:
+        return array + sum(swap(array, axis, k) for k in range(size - 1, 0, -1))
     bit = 1
     while bit < lax.axis_size(axis):
         array = array + swap(array, axis, bit)
@@ -596,9 +603,9 @@
         ),
     )
 
-    partial = call(
+    heads_out, *sends = call(
         project_kernel,
-        [((tokens, width), BF16)] * n_tp,
+        [((tokens, heads * DV), BF16)] + [((tokens, width), BF16)] * (n_tp // 2),
         place,
         group,
         local,
@@ -607,8 +614,16 @@
         final_projection_matrix,
         *entering,
         in_specs=[smem()] * 2 + [vmem()] * (4 + heads),
-        scratch_shapes=[pltpu.VMEM((tokens, heads * DV), BF16)],
-    )
+    )
+    keeps = call(
+        functools.partial(project_blocks, 0),
+        [((tokens, width), F32)] * (n_tp // 2),
+        place,
+        heads_out,
+        final_projection_matrix,
+        in_specs=[smem()] + [vmem()] * 2,
+    )
+    partial = [(sends if k % 2 else keeps)[k // 2] for k in range(n_tp)]
     keep, got = scatter_sum(partial, "tp")
 
     top = specialist_picks.shape[1]

time: 111 us -> 109 us (0.982)
  waiting for transfers between devices: 46 us -> 44.2 us
    ppermute x37 -> x38, waiting for transfers between devices: 44.5 us -> 42.8 us  [swap(): return lax.ppermute(array, axis, [(i, i ^ bit) for i in range(size)])]
    ppermute x37 -> x38, starting transfers between devices: 38 us -> 38.2 us  [swap(): return lax.ppermute(array, axis, [(i, i ^ bit) for i in range(size)])]
    pallas_call x13 -> x14, Pallas kernels: 18.6 us -> 18.8 us  [call(): pl.pallas_call(kernel, out_shape=shapes, in_specs=in_specs or [vmem()] *...]
  transfers between devices with their start and end apart: 38 -> 39, of which waited for: 20 -> 20; matrix products, arithmetic and copies ran while one was open for 0% -> 0% of each run, Pallas kernels for 10% -> 11%
where the time goes in v4:
time: 109 us
  waiting for transfers between devices  44.2 us (41%)
  starting transfers between devices  42.9 us (39%)
  Pallas kernels  18.8 us (17%)
  local copies, waits for them, and re-layouts  1.3 us (1%)
  other arithmetic  1.09 us (1%)
    ppermute x38, waiting for transfers between devices, swap(): return lax.ppermute(array, axis, [(i, i ^ bit) for i in range(size)])  42.8 us
    ppermute x38, starting transfers between devices, swap(): return lax.ppermute(array, axis, [(i, i ^ bit) for i in range(size)])  38.2 us
    pallas_call x14, Pallas kernels, call(): pl.pallas_call(kernel, out_shape=shapes, in_specs=in_specs or [vmem()] *...  18.8 us
    ppermute x1, starting transfers between devices, shards(): got = lax.ppermute(leaving, 'sp', onward)  4.66 us
  transfers between devices with their start and end apart: 39, of which 20 were waited for; matrix products, arithmetic and copies ran while one was open for 0% of the time, Pallas kernels for 11%

profile of v4, /device:TPU:0, one launch (start us, length us, event | category | flops | bytes accessed | tf_op | source)
XLA Modules:
  0.0 109.1 jit_solution(4486217468120111116)
XLA Ops:
  0.0 4.6 %shard_map.200 = (bf16[272,128]{1,0:T(8,128)(2,1)}, bf16[272,128]{1,0:T(8,128)(2,1)}, bf16[272,128]{1,0:T(8,128)(2,1)}, bf16[272,128]{1,0:T(8,128)(2,1)}, f32[128,512]{1,0:T(8,128)}, /*index=5*/f32[128,512]{1,0:T(8,128)}) custom-call(s32[1]{0:T(128)} %bitcast.4.refs_0_.place_ref.group_ref, bf16[128,512]{1,0:T(8,128)(2,1)} %refs_1_.1, ...), custom_call_target="tpu_custom_call" | custom-call | flops 2000000000 | bytes 399892 | tf_op jit(solution)/shard_map/pallas_call | solution.py:477
  4.6 3.0 %collective-permute-start = (bf16[272,128]{1,0:T(8,128)(2,1)}, bf16[272,128]{1,0:T(8,128)(2,1)S(1)}, u32[]{:S(2)}, u32[]{:S(2)}) collective-permute-start(bf16[272,128]{1,0:T(8,128)(2,1)} %get-tuple-element.72), channel_id=1, source_target_pairs={{0,4},{4,0},{8,12},{12,8},{16,20},{20,16},{24,28},{28,24},{1,5},{5... | collective-permute-start | bytes 208904 | tf_op jit(solution)/shard_map/ppermute | solution.py:422
  7.6 1.6 %collective-permute-start.1 = (bf16[272,128]{1,0:T(8,128)(2,1)}, bf16[272,128]{1,0:T(8,128)(2,1)S(1)}, u32[]{:S(2)}, u32[]{:S(2)}) collective-permute-start(bf16[272,128]{1,0:T(8,128)(2,1)} %get-tuple-element.73), channel_id=1, source_target_pairs={{0,8},{4,12},{8,0},{12,4},{16,24},{20,28},{24,16},{28,20},{1,9},{5... | collective-permute-start | bytes 208904 | tf_op jit(solution)/shard_map/ppermute | solution.py:422
  9.1 0.9 copy-done.14
  10.1 2.6 %collective-permute-done.1.refs_2_ = bf16[272,128]{1,0:T(8,128)(2,1)S(1)} collective-permute-done((bf16[272,128]{1,0:T(8,128)(2,1)}, bf16[272,128]{1,0:T(8,128)(2,1)S(1)}, u32[]{:S(2)}, u32[]{:S(2)}) %collective-permute-start.1) | collective-permute-done | bytes 69664 | tf_op jit(solution)/shard_map/ppermute | solution.py:422
  12.7 1.9 %collective-permute-done.2.refs_3_ = bf16[272,128]{1,0:T(8,128)(2,1)S(1)} collective-permute-done((bf16[272,128]{1,0:T(8,128)(2,1)}, bf16[272,128]{1,0:T(8,128)(2,1)S(1)}, u32[]{:S(2)}, u32[]{:S(2)}) %collective-permute-start.2) | collective-permute-done | bytes 69664 | tf_op jit(solution)/shard_map/ppermute | solution.py:422
  14.5 1.2 %shard_map.202 = (f32[4,128,128]{2,1,0:T(8,128)S(1)}, bf16[4,128,128]{2,1,0:T(8,128)(2,1)S(1)}, bf16[16,128]{1,0:T(8,128)(2,1)S(1)}, bf16[144,128]{1,0:T(8,128)(2,1)S(1)}, f32[256,128]{1,0:T(8,128)}) custom-call(s32[1]{0:T(128)} %bitcast.4.refs_0_.place_ref.group_ref, bf16[272,128]{1,0:T(8,128)(2,1)S(1)} %shard_map.201.refs_0_, ...), custom_call_target="tpu_custom_call" | custom-call | flops 4000000000 | bytes 278532 | tf_op jit(solution)/shard_map/pallas_call | solution.py:477
  15.7 4.7 %collective-permute-start.3 = (bf16[144,128]{1,0:T(8,128)(2,1)S(1)}, bf16[144,128]{1,0:T(8,128)(2,1)S(1)}, u32[]{:S(2)}, u32[]{:S(2)}) collective-permute-start(bf16[144,128]{1,0:T(8,128)(2,1)S(1)} %get-tuple-element.75), channel_id=1, source_target_pairs={{0,16},{4,20},{8,24},{12,28},{1,17},{5,21},{9,25},{13,29},{2,18},{... | collective-permute-start | bytes 110600 | tf_op jit(solution)/shard_map/ppermute | solution.py:592
  20.4 1.4 %collective-permute-done.3.got_ref = bf16[144,128]{1,0:T(8,128)(2,1)S(1)} collective-permute-done((bf16[144,128]{1,0:T(8,128)(2,1)S(1)}, bf16[144,128]{1,0:T(8,128)(2,1)S(1)}, u32[]{:S(2)}, u32[]{:S(2)}) %collective-permute-start.3) | collective-permute-done | bytes 36896 | tf_op jit(solution)/shard_map/ppermute | solution.py:592
  21.8 0.2 shard_map.203
  22.0 0.6 collective-permute-start.4
  22.6 0.9 collective-permute-start.5
  23.5 2.1 %collective-permute-start.6 = (bf16[128,128]{1,0:T(8,128)(2,1)S(1)}, bf16[128,128]{1,0:T(8,128)(2,1)S(1)}, u32[]{:S(2)}, u32[]{:S(2)}) collective-permute-start(bf16[128,128]{1,0:T(8,128)(2,1)S(1)} %get-tuple-element.82), channel_id=1, source_target_pairs={{0,12},{4,8},{8,4},{12,0},{16,28},{20,24},{24,20},{28,16},{1,13},{... | collective-permute-start | bytes 98312 | tf_op jit(solution)/shard_map/ppermute | solution.py:422
  25.6 0.2 shard_map.199
  26.0 0.5 collective-permute-done.5.refs_2_
  26.5 1.8 %collective-permute-done.6.refs_3_ = bf16[128,128]{1,0:T(8,128)(2,1)S(1)} collective-permute-done((bf16[128,128]{1,0:T(8,128)(2,1)S(1)}, bf16[128,128]{1,0:T(8,128)(2,1)S(1)}, u32[]{:S(2)}, u32[]{:S(2)}) %collective-permute-start.6) | collective-permute-done | bytes 32800 | tf_op jit(solution)/shard_map/ppermute | solution.py:422
  28.3 0.6 shard_map.204
  29.1 0.3 shard_map.205
  29.4 0.5 collective-permute-start.7
  29.9 0.4 collective-permute-done.8
  30.4 1.6 %collective-permute-start.9 = (bf16[128,512]{1,0:T(8,128)(2,1)S(1)}, bf16[128,512]{1,0:T(8,128)(2,1)S(1)}, u32[]{:S(2)}, u32[]{:S(2)}) collective-permute-start(bf16[128,512]{1,0:T(8,128)(2,1)S(1)} %add_convert_fusion.4), channel_id=1, source_target_pairs={{0,2},{1,3},{2,0},{3,1},{4,6},{5,7},{6,4},{7,5},{8,10},{9,11},{10,... | collective-permute-start | bytes 393224 | tf_op jit(solution)/shard_map/ppermute | solution.py:422
  32.0 4.0 %collective-permute-done.9.got_ref = bf16[128,512]{1,0:T(8,128)(2,1)S(1)} collective-permute-done((bf16[128,512]{1,0:T(8,128)(2,1)S(1)}, bf16[128,512]{1,0:T(8,128)(2,1)S(1)}, u32[]{:S(2)}, u32[]{:S(2)}) %collective-permute-start.9) | collective-permute-done | bytes 131104 | tf_op jit(solution)/shard_map/ppermute | solution.py:422
  36.1 0.6 shard_map.206
  36.7 3.3 %collective-permute-start.22 = (bf16[40,512]{1,0:T(8,128)(2,1)S(1)}, bf16[40,512]{1,0:T(8,128)(2,1)S(1)}, u32[]{:S(2)}, u32[]{:S(2)}) collective-permute-start(bf16[40,512]{1,0:T(8,128)(2,1)S(1)} %get-tuple-element.110), channel_id=1, source_target_pairs={{0,16},{4,20},{8,24},{12,28},{16,0},{20,4},{24,8},{28,12},{1,17},{... | collective-permute-start | bytes 122888 | tf_op jit(solution)/shard_map/ppermute | solution.py:422
  40.0 0.6 collective-permute-start.23
  40.6 3.9 %collective-permute-start.24 = (bf16[40,512]{1,0:T(8,128)(2,1)S(1)}, bf16[40,512]{1,0:T(8,128)(2,1)S(1)}, u32[]{:S(2)}, u32[]{:S(2)}) collective-permute-start(bf16[40,512]{1,0:T(8,128)(2,1)S(1)} %get-tuple-element.112), channel_id=1, source_target_pairs={{0,24},{4,28},{8,16},{12,20},{16,8},{20,12},{24,0},{28,4},{1,25},{... | collective-permute-start | bytes 122888 | tf_op jit(solution)/shard_map/ppermute | solution.py:422
  44.4 0.3 collective-permute-start.25
  44.8 1.1 %collective-permute-start.10 = (bf16[40,512]{1,0:T(8,128)(2,1)S(1)}, bf16[40,512]{1,0:T(8,128)(2,1)S(1)}, u32[]{:S(2)}, u32[]{:S(2)}) collective-permute-start(bf16[40,512]{1,0:T(8,128)(2,1)S(1)} %get-tuple-element.90), channel_id=1, source_target_pairs={{0,4},{4,0},{8,12},{12,8},{16,20},{20,16},{24,28},{28,24},{1,5},{5... | collective-permute-start | bytes 122888 | tf_op jit(solution)/shard_map/ppermute | solution.py:422
  45.9 3.2 %collective-permute-done.10 = bf16[40,512]{1,0:T(8,128)(2,1)S(1)} collective-permute-done((bf16[40,512]{1,0:T(8,128)(2,1)S(1)}, bf16[40,512]{1,0:T(8,128)(2,1)S(1)}, u32[]{:S(2)}, u32[]{:S(2)}) %collective-permute-start.10) | collective-permute-done | bytes 40992 | tf_op jit(solution)/shard_map/ppermute | solution.py:422
  49.1 4.4 %collective-permute-done.11 = bf16[40,512]{1,0:T(8,128)(2,1)S(1)} collective-permute-done((bf16[40,512]{1,0:T(8,128)(2,1)S(1)}, bf16[40,512]{1,0:T(8,128)(2,1)S(1)}, u32[]{:S(2)}, u32[]{:S(2)}) %collective-permute-start.11) | collective-permute-done | bytes 40992 | tf_op jit(solution)/shard_map/ppermute | solution.py:422
  53.5 4.9 %collective-permute-done.12 = bf16[40,512]{1,0:T(8,128)(2,1)S(1)} collective-permute-done((bf16[40,512]{1,0:T(8,128)(2,1)S(1)}, bf16[40,512]{1,0:T(8,128)(2,1)S(1)}, u32[]{:S(2)}, u32[]{:S(2)}) %collective-permute-start.12) | collective-permute-done | bytes 40992 | tf_op jit(solution)/shard_map/ppermute | solution.py:422
  58.4 1.5 %collective-permute-start.13 = (bf16[160,512]{1,0:T(8,128)(2,1)S(1)}, bf16[160,512]{1,0:T(8,128)(2,1)S(1)}, u32[]{:S(2)}, u32[]{:S(2)}) collective-permute-start(bf16[160,512]{1,0:T(8,128)(2,1)S(1)} %constant_dynamic-update-slice_fusion.refs_1_.own_ref), channel_id=1, source_target_pairs={{0,2},{1,3},{2,0},{3,1},{4,6},{5,7},{6,4},{7,5},{8,10},{9,11},{10,... | collective-permute-start | bytes 491528 | tf_op jit(solution)/shard_map/ppermute | solution.py:422
  60.0 0.6 collective-permute-start.26
  60.6 0.5 collective-permute-start.15
  61.1 2.6 %collective-permute-done.13.refs_1_ = bf16[160,512]{1,0:T(8,128)(2,1)S(1)} collective-permute-done((bf16[160,512]{1,0:T(8,128)(2,1)S(1)}, bf16[160,512]{1,0:T(8,128)(2,1)S(1)}, u32[]{:S(2)}, u32[]{:S(2)}) %collective-permute-start.13) | collective-permute-done | bytes 163872 | tf_op jit(solution)/shard_map/ppermute | solution.py:422
  63.8 1.8 %collective-permute-done.26.refs_1_ = bf16[160,512]{1,0:T(8,128)(2,1)S(1)} collective-permute-done((bf16[160,512]{1,0:T(8,128)(2,1)S(1)}, bf16[160,512]{1,0:T(8,128)(2,1)S(1)}, u32[]{:S(2)}, u32[]{:S(2)}) %collective-permute-start.26) | collective-permute-done | bytes 163872 | tf_op jit(solution)/shard_map/ppermute | solution.py:422
  65.5 2.0 %shard_map.210 = (f32[160,1024]{1,0:T(8,128)S(1)}, f32[160,1024]{1,0:T(8,128)S(1)}, f32[160,128]{1,0:T(8,128)S(1)}, f32[160,128]{1,0:T(8,128)S(1)}, f32[8,1024]{...) custom-call(s32[1]{0:T(128)} %bitcast.3.place_ref.refs_0_, ...), custom_call_target="tpu_custom_call" | custom-call | flops 754974720 | bytes 9764868 | tf_op jit(solution)/shard_map/pallas_call | solution.py:477
  67.6 2.0 %shard_map.207 = (f32[160,1024]{1,0:T(8,128)S(1)}, f32[160,1024]{1,0:T(8,128)S(1)}, f32[160,128]{1,0:T(8,128)S(1)}, f32[160,128]{1,0:T(8,128)S(1)}, f32[8,1024]{...) custom-call(s32[1]{0:T(128)} %bitcast.3.place_ref.refs_0_, ...), custom_call_target="tpu_custom_call" | custom-call | flops 754974720 | bytes 9764868 | tf_op jit(solution)/shard_map/pallas_call | solution.py:477
  69.8 2.9 %shard_map.208 = (bf16[160,512]{1,0:T(8,128)(2,1)S(1)}, bf16[160,512]{1,0:T(8,128)(2,1)S(1)}, bf16[160,1024]{1,0:T(8,128)(2,1)S(1)}, bf16[160,128]{1,0:T(8,128)(2,1)S(1)}, f32[160,128]{1,0:T(8,128)S(1)}) custom-call(s32[1]{0:T(128)} %bitcast.3.place_ref.refs_0_, bf16[160,512]{1,0:T(8,128)(2,1)S(1)} %collective-permute-done.13.refs_1_, ...), custom_call_target="tpu_custom_call" | custom-call | flops 1509949440 | bytes 16195588 | tf_op jit(solution)/shard_map/pallas_call | solution.py:477
  72.8 0.6 collective-permute-start.17
  73.3 2.9 %shard_map.211 = (bf16[160,512]{1,0:T(8,128)(2,1)S(1)}, bf16[160,512]{1,0:T(8,128)(2,1)S(1)}, bf16[160,1024]{1,0:T(8,128)(2,1)S(1)}, bf16[160,128]{1,0:T(8,128)(2,1)S(1)}, f32[160,128]{1,0:T(8,128)S(1)}) custom-call(s32[1]{0:T(128)} %bitcast.3.place_ref.refs_0_, bf16[160,512]{1,0:T(8,128)(2,1)S(1)} %collective-permute-done.26.refs_1_, ...), custom_call_target="tpu_custom_call" | custom-call | flops 1509949440 | bytes 16195588 | tf_op jit(solution)/shard_map/pallas_call | solution.py:477
  76.4 0.5 collective-permute-start.29
  76.9 0.6 shard_map.212
  77.5 0.6 shard_map.209
  78.2 1.6 %collective-permute-start.18 = (bf16[160,512]{1,0:T(8,128)(2,1)S(1)}, bf16[160,512]{1,0:T(8,128)(2,1)S(1)}, u32[]{:S(2)}, u32[]{:S(2)}) collective-permute-start(bf16[160,512]{1,0:T(8,128)(2,1)S(1)} %add_convert_fusion.3), channel_id=1, source_target_pairs={{0,2},{1,3},{2,0},{3,1},{4,6},{5,7},{6,4},{7,5},{8,10},{9,11},{10,... | collective-permute-start | bytes 491528 | tf_op jit(solution)/shard_map/ppermute | solution.py:422
  79.8 0.6 collective-permute-start.31
  80.4 4.9 %collective-permute-done.18 = bf16[160,512]{1,0:T(8,128)(2,1)S(1)} collective-permute-done((bf16[160,512]{1,0:T(8,128)(2,1)S(1)}, bf16[160,512]{1,0:T(8,128)(2,1)S(1)}, u32[]{:S(2)}, u32[]{:S(2)}) %collective-permute-start.18) | collective-permute-done | bytes 163872 | tf_op jit(solution)/shard_map/ppermute | solution.py:422
  85.4 0.8 collective-permute-start.19
  86.3 2.0 %collective-permute-done.31 = bf16[160,512]{1,0:T(8,128)(2,1)S(1)} collective-permute-done((bf16[160,512]{1,0:T(8,128)(2,1)S(1)}, bf16[160,512]{1,0:T(8,128)(2,1)S(1)}, u32[]{:S(2)}, u32[]{:S(2)}) %collective-permute-start.31) | collective-permute-done | bytes 163872 | tf_op jit(solution)/shard_map/ppermute | solution.py:422
  88.4 1.5 %collective-permute-start.32 = (bf16[40,512]{1,0:T(8,128)(2,1)S(1)}, bf16[40,512]{1,0:T(8,128)(2,1)S(1)}, u32[]{:S(2)}, u32[]{:S(2)}) collective-permute-start(bf16[40,512]{1,0:T(8,128)(2,1)S(1)} %get-tuple-element.136), channel_id=1, source_target_pairs={{0,16},{4,20},{8,24},{12,28},{16,0},{20,4},{24,8},{28,12},{1,17},{... | collective-permute-start | bytes 122888 | tf_op jit(solution)/shard_map/ppermute | solution.py:422
  89.9 2.3 %collective-permute-start.20 = (bf16[40,512]{1,0:T(8,128)(2,1)S(1)}, bf16[40,512]{1,0:T(8,128)(2,1)S(1)}, u32[]{:S(2)}, u32[]{:S(2)}) collective-permute-start(bf16[40,512]{1,0:T(8,128)(2,1)S(1)} %get-tuple-element.138), channel_id=1, source_target_pairs={{0,8},{4,12},{8,0},{12,4},{16,24},{20,28},{24,16},{28,20},{1,9},{5... | collective-permute-start | bytes 122888 | tf_op jit(solution)/shard_map/ppermute | solution.py:422
  92.2 0.6 collective-permute-start.21
  92.8 1.5 %collective-permute-start.33 = (bf16[40,512]{1,0:T(8,128)(2,1)S(1)}, bf16[40,512]{1,0:T(8,128)(2,1)S(1)}, u32[]{:S(2)}, u32[]{:S(2)}) collective-permute-start(bf16[40,512]{1,0:T(8,128)(2,1)S(1)} %get-tuple-element.135), channel_id=1, source_target_pairs={{0,20},{4,16},{8,28},{12,24},{16,4},{20,0},{24,12},{28,8},{1,21},{... | collective-permute-start | bytes 122888 | tf_op jit(solution)/shard_map/ppermute | solution.py:422
  94.3 3.2 %collective-permute-start.34 = (bf16[40,512]{1,0:T(8,128)(2,1)S(1)}, bf16[40,512]{1,0:T(8,128)(2,1)S(1)}, u32[]{:S(2)}, u32[]{:S(2)}) collective-permute-start(bf16[40,512]{1,0:T(8,128)(2,1)S(1)} %get-tuple-element.134), channel_id=1, source_target_pairs={{0,24},{4,28},{8,16},{12,20},{16,8},{20,12},{24,0},{28,4},{1,25},{... | collective-permute-start | bytes 122888 | tf_op jit(solution)/shard_map/ppermute | solution.py:422
  97.5 0.9 collective-permute-start.35
  98.4 0.6 collective-permute-done.33
  99.0 1.1 %collective-permute-done.34 = bf16[40,512]{1,0:T(8,128)(2,1)S(1)} collective-permute-done((bf16[40,512]{1,0:T(8,128)(2,1)S(1)}, bf16[40,512]{1,0:T(8,128)(2,1)S(1)}, u32[]{:S(2)}, u32[]{:S(2)}) %collective-permute-start.34) | collective-permute-done | bytes 40992 | tf_op jit(solution)/shard_map/ppermute | solution.py:422
  100.1 4.1 %collective-permute-done.35 = bf16[40,512]{1,0:T(8,128)(2,1)S(1)} collective-permute-done((bf16[40,512]{1,0:T(8,128)(2,1)S(1)}, bf16[40,512]{1,0:T(8,128)(2,1)S(1)}, u32[]{:S(2)}, u32[]{:S(2)}) %collective-permute-start.35) | collective-permute-done | bytes 40992 | tf_op jit(solution)/shard_map/ppermute | solution.py:422
  104.2 0.3 fusion.2
  104.6 1.6 %collective-permute-start.37 = (f32[2,128]{1,0:T(2,128)S(1)}, f32[2,128]{1,0:T(2,128)S(1)}, u32[]{:S(2)}, u32[]{:S(2)}) collective-permute-start(f32[2,128]{1,0:T(2,128)S(1)} %pad_maximum_fusion), channel_id=1, source_target_pairs={{0,2},{1,3},{2,0},{3,1},{4,6},{5,7},{6,4},{7,5},{8,10},{9,11},{10,... | collective-permute-start | bytes 3080 | tf_op jit(solution)/shard_map/ppermute | solution.py:422
  106.3 0.2 collective-permute-start.38
  106.5 1.1 %collective-permute-done.36 = f32[2,128]{1,0:T(2,128)S(1)} collective-permute-done((f32[2,128]{1,0:T(2,128)S(1)}, f32[2,128]{1,0:T(2,128)S(1)}, u32[]{:S(2)}, u32[]{:S(2)}) %collective-permute-start.36) | collective-permute-done | bytes 1056 | tf_op jit(solution)/shard_map/ppermute | solution.py:422
  107.6 0.7 collective-permute-done.37
  108.3 0.8 multiply_convert_fusion
  (89 shorter events, 1.3 us)
Async XLA Ops:
  4.6 5.5 %collective-permute-start = (bf16[272,128]{1,0:T(8,128)(2,1)}, bf16[272,128]{1,0:T(8,128)(2,1)S(1)}, u32[]{:S(2)}, u32[]{:S(2)}) collective-permute-start(bf16[272,128]{1,0:T(8,128)(2,1)} %get-tuple-element.72), channel_id=1, source_target_pairs={{0,4},{4,0},{8,12},{12,8},{16,20},{20,16},{24,28},{28,24},{1,5},{5... | collective-permute-start | bytes 208904 | tf_op jit(solution)/shard_map/ppermute | solution.py:422
  7.6 5.1 %collective-permute-start.1 = (bf16[272,128]{1,0:T(8,128)(2,1)}, bf16[272,128]{1,0:T(8,128)(2,1)S(1)}, u32[]{:S(2)}, u32[]{:S(2)}) collective-permute-start(bf16[272,128]{1,0:T(8,128)(2,1)} %get-tuple-element.73), channel_id=1, source_target_pairs={{0,8},{4,12},{8,0},{12,4},{16,24},{20,28},{24,16},{28,20},{1,9},{5... | collective-permute-start | bytes 208904 | tf_op jit(solution)/shard_map/ppermute | solution.py:422
  9.1 5.4 %collective-permute-start.2 = (bf16[272,128]{1,0:T(8,128)(2,1)}, bf16[272,128]{1,0:T(8,128)(2,1)S(1)}, u32[]{:S(2)}, u32[]{:S(2)}) collective-permute-start(bf16[272,128]{1,0:T(8,128)(2,1)} %get-tuple-element.74), channel_id=1, source_target_pairs={{0,12},{4,8},{8,4},{12,0},{16,28},{20,24},{24,20},{28,16},{1,13},{... | collective-permute-start | bytes 208904 | tf_op jit(solution)/shard_map/ppermute | solution.py:422
  9.1 0.9 copy-start.14
  15.7 6.1 %collective-permute-start.3 = (bf16[144,128]{1,0:T(8,128)(2,1)S(1)}, bf16[144,128]{1,0:T(8,128)(2,1)S(1)}, u32[]{:S(2)}, u32[]{:S(2)}) collective-permute-start(bf16[144,128]{1,0:T(8,128)(2,1)S(1)} %get-tuple-element.75), channel_id=1, source_target_pairs={{0,16},{4,20},{8,24},{12,28},{1,17},{5,21},{9,25},{13,29},{2,18},{... | collective-permute-start | bytes 110600 | tf_op jit(solution)/shard_map/ppermute | solution.py:592
  21.8 3.7 %copy-start.10 = (s32[128,2]{0,1:T(2,128)S(1)}, s32[128,2]{0,1:T(2,128)}, u32[]{:S(2)}) copy-start(s32[128,2]{0,1:T(2,128)} %param.33) | copy-start | bytes 3076
  21.8 3.7 %copy-start.11 = (bf16[128,2]{0,1:T(2,128)(2,1)S(1)}, bf16[128,2]{0,1:T(2,128)(2,1)}, u32[]{:S(2)}) copy-start(bf16[128,2]{0,1:T(2,128)(2,1)} %param.34) | copy-start | bytes 1540
  22.0 4.0 %collective-permute-start.4 = (bf16[128,128]{1,0:T(8,128)(2,1)S(1)}, bf16[128,128]{1,0:T(8,128)(2,1)S(1)}, u32[]{:S(2)}, u32[]{:S(2)}) collective-permute-start(bf16[128,128]{1,0:T(8,128)(2,1)S(1)} %get-tuple-element.80), channel_id=1, source_target_pairs={{0,4},{4,0},{8,12},{12,8},{16,20},{20,16},{24,28},{28,24},{1,5},{5... | collective-permute-start | bytes 98312 | tf_op jit(solution)/shard_map/ppermute | solution.py:422
  22.6 3.9 %collective-permute-start.5 = (bf16[128,128]{1,0:T(8,128)(2,1)S(1)}, bf16[128,128]{1,0:T(8,128)(2,1)S(1)}, u32[]{:S(2)}, u32[]{:S(2)}) collective-permute-start(bf16[128,128]{1,0:T(8,128)(2,1)S(1)} %get-tuple-element.81), channel_id=1, source_target_pairs={{0,8},{4,12},{8,0},{12,4},{16,24},{20,28},{24,16},{28,20},{1,9},{5... | collective-permute-start | bytes 98312 | tf_op jit(solution)/shard_map/ppermute | solution.py:422
  23.5 4.8 %collective-permute-start.6 = (bf16[128,128]{1,0:T(8,128)(2,1)S(1)}, bf16[128,128]{1,0:T(8,128)(2,1)S(1)}, u32[]{:S(2)}, u32[]{:S(2)}) collective-permute-start(bf16[128,128]{1,0:T(8,128)(2,1)S(1)} %get-tuple-element.82), channel_id=1, source_target_pairs={{0,12},{4,8},{8,4},{12,0},{16,28},{20,24},{24,20},{28,16},{1,13},{... | collective-permute-start | bytes 98312 | tf_op jit(solution)/shard_map/ppermute | solution.py:422
  25.6 2.7 %copy-start.6 = (bf16[512,2048]{1,0:T(8,128)(2,1)S(1)}, bf16[512,2048]{1,0:T(8,128)(2,1)}, u32[]{:S(2)}) copy-start(bf16[512,2048]{1,0:T(8,128)(2,1)} %weight_ref.3) | copy-start | bytes 6291460
  25.6 2.7 %copy-start.7 = (bf16[128,512]{1,0:T(8,128)(2,1)S(1)}, bf16[128,512]{1,0:T(8,128)(2,1)}, u32[]{:S(2)}) copy-start(bf16[128,512]{1,0:T(8,128)(2,1)} %valve_ref.1) | copy-start | bytes 393220
  25.6 2.7 %copy-start.12 = (f32[128,512]{1,0:T(8,128)S(1)}, f32[128,512]{1,0:T(8,128)}, u32[]{:S(2)}) copy-start(f32[128,512]{1,0:T(8,128)} %get-tuple-element.69.local_ref) | copy-start | bytes 786436
  25.6 2.7 %copy-start.13 = (f32[128,512]{1,0:T(8,128)S(1)}, f32[128,512]{1,0:T(8,128)}, u32[]{:S(2)}) copy-start(f32[128,512]{1,0:T(8,128)} %get-tuple-element.70.query_ref) | copy-start | bytes 786436
  29.0 1.4 %collective-permute-start.8 = (bf16[128,512]{1,0:T(8,128)(2,1)S(1)}, bf16[128,512]{1,0:T(8,128)(2,1)S(1)}, u32[]{:S(2)}, u32[]{:S(2)}) collective-permute-start(bf16[128,512]{1,0:T(8,128)(2,1)S(1)} %get-tuple-element.87), channel_id=1, source_target_pairs={{0,1},{1,0},{2,3},{3,2},{4,5},{5,4},{6,7},{7,6},{8,9},{9,8},{10,11... | collective-permute-start | bytes 393224 | tf_op jit(solution)/shard_map/ppermute | solution.py:422
  29.0 7.0 %copy-start.8 = (bf16[128,512]{1,0:T(8,128)(2,1)S(1)}, bf16[128,512]{1,0:T(8,128)(2,1)}, u32[]{:S(2)}) copy-start(bf16[128,512]{1,0:T(8,128)(2,1)} %row_ref.1) | copy-start | bytes 393220
  29.0 7.0 %copy-start.9 = (f32[512]{0:T(512)S(1)}, f32[512]{0:T(512)}, u32[]{:S(2)}) copy-start(f32[512]{0:T(512)} %param.32) | copy-start | bytes 6148
  29.4 2.6 %collective-permute-start.7 = (bf16[128,512]{1,0:T(8,128)(2,1)S(1)}, bf16[128,512]{1,0:T(8,128)(2,1)S(1)}, u32[]{:S(2)}, u32[]{:S(2)}) collective-permute-start(bf16[128,512]{1,0:T(8,128)(2,1)S(1)} %get-tuple-element.85), channel_id=1, source_target_pairs={{0,1},{1,0},{2,3},{3,2},{4,5},{5,4},{6,7},{7,6},{8,9},{9,8},{10,11... | collective-permute-start | bytes 393224 | tf_op jit(solution)/shard_map/ppermute | solution.py:422
  30.4 5.6 %collective-permute-start.9 = (bf16[128,512]{1,0:T(8,128)(2,1)S(1)}, bf16[128,512]{1,0:T(8,128)(2,1)S(1)}, u32[]{:S(2)}, u32[]{:S(2)}) collective-permute-start(bf16[128,512]{1,0:T(8,128)(2,1)S(1)} %add_convert_fusion.4), channel_id=1, source_target_pairs={{0,2},{1,3},{2,0},{3,1},{4,6},{5,7},{6,4},{7,5},{8,10},{9,11},{10,... | collective-permute-start | bytes 393224 | tf_op jit(solution)/shard_map/ppermute | solution.py:422
  36.0 29.5 %copy-start = (bf16[1,2048,1024]{2,1,0:T(8,128)(2,1)S(1)}, bf16[1,2048,1024]{2,1,0:T(8,128)(2,1)}, u32[]{:S(2)}) copy-start(bf16[1,2048,1024]{2,1,0:T(8,128)(2,1)} %refs_3_.9) | copy-start | bytes 12582916
  36.0 29.5 %copy-start.1 = (bf16[1,2048,1024]{2,1,0:T(8,128)(2,1)S(1)}, bf16[1,2048,1024]{2,1,0:T(8,128)(2,1)}, u32[]{:S(2)}) copy-start(bf16[1,2048,1024]{2,1,0:T(8,128)(2,1)} %refs_4_.9) | copy-start | bytes 12582916
  36.0 29.5 %copy-start.3 = (bf16[2048,128]{1,0:T(8,128)(2,1)S(1)}, bf16[2048,128]{1,0:T(8,128)(2,1)}, u32[]{:S(2)}) copy-start(bf16[2048,128]{1,0:T(8,128)(2,1)} %refs_5_.9) | copy-start | bytes 1572868
  36.0 29.5 %copy-start.4 = (bf16[2048,128]{1,0:T(8,128)(2,1)S(1)}, bf16[2048,128]{1,0:T(8,128)(2,1)}, u32[]{:S(2)}) copy-start(bf16[2048,128]{1,0:T(8,128)(2,1)} %refs_6_.9) | copy-start | bytes 1572868
  36.7 23.2 %collective-permute-start.22 = (bf16[40,512]{1,0:T(8,128)(2,1)S(1)}, bf16[40,512]{1,0:T(8,128)(2,1)S(1)}, u32[]{:S(2)}, u32[]{:S(2)}) collective-permute-start(bf16[40,512]{1,0:T(8,128)(2,1)S(1)} %get-tuple-element.110), channel_id=1, source_target_pairs={{0,16},{4,20},{8,24},{12,28},{16,0},{20,4},{24,8},{28,12},{1,17},{... | collective-permute-start | bytes 122888 | tf_op jit(solution)/shard_map/ppermute | solution.py:422
  40.0 20.0 %collective-permute-start.23 = (bf16[40,512]{1,0:T(8,128)(2,1)S(1)}, bf16[40,512]{1,0:T(8,128)(2,1)S(1)}, u32[]{:S(2)}, u32[]{:S(2)}) collective-permute-start(bf16[40,512]{1,0:T(8,128)(2,1)S(1)} %get-tuple-element.111), channel_id=1, source_target_pairs={{0,20},{4,16},{8,28},{12,24},{16,4},{20,0},{24,12},{28,8},{1,21},{... | collective-permute-start | bytes 122888 | tf_op jit(solution)/shard_map/ppermute | solution.py:422
  40.6 19.4 %collective-permute-start.24 = (bf16[40,512]{1,0:T(8,128)(2,1)S(1)}, bf16[40,512]{1,0:T(8,128)(2,1)S(1)}, u32[]{:S(2)}, u32[]{:S(2)}) collective-permute-start(bf16[40,512]{1,0:T(8,128)(2,1)S(1)} %get-tuple-element.112), channel_id=1, source_target_pairs={{0,24},{4,28},{8,16},{12,20},{16,8},{20,12},{24,0},{28,4},{1,25},{... | collective-permute-start | bytes 122888 | tf_op jit(solution)/shard_map/ppermute | solution.py:422
  44.4 15.6 %collective-permute-start.25 = (bf16[40,512]{1,0:T(8,128)(2,1)S(1)}, bf16[40,512]{1,0:T(8,128)(2,1)S(1)}, u32[]{:S(2)}, u32[]{:S(2)}) collective-permute-start(bf16[40,512]{1,0:T(8,128)(2,1)S(1)} %get-tuple-element.113), channel_id=1, source_target_pairs={{0,28},{4,24},{8,20},{12,16},{16,12},{20,8},{24,4},{28,0},{1,29},{... | collective-permute-start | bytes 122888 | tf_op jit(solution)/shard_map/ppermute | solution.py:422
  44.8 4.4 %collective-permute-start.10 = (bf16[40,512]{1,0:T(8,128)(2,1)S(1)}, bf16[40,512]{1,0:T(8,128)(2,1)S(1)}, u32[]{:S(2)}, u32[]{:S(2)}) collective-permute-start(bf16[40,512]{1,0:T(8,128)(2,1)S(1)} %get-tuple-element.90), channel_id=1, source_target_pairs={{0,4},{4,0},{8,12},{12,8},{16,20},{20,16},{24,28},{28,24},{1,5},{5... | collective-permute-start | bytes 122888 | tf_op jit(solution)/shard_map/ppermute | solution.py:422
  49.1 4.4 %collective-permute-start.11 = (bf16[40,512]{1,0:T(8,128)(2,1)S(1)}, bf16[40,512]{1,0:T(8,128)(2,1)S(1)}, u32[]{:S(2)}, u32[]{:S(2)}) collective-permute-start(bf16[40,512]{1,0:T(8,128)(2,1)S(1)} %get-tuple-element.91), channel_id=1, source_target_pairs={{0,8},{4,12},{8,0},{12,4},{16,24},{20,28},{24,16},{28,20},{1,9},{5... | collective-permute-start | bytes 122888 | tf_op jit(solution)/shard_map/ppermute | solution.py:422
  53.5 4.9 %collective-permute-start.12 = (bf16[40,512]{1,0:T(8,128)(2,1)S(1)}, bf16[40,512]{1,0:T(8,128)(2,1)S(1)}, u32[]{:S(2)}, u32[]{:S(2)}) collective-permute-start(bf16[40,512]{1,0:T(8,128)(2,1)S(1)} %get-tuple-element.92), channel_id=1, source_target_pairs={{0,12},{4,8},{8,4},{12,0},{16,28},{20,24},{24,20},{28,16},{1,13},{... | collective-permute-start | bytes 122888 | tf_op jit(solution)/shard_map/ppermute | solution.py:422
  58.4 5.3 %collective-permute-start.13 = (bf16[160,512]{1,0:T(8,128)(2,1)S(1)}, bf16[160,512]{1,0:T(8,128)(2,1)S(1)}, u32[]{:S(2)}, u32[]{:S(2)}) collective-permute-start(bf16[160,512]{1,0:T(8,128)(2,1)S(1)} %constant_dynamic-update-slice_fusion.refs_1_.own_ref), channel_id=1, source_target_pairs={{0,2},{1,3},{2,0},{3,1},{4,6},{5,7},{6,4},{7,5},{8,10},{9,11},{10,... | collective-permute-start | bytes 491528 | tf_op jit(solution)/shard_map/ppermute | solution.py:422
  60.0 5.5 %collective-permute-start.26 = (bf16[160,512]{1,0:T(8,128)(2,1)S(1)}, bf16[160,512]{1,0:T(8,128)(2,1)S(1)}, u32[]{:S(2)}, u32[]{:S(2)}) collective-permute-start(bf16[160,512]{1,0:T(8,128)(2,1)S(1)} %constant_dynamic-update-slice_fusion.4.refs_1_.own_ref), channel_id=1, source_target_pairs={{0,2},{1,3},{2,0},{3,1},{4,6},{5,7},{6,4},{7,5},{8,10},{9,11},{10,... | collective-permute-start | bytes 491528 | tf_op jit(solution)/shard_map/ppermute | solution.py:422
  60.6 4.9 %collective-permute-start.28 = (bf16[160,512]{1,0:T(8,128)(2,1)S(1)}, bf16[160,512]{1,0:T(8,128)(2,1)S(1)}, u32[]{:S(2)}, u32[]{:S(2)}) collective-permute-start(bf16[160,512]{1,0:T(8,128)(2,1)S(1)} %constant_dynamic-update-slice_fusion.4.refs_1_.own_ref), channel_id=1, source_target_pairs={{0,1},{1,0},{2,3},{3,2},{4,5},{5,4},{6,7},{7,6},{8,9},{9,8},{10,11... | collective-permute-start | bytes 491528 | tf_op jit(solution)/shard_map/ppermute | solution.py:422
  60.6 7.0 %collective-permute-start.15 = (bf16[160,512]{1,0:T(8,128)(2,1)S(1)}, bf16[160,512]{1,0:T(8,128)(2,1)S(1)}, u32[]{:S(2)}, u32[]{:S(2)}) collective-permute-start(bf16[160,512]{1,0:T(8,128)(2,1)S(1)} %constant_dynamic-update-slice_fusion.refs_1_.own_ref), channel_id=1, source_target_pairs={{0,1},{1,0},{2,3},{3,2},{4,5},{5,4},{6,7},{7,6},{8,9},{9,8},{10,11... | collective-permute-start | bytes 491528 | tf_op jit(solution)/shard_map/ppermute | solution.py:422
  63.8 5.8 %collective-permute-start.14 = (bf16[160,512]{1,0:T(8,128)(2,1)S(1)}, bf16[160,512]{1,0:T(8,128)(2,1)S(1)}, u32[]{:S(2)}, u32[]{:S(2)}) collective-permute-start(bf16[160,512]{1,0:T(8,128)(2,1)S(1)} %collective-permute-done.13.refs_1_), channel_id=1, source_target_pairs={{0,1},{1,0},{2,3},{3,2},{4,5},{5,4},{6,7},{7,6},{8,9},{9,8},{10,11... | collective-permute-start | bytes 491528 | tf_op jit(solution)/shard_map/ppermute | solution.py:422
  65.5 7.8 %collective-permute-start.27 = (bf16[160,512]{1,0:T(8,128)(2,1)S(1)}, bf16[160,512]{1,0:T(8,128)(2,1)S(1)}, u32[]{:S(2)}, u32[]{:S(2)}) collective-permute-start(bf16[160,512]{1,0:T(8,128)(2,1)S(1)} %collective-permute-done.26.refs_1_), channel_id=1, source_target_pairs={{0,1},{1,0},{2,3},{3,2},{4,5},{5,4},{6,7},{7,6},{8,9},{9,8},{10,11... | collective-permute-start | bytes 491528 | tf_op jit(solution)/shard_map/ppermute | solution.py:422
  67.5 2.2 %copy-start.2 = (bf16[1,1024,2048]{2,1,0:T(8,128)(2,1)S(1)}, bf16[1,1024,2048]{2,1,0:T(8,128)(2,1)}, u32[]{:S(2)}) copy-start(bf16[1,1024,2048]{2,1,0:T(8,128)(2,1)} %lower_ref.3) | copy-start | bytes 12582916
  67.6 2.3 %copy-start.5 = (bf16[128,2048]{1,0:T(8,128)(2,1)S(1)}, bf16[128,2048]{1,0:T(8,128)(2,1)}, u32[]{:S(2)}) copy-start(bf16[128,2048]{1,0:T(8,128)(2,1)} %cl_ref.3) | copy-start | bytes 1572868
  72.8 5.4 %collective-permute-start.17 = (bf16[160,512]{1,0:T(8,128)(2,1)S(1)}, bf16[160,512]{1,0:T(8,128)(2,1)S(1)}, u32[]{:S(2)}, u32[]{:S(2)}) collective-permute-start(bf16[160,512]{1,0:T(8,128)(2,1)S(1)} %get-tuple-element.109), channel_id=1, source_target_pairs={{0,1},{1,0},{2,3},{3,2},{4,5},{5,4},{6,7},{7,6},{8,9},{9,8},{10,11... | collective-permute-start | bytes 491528 | tf_op jit(solution)/shard_map/ppermute | solution.py:422
  76.3 3.5 %collective-permute-start.30 = (bf16[160,512]{1,0:T(8,128)(2,1)S(1)}, bf16[160,512]{1,0:T(8,128)(2,1)S(1)}, u32[]{:S(2)}, u32[]{:S(2)}) collective-permute-start(bf16[160,512]{1,0:T(8,128)(2,1)S(1)} %get-tuple-element.130), channel_id=1, source_target_pairs={{0,1},{1,0},{2,3},{3,2},{4,5},{5,4},{6,7},{7,6},{8,9},{9,8},{10,11... | collective-permute-start | bytes 491528 | tf_op jit(solution)/shard_map/ppermute | solution.py:422
  76.4 9.9 %collective-permute-start.29 = (bf16[160,512]{1,0:T(8,128)(2,1)S(1)}, bf16[160,512]{1,0:T(8,128)(2,1)S(1)}, u32[]{:S(2)}, u32[]{:S(2)}) collective-permute-start(bf16[160,512]{1,0:T(8,128)(2,1)S(1)} %get-tuple-element.128), channel_id=1, source_target_pairs={{0,1},{1,0},{2,3},{3,2},{4,5},{5,4},{6,7},{7,6},{8,9},{9,8},{10,11... | collective-permute-start | bytes 491528 | tf_op jit(solution)/shard_map/ppermute | solution.py:422
  76.8 3.6 %collective-permute-start.16 = (bf16[160,512]{1,0:T(8,128)(2,1)S(1)}, bf16[160,512]{1,0:T(8,128)(2,1)S(1)}, u32[]{:S(2)}, u32[]{:S(2)}) collective-permute-start(bf16[160,512]{1,0:T(8,128)(2,1)S(1)} %get-tuple-element.107), channel_id=1, source_target_pairs={{0,1},{1,0},{2,3},{3,2},{4,5},{5,4},{6,7},{7,6},{8,9},{9,8},{10,11... | collective-permute-start | bytes 491528 | tf_op jit(solution)/shard_map/ppermute | solution.py:422
  77.5 30.8 %copy-start.15 = (f32[512]{0:T(512)S(1)}, f32[512]{0:T(512)}, u32[]{:S(2)}) copy-start(f32[512]{0:T(512)} %param.41) | copy-start | bytes 6148
  78.2 7.1 %collective-permute-start.18 = (bf16[160,512]{1,0:T(8,128)(2,1)S(1)}, bf16[160,512]{1,0:T(8,128)(2,1)S(1)}, u32[]{:S(2)}, u32[]{:S(2)}) collective-permute-start(bf16[160,512]{1,0:T(8,128)(2,1)S(1)} %add_convert_fusion.3), channel_id=1, source_target_pairs={{0,2},{1,3},{2,0},{3,1},{4,6},{5,7},{6,4},{7,5},{8,10},{9,11},{10,... | collective-permute-start | bytes 491528 | tf_op jit(solution)/shard_map/ppermute | solution.py:422
  79.8 8.5 %collective-permute-start.31 = (bf16[160,512]{1,0:T(8,128)(2,1)S(1)}, bf16[160,512]{1,0:T(8,128)(2,1)S(1)}, u32[]{:S(2)}, u32[]{:S(2)}) collective-permute-start(bf16[160,512]{1,0:T(8,128)(2,1)S(1)} %add_convert_fusion.1), channel_id=1, source_target_pairs={{0,2},{1,3},{2,0},{3,1},{4,6},{5,7},{6,4},{7,5},{8,10},{9,11},{10,... | collective-permute-start | bytes 491528 | tf_op jit(solution)/shard_map/ppermute | solution.py:422
  85.4 8.9 %collective-permute-start.19 = (bf16[40,512]{1,0:T(8,128)(2,1)S(1)}, bf16[40,512]{1,0:T(8,128)(2,1)S(1)}, u32[]{:S(2)}, u32[]{:S(2)}) collective-permute-start(bf16[40,512]{1,0:T(8,128)(2,1)S(1)} %get-tuple-element.139), channel_id=1, source_target_pairs={{0,4},{4,0},{8,12},{12,8},{16,20},{20,16},{24,28},{28,24},{1,5},{5... | collective-permute-start | bytes 122888 | tf_op jit(solution)/shard_map/ppermute | solution.py:422
  88.4 10.0 %collective-permute-start.32 = (bf16[40,512]{1,0:T(8,128)(2,1)S(1)}, bf16[40,512]{1,0:T(8,128)(2,1)S(1)}, u32[]{:S(2)}, u32[]{:S(2)}) collective-permute-start(bf16[40,512]{1,0:T(8,128)(2,1)S(1)} %get-tuple-element.136), channel_id=1, source_target_pairs={{0,16},{4,20},{8,24},{12,28},{16,0},{20,4},{24,8},{28,12},{1,17},{... | collective-permute-start | bytes 122888 | tf_op jit(solution)/shard_map/ppermute | solution.py:422
  89.9 7.6 %collective-permute-start.20 = (bf16[40,512]{1,0:T(8,128)(2,1)S(1)}, bf16[40,512]{1,0:T(8,128)(2,1)S(1)}, u32[]{:S(2)}, u32[]{:S(2)}) collective-permute-start(bf16[40,512]{1,0:T(8,128)(2,1)S(1)} %get-tuple-element.138), channel_id=1, source_target_pairs={{0,8},{4,12},{8,0},{12,4},{16,24},{20,28},{24,16},{28,20},{1,9},{5... | collective-permute-start | bytes 122888 | tf_op jit(solution)/shard_map/ppermute | solution.py:422
  92.2 6.2 %collective-permute-start.21 = (bf16[40,512]{1,0:T(8,128)(2,1)S(1)}, bf16[40,512]{1,0:T(8,128)(2,1)S(1)}, u32[]{:S(2)}, u32[]{:S(2)}) collective-permute-start(bf16[40,512]{1,0:T(8,128)(2,1)S(1)} %get-tuple-element.137), channel_id=1, source_target_pairs={{0,12},{4,8},{8,4},{12,0},{16,28},{20,24},{24,20},{28,16},{1,13},{... | collective-permute-start | bytes 122888 | tf_op jit(solution)/shard_map/ppermute | solution.py:422
  92.8 6.2 %collective-permute-start.33 = (bf16[40,512]{1,0:T(8,128)(2,1)S(1)}, bf16[40,512]{1,0:T(8,128)(2,1)S(1)}, u32[]{:S(2)}, u32[]{:S(2)}) collective-permute-start(bf16[40,512]{1,0:T(8,128)(2,1)S(1)} %get-tuple-element.135), channel_id=1, source_target_pairs={{0,20},{4,16},{8,28},{12,24},{16,4},{20,0},{24,12},{28,8},{1,21},{... | collective-permute-start | bytes 122888 | tf_op jit(solution)/shard_map/ppermute | solution.py:422
  94.3 5.8 %collective-permute-start.34 = (bf16[40,512]{1,0:T(8,128)(2,1)S(1)}, bf16[40,512]{1,0:T(8,128)(2,1)S(1)}, u32[]{:S(2)}, u32[]{:S(2)}) collective-permute-start(bf16[40,512]{1,0:T(8,128)(2,1)S(1)} %get-tuple-element.134), channel_id=1, source_target_pairs={{0,24},{4,28},{8,16},{12,20},{16,8},{20,12},{24,0},{28,4},{1,25},{... | collective-permute-start | bytes 122888 | tf_op jit(solution)/shard_map/ppermute | solution.py:422
  97.5 6.7 %collective-permute-start.35 = (bf16[40,512]{1,0:T(8,128)(2,1)S(1)}, bf16[40,512]{1,0:T(8,128)(2,1)S(1)}, u32[]{:S(2)}, u32[]{:S(2)}) collective-permute-start(bf16[40,512]{1,0:T(8,128)(2,1)S(1)} %get-tuple-element.133), channel_id=1, source_target_pairs={{0,28},{4,24},{8,20},{12,16},{16,12},{20,8},{24,4},{28,0},{1,29},{... | collective-permute-start | bytes 122888 | tf_op jit(solution)/shard_map/ppermute | solution.py:422
  104.6 3.1 %collective-permute-start.36 = (f32[2,128]{1,0:T(2,128)S(1)}, f32[2,128]{1,0:T(2,128)S(1)}, u32[]{:S(2)}, u32[]{:S(2)}) collective-permute-start(f32[2,128]{1,0:T(2,128)S(1)} %pad_maximum_fusion), channel_id=1, source_target_pairs={{0,3},{1,2},{2,1},{3,0},{4,7},{5,6},{6,5},{7,4},{8,11},{9,10},{10,... | collective-permute-start | bytes 3080 | tf_op jit(solution)/shard_map/ppermute | solution.py:422
  104.6 3.6 %collective-permute-start.37 = (f32[2,128]{1,0:T(2,128)S(1)}, f32[2,128]{1,0:T(2,128)S(1)}, u32[]{:S(2)}, u32[]{:S(2)}) collective-permute-start(f32[2,128]{1,0:T(2,128)S(1)} %pad_maximum_fusion), channel_id=1, source_target_pairs={{0,2},{1,3},{2,0},{3,1},{4,6},{5,7},{6,4},{7,5},{8,10},{9,11},{10,... | collective-permute-start | bytes 3080 | tf_op jit(solution)/shard_map/ppermute | solution.py:422
  106.3 2.0 %collective-permute-start.38 = (f32[2,128]{1,0:T(2,128)S(1)}, f32[2,128]{1,0:T(2,128)S(1)}, u32[]{:S(2)}, u32[]{:S(2)}) collective-permute-start(f32[2,128]{1,0:T(2,128)S(1)} %pad_maximum_fusion), channel_id=1, source_target_pairs={{0,1},{1,0},{2,3},{3,2},{4,5},{5,4},{6,7},{7,6},{8,9},{9,8},{10,11... | collective-permute-start | bytes 3080 | tf_op jit(solution)/shard_map/ppermute | solution.py:422

commit v5 on v4

--- a/solution.py
+++ b/solution.py
@@ -348,7 +348,7 @@
             product(weight_refs[j], sum_refs[j], gain_refs[j], cut)
         return 0
 
-    lax.fori_loop(0, weight_refs[0].shape[2] // step, chunk, 0)
+    lax.fori_loop(0, weight_refs[0].shape[2] // step, chunk, 0, unroll=True)
     for k in range(2):
         note_refs[k][...] = read_notes(piece_refs[k], capacity, slots, fields)
 
@@ -395,7 +395,7 @@
         hidden_ref[:, cut] = (silu(gate) * lift * share).astype(BF16)
         return 0
 
-    lax.fori_loop(0, weight_refs[0].shape[2] // step, chunk, 0)
+    lax.fori_loop(0, weight_refs[0].shape[2] // step, chunk, 0, unroll=True)
     lane = lax.broadcasted_iota(jnp.int32, (height, 128), 1)
     row_ref[...] = jnp.where(lane == 0, offsets[0], flag * scale * ALPHA)
     for k in range(count - 1, 0, -2):
@@ -664,7 +664,7 @@
         arrived.append(jnp.concatenate(moved, 0))
     hidden = specialist_valve_matrix.shape[2]
     shared = common_valve_matrix.shape[1]
-    step = min(hidden, 256)
+    step = min(hidden, 512)
     weights = (specialist_valve_matrix, specialist_raising_matrix, common_valve_matrix, common_raising_matrix)
     work = 4 * total * width * (hidden + shared)
     height = total // len(parts)

time: 109 us -> 107 us (0.982)
  Pallas kernels: 18.8 us -> 15.7 us
    pallas_call x14, Pallas kernels: 18.8 us -> 15.7 us  [call(): pl.pallas_call(kernel, out_shape=shapes, in_specs=in_specs or [vmem()] *...]
  transfers between devices with their start and end apart: 39 -> 39, of which waited for: 20 -> 20; matrix products, arithmetic and copies ran while one was open for 0% -> 0% of each run, Pallas kernels for 11% -> 8%
where the time goes in v5:
time: 107 us
  waiting for transfers between devices  44.2 us (41%)
  starting transfers between devices  42.9 us (40%)
  Pallas kernels  15.7 us (15%)
  local copies, waits for them, and re-layouts  2.21 us (2%)
  other arithmetic  1.09 us (1%)
    ppermute x38, waiting for transfers between devices, swap(): return lax.ppermute(array, axis, [(i, i ^ bit) for i in range(size)])  42.8 us
    ppermute x38, starting transfers between devices, swap(): return lax.ppermute(array, axis, [(i, i ^ bit) for i in range(size)])  38.2 us
    pallas_call x14, Pallas kernels, call(): pl.pallas_call(kernel, out_shape=shapes, in_specs=in_specs or [vmem()] *...  15.7 us
    ppermute x1, starting transfers between devices, shards(): got = lax.ppermute(leaving, 'sp', onward)  4.66 us
    unnamed x44, local copies, waits for them, and re-layouts  2.17 us
  transfers between devices with their start and end apart: 39, of which 20 were waited for; matrix products, arithmetic and copies ran while one was open for 0% of the time, Pallas kernels for 8%

profile of v5, /device:TPU:0, one launch (start us, length us, event | category | flops | bytes accessed | tf_op | source)
XLA Modules:
  0.0 106.8 jit_solution(7088696994518005424)
XLA Ops:
  0.0 4.6 %shard_map.200 = (bf16[272,128]{1,0:T(8,128)(2,1)}, bf16[272,128]{1,0:T(8,128)(2,1)}, bf16[272,128]{1,0:T(8,128)(2,1)}, bf16[272,128]{1,0:T(8,128)(2,1)}, f32[128,512]{1,0:T(8,128)}, /*index=5*/f32[128,512]{1,0:T(8,128)}) custom-call(s32[1]{0:T(128)} %bitcast.4.refs_0_.place_ref.group_ref, bf16[128,512]{1,0:T(8,128)(2,1)} %refs_1_.1, ...), custom_call_target="tpu_custom_call" | custom-call | flops 2000000000 | bytes 399892 | tf_op jit(solution)/shard_map/pallas_call | solution.py:477
  4.6 3.0 %collective-permute-start = (bf16[272,128]{1,0:T(8,128)(2,1)}, bf16[272,128]{1,0:T(8,128)(2,1)S(1)}, u32[]{:S(2)}, u32[]{:S(2)}) collective-permute-start(bf16[272,128]{1,0:T(8,128)(2,1)} %get-tuple-element.72), channel_id=1, source_target_pairs={{0,4},{4,0},{8,12},{12,8},{16,20},{20,16},{24,28},{28,24},{1,5},{5... | collective-permute-start | bytes 208904 | tf_op jit(solution)/shard_map/ppermute | solution.py:422
  7.6 1.6 %collective-permute-start.1 = (bf16[272,128]{1,0:T(8,128)(2,1)}, bf16[272,128]{1,0:T(8,128)(2,1)S(1)}, u32[]{:S(2)}, u32[]{:S(2)}) collective-permute-start(bf16[272,128]{1,0:T(8,128)(2,1)} %get-tuple-element.73), channel_id=1, source_target_pairs={{0,8},{4,12},{8,0},{12,4},{16,24},{20,28},{24,16},{28,20},{1,9},{5... | collective-permute-start | bytes 208904 | tf_op jit(solution)/shard_map/ppermute | solution.py:422
  9.1 0.9 copy-done.14
  10.1 2.6 %collective-permute-done.1.refs_2_ = bf16[272,128]{1,0:T(8,128)(2,1)S(1)} collective-permute-done((bf16[272,128]{1,0:T(8,128)(2,1)}, bf16[272,128]{1,0:T(8,128)(2,1)S(1)}, u32[]{:S(2)}, u32[]{:S(2)}) %collective-permute-start.1) | collective-permute-done | bytes 69664 | tf_op jit(solution)/shard_map/ppermute | solution.py:422
  12.7 1.9 %collective-permute-done.2.refs_3_ = bf16[272,128]{1,0:T(8,128)(2,1)S(1)} collective-permute-done((bf16[272,128]{1,0:T(8,128)(2,1)}, bf16[272,128]{1,0:T(8,128)(2,1)S(1)}, u32[]{:S(2)}, u32[]{:S(2)}) %collective-permute-start.2) | collective-permute-done | bytes 69664 | tf_op jit(solution)/shard_map/ppermute | solution.py:422
  14.5 1.2 %shard_map.202 = (f32[4,128,128]{2,1,0:T(8,128)S(1)}, bf16[4,128,128]{2,1,0:T(8,128)(2,1)S(1)}, bf16[16,128]{1,0:T(8,128)(2,1)S(1)}, bf16[144,128]{1,0:T(8,128)(2,1)S(1)}, f32[256,128]{1,0:T(8,128)}) custom-call(s32[1]{0:T(128)} %bitcast.4.refs_0_.place_ref.group_ref, bf16[272,128]{1,0:T(8,128)(2,1)S(1)} %shard_map.201.refs_0_, ...), custom_call_target="tpu_custom_call" | custom-call | flops 4000000000 | bytes 278532 | tf_op jit(solution)/shard_map/pallas_call | solution.py:477
  15.7 4.7 %collective-permute-start.3 = (bf16[144,128]{1,0:T(8,128)(2,1)S(1)}, bf16[144,128]{1,0:T(8,128)(2,1)S(1)}, u32[]{:S(2)}, u32[]{:S(2)}) collective-permute-start(bf16[144,128]{1,0:T(8,128)(2,1)S(1)} %get-tuple-element.75), channel_id=1, source_target_pairs={{0,16},{4,20},{8,24},{12,28},{1,17},{5,21},{9,25},{13,29},{2,18},{... | collective-permute-start | bytes 110600 | tf_op jit(solution)/shard_map/ppermute | solution.py:592
  20.4 1.4 %collective-permute-done.3.got_ref = bf16[144,128]{1,0:T(8,128)(2,1)S(1)} collective-permute-done((bf16[144,128]{1,0:T(8,128)(2,1)S(1)}, bf16[144,128]{1,0:T(8,128)(2,1)S(1)}, u32[]{:S(2)}, u32[]{:S(2)}) %collective-permute-start.3) | collective-permute-done | bytes 36896 | tf_op jit(solution)/shard_map/ppermute | solution.py:592
  22.0 0.6 collective-permute-start.4
  22.6 0.9 collective-permute-start.5
  23.5 2.1 %collective-permute-start.6 = (bf16[128,128]{1,0:T(8,128)(2,1)S(1)}, bf16[128,128]{1,0:T(8,128)(2,1)S(1)}, u32[]{:S(2)}, u32[]{:S(2)}) collective-permute-start(bf16[128,128]{1,0:T(8,128)(2,1)S(1)} %get-tuple-element.82), channel_id=1, source_target_pairs={{0,12},{4,8},{8,4},{12,0},{16,28},{20,24},{24,20},{28,16},{1,13},{... | collective-permute-start | bytes 98312 | tf_op jit(solution)/shard_map/ppermute | solution.py:422
  25.6 0.2 shard_map.199
  26.0 0.5 collective-permute-done.5.refs_2_
  26.5 1.8 %collective-permute-done.6.refs_3_ = bf16[128,128]{1,0:T(8,128)(2,1)S(1)} collective-permute-done((bf16[128,128]{1,0:T(8,128)(2,1)S(1)}, bf16[128,128]{1,0:T(8,128)(2,1)S(1)}, u32[]{:S(2)}, u32[]{:S(2)}) %collective-permute-start.6) | collective-permute-done | bytes 32800 | tf_op jit(solution)/shard_map/ppermute | solution.py:422
  28.3 0.6 shard_map.204
  29.1 0.3 shard_map.205
  29.4 0.5 collective-permute-start.7
  29.9 0.4 collective-permute-done.8
  30.4 1.6 %collective-permute-start.9 = (bf16[128,512]{1,0:T(8,128)(2,1)S(1)}, bf16[128,512]{1,0:T(8,128)(2,1)S(1)}, u32[]{:S(2)}, u32[]{:S(2)}) collective-permute-start(bf16[128,512]{1,0:T(8,128)(2,1)S(1)} %add_convert_fusion.4), channel_id=1, source_target_pairs={{0,2},{1,3},{2,0},{3,1},{4,6},{5,7},{6,4},{7,5},{8,10},{9,11},{10,... | collective-permute-start | bytes 393224 | tf_op jit(solution)/shard_map/ppermute | solution.py:422
  32.0 4.0 %collective-permute-done.9.got_ref = bf16[128,512]{1,0:T(8,128)(2,1)S(1)} collective-permute-done((bf16[128,512]{1,0:T(8,128)(2,1)S(1)}, bf16[128,512]{1,0:T(8,128)(2,1)S(1)}, u32[]{:S(2)}, u32[]{:S(2)}) %collective-permute-start.9) | collective-permute-done | bytes 131104 | tf_op jit(solution)/shard_map/ppermute | solution.py:422
  36.1 0.6 shard_map.206
  36.7 3.3 %collective-permute-start.22 = (bf16[40,512]{1,0:T(8,128)(2,1)S(1)}, bf16[40,512]{1,0:T(8,128)(2,1)S(1)}, u32[]{:S(2)}, u32[]{:S(2)}) collective-permute-start(bf16[40,512]{1,0:T(8,128)(2,1)S(1)} %get-tuple-element.110), channel_id=1, source_target_pairs={{0,16},{4,20},{8,24},{12,28},{16,0},{20,4},{24,8},{28,12},{1,17},{... | collective-permute-start | bytes 122888 | tf_op jit(solution)/shard_map/ppermute | solution.py:422
  40.0 0.6 collective-permute-start.23
  40.6 3.9 %collective-permute-start.24 = (bf16[40,512]{1,0:T(8,128)(2,1)S(1)}, bf16[40,512]{1,0:T(8,128)(2,1)S(1)}, u32[]{:S(2)}, u32[]{:S(2)}) collective-permute-start(bf16[40,512]{1,0:T(8,128)(2,1)S(1)} %get-tuple-element.112), channel_id=1, source_target_pairs={{0,24},{4,28},{8,16},{12,20},{16,8},{20,12},{24,0},{28,4},{1,25},{... | collective-permute-start | bytes 122888 | tf_op jit(solution)/shard_map/ppermute | solution.py:422
  44.4 0.3 collective-permute-start.25
  44.8 1.1 %collective-permute-start.10 = (bf16[40,512]{1,0:T(8,128)(2,1)S(1)}, bf16[40,512]{1,0:T(8,128)(2,1)S(1)}, u32[]{:S(2)}, u32[]{:S(2)}) collective-permute-start(bf16[40,512]{1,0:T(8,128)(2,1)S(1)} %get-tuple-element.90), channel_id=1, source_target_pairs={{0,4},{4,0},{8,12},{12,8},{16,20},{20,16},{24,28},{28,24},{1,5},{5... | collective-permute-start | bytes 122888 | tf_op jit(solution)/shard_map/ppermute | solution.py:422
  45.9 3.2 %collective-permute-done.10 = bf16[40,512]{1,0:T(8,128)(2,1)S(1)} collective-permute-done((bf16[40,512]{1,0:T(8,128)(2,1)S(1)}, bf16[40,512]{1,0:T(8,128)(2,1)S(1)}, u32[]{:S(2)}, u32[]{:S(2)}) %collective-permute-start.10) | collective-permute-done | bytes 40992 | tf_op jit(solution)/shard_map/ppermute | solution.py:422
  49.1 4.4 %collective-permute-done.11 = bf16[40,512]{1,0:T(8,128)(2,1)S(1)} collective-permute-done((bf16[40,512]{1,0:T(8,128)(2,1)S(1)}, bf16[40,512]{1,0:T(8,128)(2,1)S(1)}, u32[]{:S(2)}, u32[]{:S(2)}) %collective-permute-start.11) | collective-permute-done | bytes 40992 | tf_op jit(solution)/shard_map/ppermute | solution.py:422
  53.5 4.9 %collective-permute-done.12 = bf16[40,512]{1,0:T(8,128)(2,1)S(1)} collective-permute-done((bf16[40,512]{1,0:T(8,128)(2,1)S(1)}, bf16[40,512]{1,0:T(8,128)(2,1)S(1)}, u32[]{:S(2)}, u32[]{:S(2)}) %collective-permute-start.12) | collective-permute-done | bytes 40992 | tf_op jit(solution)/shard_map/ppermute | solution.py:422
  58.4 1.5 %collective-permute-start.13 = (bf16[160,512]{1,0:T(8,128)(2,1)S(1)}, bf16[160,512]{1,0:T(8,128)(2,1)S(1)}, u32[]{:S(2)}, u32[]{:S(2)}) collective-permute-start(bf16[160,512]{1,0:T(8,128)(2,1)S(1)} %constant_dynamic-update-slice_fusion.refs_1_.own_ref), channel_id=1, source_target_pairs={{0,2},{1,3},{2,0},{3,1},{4,6},{5,7},{6,4},{7,5},{8,10},{9,11},{10,... | collective-permute-start | bytes 491528 | tf_op jit(solution)/shard_map/ppermute | solution.py:422
  60.0 0.6 collective-permute-start.26
  60.6 0.5 collective-permute-start.15
  61.1 2.6 %collective-permute-done.13.refs_1_ = bf16[160,512]{1,0:T(8,128)(2,1)S(1)} collective-permute-done((bf16[160,512]{1,0:T(8,128)(2,1)S(1)}, bf16[160,512]{1,0:T(8,128)(2,1)S(1)}, u32[]{:S(2)}, u32[]{:S(2)}) %collective-permute-start.13) | collective-permute-done | bytes 163872 | tf_op jit(solution)/shard_map/ppermute | solution.py:422
  63.8 1.8 %collective-permute-done.26.refs_1_ = bf16[160,512]{1,0:T(8,128)(2,1)S(1)} collective-permute-done((bf16[160,512]{1,0:T(8,128)(2,1)S(1)}, bf16[160,512]{1,0:T(8,128)(2,1)S(1)}, u32[]{:S(2)}, u32[]{:S(2)}) %collective-permute-start.26) | collective-permute-done | bytes 163872 | tf_op jit(solution)/shard_map/ppermute | solution.py:422
  65.5 1.1 %shard_map.210 = (f32[160,1024]{1,0:T(8,128)S(1)}, f32[160,1024]{1,0:T(8,128)S(1)}, f32[160,128]{1,0:T(8,128)S(1)}, f32[160,128]{1,0:T(8,128)S(1)}, f32[8,1024]{...) custom-call(s32[1]{0:T(128)} %bitcast.3.place_ref.refs_0_, ...), custom_call_target="tpu_custom_call" | custom-call | flops 754974720 | bytes 9764868 | tf_op jit(solution)/shard_map/pallas_call | solution.py:477
  66.7 1.1 %shard_map.207 = (f32[160,1024]{1,0:T(8,128)S(1)}, f32[160,1024]{1,0:T(8,128)S(1)}, f32[160,128]{1,0:T(8,128)S(1)}, f32[160,128]{1,0:T(8,128)S(1)}, f32[8,1024]{...) custom-call(s32[1]{0:T(128)} %bitcast.3.place_ref.refs_0_, ...), custom_call_target="tpu_custom_call" | custom-call | flops 754974720 | bytes 9764868 | tf_op jit(solution)/shard_map/pallas_call | solution.py:477
  67.8 1.1 copy-done.2
  69.0 2.2 %shard_map.208 = (bf16[160,512]{1,0:T(8,128)(2,1)S(1)}, bf16[160,512]{1,0:T(8,128)(2,1)S(1)}, bf16[160,1024]{1,0:T(8,128)(2,1)S(1)}, bf16[160,128]{1,0:T(8,128)(2,1)S(1)}, f32[160,128]{1,0:T(8,128)S(1)}) custom-call(s32[1]{0:T(128)} %bitcast.3.place_ref.refs_0_, bf16[160,512]{1,0:T(8,128)(2,1)S(1)} %collective-permute-done.13.refs_1_, ...), custom_call_target="tpu_custom_call" | custom-call | flops 1509949440 | bytes 16195588 | tf_op jit(solution)/shard_map/pallas_call | solution.py:477
  71.2 0.6 collective-permute-start.17
  71.8 2.2 %shard_map.211 = (bf16[160,512]{1,0:T(8,128)(2,1)S(1)}, bf16[160,512]{1,0:T(8,128)(2,1)S(1)}, bf16[160,1024]{1,0:T(8,128)(2,1)S(1)}, bf16[160,128]{1,0:T(8,128)(2,1)S(1)}, f32[160,128]{1,0:T(8,128)S(1)}) custom-call(s32[1]{0:T(128)} %bitcast.3.place_ref.refs_0_, bf16[160,512]{1,0:T(8,128)(2,1)S(1)} %collective-permute-done.26.refs_1_, ...), custom_call_target="tpu_custom_call" | custom-call | flops 1509949440 | bytes 16195588 | tf_op jit(solution)/shard_map/pallas_call | solution.py:477
  74.1 0.5 collective-permute-start.29
  74.7 0.6 shard_map.212
  75.3 0.6 shard_map.209
  75.9 1.6 %collective-permute-start.18 = (bf16[160,512]{1,0:T(8,128)(2,1)S(1)}, bf16[160,512]{1,0:T(8,128)(2,1)S(1)}, u32[]{:S(2)}, u32[]{:S(2)}) collective-permute-start(bf16[160,512]{1,0:T(8,128)(2,1)S(1)} %add_convert_fusion.3), channel_id=1, source_target_pairs={{0,2},{1,3},{2,0},{3,1},{4,6},{5,7},{6,4},{7,5},{8,10},{9,11},{10,... | collective-permute-start | bytes 491528 | tf_op jit(solution)/shard_map/ppermute | solution.py:422
  77.5 0.6 collective-permute-start.31
  78.2 4.9 %collective-permute-done.18 = bf16[160,512]{1,0:T(8,128)(2,1)S(1)} collective-permute-done((bf16[160,512]{1,0:T(8,128)(2,1)S(1)}, bf16[160,512]{1,0:T(8,128)(2,1)S(1)}, u32[]{:S(2)}, u32[]{:S(2)}) %collective-permute-start.18) | collective-permute-done | bytes 163872 | tf_op jit(solution)/shard_map/ppermute | solution.py:422
  83.2 0.8 collective-permute-start.19
  84.0 2.0 %collective-permute-done.31 = bf16[160,512]{1,0:T(8,128)(2,1)S(1)} collective-permute-done((bf16[160,512]{1,0:T(8,128)(2,1)S(1)}, bf16[160,512]{1,0:T(8,128)(2,1)S(1)}, u32[]{:S(2)}, u32[]{:S(2)}) %collective-permute-start.31) | collective-permute-done | bytes 163872 | tf_op jit(solution)/shard_map/ppermute | solution.py:422
  86.1 1.5 %collective-permute-start.32 = (bf16[40,512]{1,0:T(8,128)(2,1)S(1)}, bf16[40,512]{1,0:T(8,128)(2,1)S(1)}, u32[]{:S(2)}, u32[]{:S(2)}) collective-permute-start(bf16[40,512]{1,0:T(8,128)(2,1)S(1)} %get-tuple-element.136), channel_id=1, source_target_pairs={{0,16},{4,20},{8,24},{12,28},{16,0},{20,4},{24,8},{28,12},{1,17},{... | collective-permute-start | bytes 122888 | tf_op jit(solution)/shard_map/ppermute | solution.py:422
  87.7 2.3 %collective-permute-start.20 = (bf16[40,512]{1,0:T(8,128)(2,1)S(1)}, bf16[40,512]{1,0:T(8,128)(2,1)S(1)}, u32[]{:S(2)}, u32[]{:S(2)}) collective-permute-start(bf16[40,512]{1,0:T(8,128)(2,1)S(1)} %get-tuple-element.138), channel_id=1, source_target_pairs={{0,8},{4,12},{8,0},{12,4},{16,24},{20,28},{24,16},{28,20},{1,9},{5... | collective-permute-start | bytes 122888 | tf_op jit(solution)/shard_map/ppermute | solution.py:422
  89.9 0.6 collective-permute-start.21
  90.6 1.5 %collective-permute-start.33 = (bf16[40,512]{1,0:T(8,128)(2,1)S(1)}, bf16[40,512]{1,0:T(8,128)(2,1)S(1)}, u32[]{:S(2)}, u32[]{:S(2)}) collective-permute-start(bf16[40,512]{1,0:T(8,128)(2,1)S(1)} %get-tuple-element.135), channel_id=1, source_target_pairs={{0,20},{4,16},{8,28},{12,24},{16,4},{20,0},{24,12},{28,8},{1,21},{... | collective-permute-start | bytes 122888 | tf_op jit(solution)/shard_map/ppermute | solution.py:422
  92.1 3.2 %collective-permute-start.34 = (bf16[40,512]{1,0:T(8,128)(2,1)S(1)}, bf16[40,512]{1,0:T(8,128)(2,1)S(1)}, u32[]{:S(2)}, u32[]{:S(2)}) collective-permute-start(bf16[40,512]{1,0:T(8,128)(2,1)S(1)} %get-tuple-element.134), channel_id=1, source_target_pairs={{0,24},{4,28},{8,16},{12,20},{16,8},{20,12},{24,0},{28,4},{1,25},{... | collective-permute-start | bytes 122888 | tf_op jit(solution)/shard_map/ppermute | solution.py:422
  95.2 0.9 collective-permute-start.35
  96.2 0.6 collective-permute-done.33
  96.7 1.1 %collective-permute-done.34 = bf16[40,512]{1,0:T(8,128)(2,1)S(1)} collective-permute-done((bf16[40,512]{1,0:T(8,128)(2,1)S(1)}, bf16[40,512]{1,0:T(8,128)(2,1)S(1)}, u32[]{:S(2)}, u32[]{:S(2)}) %collective-permute-start.34) | collective-permute-done | bytes 40992 | tf_op jit(solution)/shard_map/ppermute | solution.py:422
  97.9 4.1 %collective-permute-done.35 = bf16[40,512]{1,0:T(8,128)(2,1)S(1)} collective-permute-done((bf16[40,512]{1,0:T(8,128)(2,1)S(1)}, bf16[40,512]{1,0:T(8,128)(2,1)S(1)}, u32[]{:S(2)}, u32[]{:S(2)}) %collective-permute-start.35) | collective-permute-done | bytes 40992 | tf_op jit(solution)/shard_map/ppermute | solution.py:422
  101.9 0.3 fusion.2
  102.4 1.7 %collective-permute-start.37 = (f32[2,128]{1,0:T(2,128)S(1)}, f32[2,128]{1,0:T(2,128)S(1)}, u32[]{:S(2)}, u32[]{:S(2)}) collective-permute-start(f32[2,128]{1,0:T(2,128)S(1)} %pad_maximum_fusion), channel_id=1, source_target_pairs={{0,2},{1,3},{2,0},{3,1},{4,6},{5,7},{6,4},{7,5},{8,10},{9,11},{10,... | collective-permute-start | bytes 3080 | tf_op jit(solution)/shard_map/ppermute | solution.py:422
  104.0 0.2 collective-permute-start.38
  104.2 1.1 %collective-permute-done.36 = f32[2,128]{1,0:T(2,128)S(1)} collective-permute-done((f32[2,128]{1,0:T(2,128)S(1)}, f32[2,128]{1,0:T(2,128)S(1)}, u32[]{:S(2)}, u32[]{:S(2)}) %collective-permute-start.36) | collective-permute-done | bytes 1056 | tf_op jit(solution)/shard_map/ppermute | solution.py:422
  105.4 0.7 collective-permute-done.37
  106.1 0.8 multiply_convert_fusion
  (89 shorter events, 1.4 us)
Async XLA Ops:
  4.6 5.5 %collective-permute-start = (bf16[272,128]{1,0:T(8,128)(2,1)}, bf16[272,128]{1,0:T(8,128)(2,1)S(1)}, u32[]{:S(2)}, u32[]{:S(2)}) collective-permute-start(bf16[272,128]{1,0:T(8,128)(2,1)} %get-tuple-element.72), channel_id=1, source_target_pairs={{0,4},{4,0},{8,12},{12,8},{16,20},{20,16},{24,28},{28,24},{1,5},{5... | collective-permute-start | bytes 208904 | tf_op jit(solution)/shard_map/ppermute | solution.py:422
  7.6 5.1 %collective-permute-start.1 = (bf16[272,128]{1,0:T(8,128)(2,1)}, bf16[272,128]{1,0:T(8,128)(2,1)S(1)}, u32[]{:S(2)}, u32[]{:S(2)}) collective-permute-start(bf16[272,128]{1,0:T(8,128)(2,1)} %get-tuple-element.73), channel_id=1, source_target_pairs={{0,8},{4,12},{8,0},{12,4},{16,24},{20,28},{24,16},{28,20},{1,9},{5... | collective-permute-start | bytes 208904 | tf_op jit(solution)/shard_map/ppermute | solution.py:422
  9.1 5.4 %collective-permute-start.2 = (bf16[272,128]{1,0:T(8,128)(2,1)}, bf16[272,128]{1,0:T(8,128)(2,1)S(1)}, u32[]{:S(2)}, u32[]{:S(2)}) collective-permute-start(bf16[272,128]{1,0:T(8,128)(2,1)} %get-tuple-element.74), channel_id=1, source_target_pairs={{0,12},{4,8},{8,4},{12,0},{16,28},{20,24},{24,20},{28,16},{1,13},{... | collective-permute-start | bytes 208904 | tf_op jit(solution)/shard_map/ppermute | solution.py:422
  9.1 0.9 copy-start.14
  15.7 6.1 %collective-permute-start.3 = (bf16[144,128]{1,0:T(8,128)(2,1)S(1)}, bf16[144,128]{1,0:T(8,128)(2,1)S(1)}, u32[]{:S(2)}, u32[]{:S(2)}) collective-permute-start(bf16[144,128]{1,0:T(8,128)(2,1)S(1)} %get-tuple-element.75), channel_id=1, source_target_pairs={{0,16},{4,20},{8,24},{12,28},{1,17},{5,21},{9,25},{13,29},{2,18},{... | collective-permute-start | bytes 110600 | tf_op jit(solution)/shard_map/ppermute | solution.py:592
  21.8 3.7 %copy-start.10 = (s32[128,2]{0,1:T(2,128)S(1)}, s32[128,2]{0,1:T(2,128)}, u32[]{:S(2)}) copy-start(s32[128,2]{0,1:T(2,128)} %param.33) | copy-start | bytes 3076
  21.8 3.7 %copy-start.11 = (bf16[128,2]{0,1:T(2,128)(2,1)S(1)}, bf16[128,2]{0,1:T(2,128)(2,1)}, u32[]{:S(2)}) copy-start(bf16[128,2]{0,1:T(2,128)(2,1)} %param.34) | copy-start | bytes 1540
  22.0 4.0 %collective-permute-start.4 = (bf16[128,128]{1,0:T(8,128)(2,1)S(1)}, bf16[128,128]{1,0:T(8,128)(2,1)S(1)}, u32[]{:S(2)}, u32[]{:S(2)}) collective-permute-start(bf16[128,128]{1,0:T(8,128)(2,1)S(1)} %get-tuple-element.80), channel_id=1, source_target_pairs={{0,4},{4,0},{8,12},{12,8},{16,20},{20,16},{24,28},{28,24},{1,5},{5... | collective-permute-start | bytes 98312 | tf_op jit(solution)/shard_map/ppermute | solution.py:422
  22.6 3.9 %collective-permute-start.5 = (bf16[128,128]{1,0:T(8,128)(2,1)S(1)}, bf16[128,128]{1,0:T(8,128)(2,1)S(1)}, u32[]{:S(2)}, u32[]{:S(2)}) collective-permute-start(bf16[128,128]{1,0:T(8,128)(2,1)S(1)} %get-tuple-element.81), channel_id=1, source_target_pairs={{0,8},{4,12},{8,0},{12,4},{16,24},{20,28},{24,16},{28,20},{1,9},{5... | collective-permute-start | bytes 98312 | tf_op jit(solution)/shard_map/ppermute | solution.py:422
  23.5 4.8 %collective-permute-start.6 = (bf16[128,128]{1,0:T(8,128)(2,1)S(1)}, bf16[128,128]{1,0:T(8,128)(2,1)S(1)}, u32[]{:S(2)}, u32[]{:S(2)}) collective-permute-start(bf16[128,128]{1,0:T(8,128)(2,1)S(1)} %get-tuple-element.82), channel_id=1, source_target_pairs={{0,12},{4,8},{8,4},{12,0},{16,28},{20,24},{24,20},{28,16},{1,13},{... | collective-permute-start | bytes 98312 | tf_op jit(solution)/shard_map/ppermute | solution.py:422
  25.6 2.7 %copy-start.6 = (bf16[512,2048]{1,0:T(8,128)(2,1)S(1)}, bf16[512,2048]{1,0:T(8,128)(2,1)}, u32[]{:S(2)}) copy-start(bf16[512,2048]{1,0:T(8,128)(2,1)} %weight_ref.3) | copy-start | bytes 6291460
  25.6 2.7 %copy-start.7 = (bf16[128,512]{1,0:T(8,128)(2,1)S(1)}, bf16[128,512]{1,0:T(8,128)(2,1)}, u32[]{:S(2)}) copy-start(bf16[128,512]{1,0:T(8,128)(2,1)} %valve_ref.1) | copy-start | bytes 393220
  25.6 2.7 %copy-start.12 = (f32[128,512]{1,0:T(8,128)S(1)}, f32[128,512]{1,0:T(8,128)}, u32[]{:S(2)}) copy-start(f32[128,512]{1,0:T(8,128)} %get-tuple-element.69.local_ref) | copy-start | bytes 786436
  25.6 2.7 %copy-start.13 = (f32[128,512]{1,0:T(8,128)S(1)}, f32[128,512]{1,0:T(8,128)}, u32[]{:S(2)}) copy-start(f32[128,512]{1,0:T(8,128)} %get-tuple-element.70.query_ref) | copy-start | bytes 786436
  29.0 1.4 %collective-permute-start.8 = (bf16[128,512]{1,0:T(8,128)(2,1)S(1)}, bf16[128,512]{1,0:T(8,128)(2,1)S(1)}, u32[]{:S(2)}, u32[]{:S(2)}) collective-permute-start(bf16[128,512]{1,0:T(8,128)(2,1)S(1)} %get-tuple-element.87), channel_id=1, source_target_pairs={{0,1},{1,0},{2,3},{3,2},{4,5},{5,4},{6,7},{7,6},{8,9},{9,8},{10,11... | collective-permute-start | bytes 393224 | tf_op jit(solution)/shard_map/ppermute | solution.py:422
  29.0 7.0 %copy-start.8 = (bf16[128,512]{1,0:T(8,128)(2,1)S(1)}, bf16[128,512]{1,0:T(8,128)(2,1)}, u32[]{:S(2)}) copy-start(bf16[128,512]{1,0:T(8,128)(2,1)} %row_ref.1) | copy-start | bytes 393220
  29.0 7.0 %copy-start.9 = (f32[512]{0:T(512)S(1)}, f32[512]{0:T(512)}, u32[]{:S(2)}) copy-start(f32[512]{0:T(512)} %param.32) | copy-start | bytes 6148
  29.4 2.6 %collective-permute-start.7 = (bf16[128,512]{1,0:T(8,128)(2,1)S(1)}, bf16[128,512]{1,0:T(8,128)(2,1)S(1)}, u32[]{:S(2)}, u32[]{:S(2)}) collective-permute-start(bf16[128,512]{1,0:T(8,128)(2,1)S(1)} %get-tuple-element.85), channel_id=1, source_target_pairs={{0,1},{1,0},{2,3},{3,2},{4,5},{5,4},{6,7},{7,6},{8,9},{9,8},{10,11... | collective-permute-start | bytes 393224 | tf_op jit(solution)/shard_map/ppermute | solution.py:422
  30.4 5.6 %collective-permute-start.9 = (bf16[128,512]{1,0:T(8,128)(2,1)S(1)}, bf16[128,512]{1,0:T(8,128)(2,1)S(1)}, u32[]{:S(2)}, u32[]{:S(2)}) collective-permute-start(bf16[128,512]{1,0:T(8,128)(2,1)S(1)} %add_convert_fusion.4), channel_id=1, source_target_pairs={{0,2},{1,3},{2,0},{3,1},{4,6},{5,7},{6,4},{7,5},{8,10},{9,11},{10,... | collective-permute-start | bytes 393224 | tf_op jit(solution)/shard_map/ppermute | solution.py:422
  36.0 29.5 %copy-start = (bf16[1,2048,1024]{2,1,0:T(8,128)(2,1)S(1)}, bf16[1,2048,1024]{2,1,0:T(8,128)(2,1)}, u32[]{:S(2)}) copy-start(bf16[1,2048,1024]{2,1,0:T(8,128)(2,1)} %refs_3_.9) | copy-start | bytes 12582916
  36.0 29.5 %copy-start.1 = (bf16[1,2048,1024]{2,1,0:T(8,128)(2,1)S(1)}, bf16[1,2048,1024]{2,1,0:T(8,128)(2,1)}, u32[]{:S(2)}) copy-start(bf16[1,2048,1024]{2,1,0:T(8,128)(2,1)} %refs_4_.9) | copy-start | bytes 12582916
  36.0 29.5 %copy-start.3 = (bf16[2048,128]{1,0:T(8,128)(2,1)S(1)}, bf16[2048,128]{1,0:T(8,128)(2,1)}, u32[]{:S(2)}) copy-start(bf16[2048,128]{1,0:T(8,128)(2,1)} %refs_5_.9) | copy-start | bytes 1572868
  36.0 29.5 %copy-start.4 = (bf16[2048,128]{1,0:T(8,128)(2,1)S(1)}, bf16[2048,128]{1,0:T(8,128)(2,1)}, u32[]{:S(2)}) copy-start(bf16[2048,128]{1,0:T(8,128)(2,1)} %refs_6_.9) | copy-start | bytes 1572868
  36.7 23.2 %collective-permute-start.22 = (bf16[40,512]{1,0:T(8,128)(2,1)S(1)}, bf16[40,512]{1,0:T(8,128)(2,1)S(1)}, u32[]{:S(2)}, u32[]{:S(2)}) collective-permute-start(bf16[40,512]{1,0:T(8,128)(2,1)S(1)} %get-tuple-element.110), channel_id=1, source_target_pairs={{0,16},{4,20},{8,24},{12,28},{16,0},{20,4},{24,8},{28,12},{1,17},{... | collective-permute-start | bytes 122888 | tf_op jit(solution)/shard_map/ppermute | solution.py:422
  40.0 20.0 %collective-permute-start.23 = (bf16[40,512]{1,0:T(8,128)(2,1)S(1)}, bf16[40,512]{1,0:T(8,128)(2,1)S(1)}, u32[]{:S(2)}, u32[]{:S(2)}) collective-permute-start(bf16[40,512]{1,0:T(8,128)(2,1)S(1)} %get-tuple-element.111), channel_id=1, source_target_pairs={{0,20},{4,16},{8,28},{12,24},{16,4},{20,0},{24,12},{28,8},{1,21},{... | collective-permute-start | bytes 122888 | tf_op jit(solution)/shard_map/ppermute | solution.py:422
  40.6 19.4 %collective-permute-start.24 = (bf16[40,512]{1,0:T(8,128)(2,1)S(1)}, bf16[40,512]{1,0:T(8,128)(2,1)S(1)}, u32[]{:S(2)}, u32[]{:S(2)}) collective-permute-start(bf16[40,512]{1,0:T(8,128)(2,1)S(1)} %get-tuple-element.112), channel_id=1, source_target_pairs={{0,24},{4,28},{8,16},{12,20},{16,8},{20,12},{24,0},{28,4},{1,25},{... | collective-permute-start | bytes 122888 | tf_op jit(solution)/shard_map/ppermute | solution.py:422
  44.4 15.6 %collective-permute-start.25 = (bf16[40,512]{1,0:T(8,128)(2,1)S(1)}, bf16[40,512]{1,0:T(8,128)(2,1)S(1)}, u32[]{:S(2)}, u32[]{:S(2)}) collective-permute-start(bf16[40,512]{1,0:T(8,128)(2,1)S(1)} %get-tuple-element.113), channel_id=1, source_target_pairs={{0,28},{4,24},{8,20},{12,16},{16,12},{20,8},{24,4},{28,0},{1,29},{... | collective-permute-start | bytes 122888 | tf_op jit(solution)/shard_map/ppermute | solution.py:422
  44.8 4.4 %collective-permute-start.10 = (bf16[40,512]{1,0:T(8,128)(2,1)S(1)}, bf16[40,512]{1,0:T(8,128)(2,1)S(1)}, u32[]{:S(2)}, u32[]{:S(2)}) collective-permute-start(bf16[40,512]{1,0:T(8,128)(2,1)S(1)} %get-tuple-element.90), channel_id=1, source_target_pairs={{0,4},{4,0},{8,12},{12,8},{16,20},{20,16},{24,28},{28,24},{1,5},{5... | collective-permute-start | bytes 122888 | tf_op jit(solution)/shard_map/ppermute | solution.py:422
  49.1 4.4 %collective-permute-start.11 = (bf16[40,512]{1,0:T(8,128)(2,1)S(1)}, bf16[40,512]{1,0:T(8,128)(2,1)S(1)}, u32[]{:S(2)}, u32[]{:S(2)}) collective-permute-start(bf16[40,512]{1,0:T(8,128)(2,1)S(1)} %get-tuple-element.91), channel_id=1, source_target_pairs={{0,8},{4,12},{8,0},{12,4},{16,24},{20,28},{24,16},{28,20},{1,9},{5... | collective-permute-start | bytes 122888 | tf_op jit(solution)/shard_map/ppermute | solution.py:422
  53.5 4.9 %collective-permute-start.12 = (bf16[40,512]{1,0:T(8,128)(2,1)S(1)}, bf16[40,512]{1,0:T(8,128)(2,1)S(1)}, u32[]{:S(2)}, u32[]{:S(2)}) collective-permute-start(bf16[40,512]{1,0:T(8,128)(2,1)S(1)} %get-tuple-element.92), channel_id=1, source_target_pairs={{0,12},{4,8},{8,4},{12,0},{16,28},{20,24},{24,20},{28,16},{1,13},{... | collective-permute-start | bytes 122888 | tf_op jit(solution)/shard_map/ppermute | solution.py:422
  58.4 5.3 %collective-permute-start.13 = (bf16[160,512]{1,0:T(8,128)(2,1)S(1)}, bf16[160,512]{1,0:T(8,128)(2,1)S(1)}, u32[]{:S(2)}, u32[]{:S(2)}) collective-permute-start(bf16[160,512]{1,0:T(8,128)(2,1)S(1)} %constant_dynamic-update-slice_fusion.refs_1_.own_ref), channel_id=1, source_target_pairs={{0,2},{1,3},{2,0},{3,1},{4,6},{5,7},{6,4},{7,5},{8,10},{9,11},{10,... | collective-permute-start | bytes 491528 | tf_op jit(solution)/shard_map/ppermute | solution.py:422
  60.0 5.5 %collective-permute-start.26 = (bf16[160,512]{1,0:T(8,128)(2,1)S(1)}, bf16[160,512]{1,0:T(8,128)(2,1)S(1)}, u32[]{:S(2)}, u32[]{:S(2)}) collective-permute-start(bf16[160,512]{1,0:T(8,128)(2,1)S(1)} %constant_dynamic-update-slice_fusion.4.refs_1_.own_ref), channel_id=1, source_target_pairs={{0,2},{1,3},{2,0},{3,1},{4,6},{5,7},{6,4},{7,5},{8,10},{9,11},{10,... | collective-permute-start | bytes 491528 | tf_op jit(solution)/shard_map/ppermute | solution.py:422
  60.6 4.9 %collective-permute-start.28 = (bf16[160,512]{1,0:T(8,128)(2,1)S(1)}, bf16[160,512]{1,0:T(8,128)(2,1)S(1)}, u32[]{:S(2)}, u32[]{:S(2)}) collective-permute-start(bf16[160,512]{1,0:T(8,128)(2,1)S(1)} %constant_dynamic-update-slice_fusion.4.refs_1_.own_ref), channel_id=1, source_target_pairs={{0,1},{1,0},{2,3},{3,2},{4,5},{5,4},{6,7},{7,6},{8,9},{9,8},{10,11... | collective-permute-start | bytes 491528 | tf_op jit(solution)/shard_map/ppermute | solution.py:422
  60.6 6.1 %collective-permute-start.15 = (bf16[160,512]{1,0:T(8,128)(2,1)S(1)}, bf16[160,512]{1,0:T(8,128)(2,1)S(1)}, u32[]{:S(2)}, u32[]{:S(2)}) collective-permute-start(bf16[160,512]{1,0:T(8,128)(2,1)S(1)} %constant_dynamic-update-slice_fusion.refs_1_.own_ref), channel_id=1, source_target_pairs={{0,1},{1,0},{2,3},{3,2},{4,5},{5,4},{6,7},{7,6},{8,9},{9,8},{10,11... | collective-permute-start | bytes 491528 | tf_op jit(solution)/shard_map/ppermute | solution.py:422
  63.8 4.0 %collective-permute-start.14 = (bf16[160,512]{1,0:T(8,128)(2,1)S(1)}, bf16[160,512]{1,0:T(8,128)(2,1)S(1)}, u32[]{:S(2)}, u32[]{:S(2)}) collective-permute-start(bf16[160,512]{1,0:T(8,128)(2,1)S(1)} %collective-permute-done.13.refs_1_), channel_id=1, source_target_pairs={{0,1},{1,0},{2,3},{3,2},{4,5},{5,4},{6,7},{7,6},{8,9},{9,8},{10,11... | collective-permute-start | bytes 491528 | tf_op jit(solution)/shard_map/ppermute | solution.py:422
  65.5 6.3 %collective-permute-start.27 = (bf16[160,512]{1,0:T(8,128)(2,1)S(1)}, bf16[160,512]{1,0:T(8,128)(2,1)S(1)}, u32[]{:S(2)}, u32[]{:S(2)}) collective-permute-start(bf16[160,512]{1,0:T(8,128)(2,1)S(1)} %collective-permute-done.26.refs_1_), channel_id=1, source_target_pairs={{0,1},{1,0},{2,3},{3,2},{4,5},{5,4},{6,7},{7,6},{8,9},{9,8},{10,11... | collective-permute-start | bytes 491528 | tf_op jit(solution)/shard_map/ppermute | solution.py:422
  66.6 2.2 %copy-start.2 = (bf16[1,1024,2048]{2,1,0:T(8,128)(2,1)S(1)}, bf16[1,1024,2048]{2,1,0:T(8,128)(2,1)}, u32[]{:S(2)}) copy-start(bf16[1,1024,2048]{2,1,0:T(8,128)(2,1)} %lower_ref.3) | copy-start | bytes 12582916
  66.7 2.3 %copy-start.5 = (bf16[128,2048]{1,0:T(8,128)(2,1)S(1)}, bf16[128,2048]{1,0:T(8,128)(2,1)}, u32[]{:S(2)}) copy-start(bf16[128,2048]{1,0:T(8,128)(2,1)} %cl_ref.3) | copy-start | bytes 1572868
  71.2 4.7 %collective-permute-start.17 = (bf16[160,512]{1,0:T(8,128)(2,1)S(1)}, bf16[160,512]{1,0:T(8,128)(2,1)S(1)}, u32[]{:S(2)}, u32[]{:S(2)}) collective-permute-start(bf16[160,512]{1,0:T(8,128)(2,1)S(1)} %get-tuple-element.109), channel_id=1, source_target_pairs={{0,1},{1,0},{2,3},{3,2},{4,5},{5,4},{6,7},{7,6},{8,9},{9,8},{10,11... | collective-permute-start | bytes 491528 | tf_op jit(solution)/shard_map/ppermute | solution.py:422
  74.0 3.5 %collective-permute-start.30 = (bf16[160,512]{1,0:T(8,128)(2,1)S(1)}, bf16[160,512]{1,0:T(8,128)(2,1)S(1)}, u32[]{:S(2)}, u32[]{:S(2)}) collective-permute-start(bf16[160,512]{1,0:T(8,128)(2,1)S(1)} %get-tuple-element.130), channel_id=1, source_target_pairs={{0,1},{1,0},{2,3},{3,2},{4,5},{5,4},{6,7},{7,6},{8,9},{9,8},{10,11... | collective-permute-start | bytes 491528 | tf_op jit(solution)/shard_map/ppermute | solution.py:422
  74.1 9.9 %collective-permute-start.29 = (bf16[160,512]{1,0:T(8,128)(2,1)S(1)}, bf16[160,512]{1,0:T(8,128)(2,1)S(1)}, u32[]{:S(2)}, u32[]{:S(2)}) collective-permute-start(bf16[160,512]{1,0:T(8,128)(2,1)S(1)} %get-tuple-element.128), channel_id=1, source_target_pairs={{0,1},{1,0},{2,3},{3,2},{4,5},{5,4},{6,7},{7,6},{8,9},{9,8},{10,11... | collective-permute-start | bytes 491528 | tf_op jit(solution)/shard_map/ppermute | solution.py:422
  74.6 3.6 %collective-permute-start.16 = (bf16[160,512]{1,0:T(8,128)(2,1)S(1)}, bf16[160,512]{1,0:T(8,128)(2,1)S(1)}, u32[]{:S(2)}, u32[]{:S(2)}) collective-permute-start(bf16[160,512]{1,0:T(8,128)(2,1)S(1)} %get-tuple-element.107), channel_id=1, source_target_pairs={{0,1},{1,0},{2,3},{3,2},{4,5},{5,4},{6,7},{7,6},{8,9},{9,8},{10,11... | collective-permute-start | bytes 491528 | tf_op jit(solution)/shard_map/ppermute | solution.py:422
  75.3 30.8 %copy-start.15 = (f32[512]{0:T(512)S(1)}, f32[512]{0:T(512)}, u32[]{:S(2)}) copy-start(f32[512]{0:T(512)} %param.41) | copy-start | bytes 6148
  75.9 7.1 %collective-permute-start.18 = (bf16[160,512]{1,0:T(8,128)(2,1)S(1)}, bf16[160,512]{1,0:T(8,128)(2,1)S(1)}, u32[]{:S(2)}, u32[]{:S(2)}) collective-permute-start(bf16[160,512]{1,0:T(8,128)(2,1)S(1)} %add_convert_fusion.3), channel_id=1, source_target_pairs={{0,2},{1,3},{2,0},{3,1},{4,6},{5,7},{6,4},{7,5},{8,10},{9,11},{10,... | collective-permute-start | bytes 491528 | tf_op jit(solution)/shard_map/ppermute | solution.py:422
  77.5 8.5 %collective-permute-start.31 = (bf16[160,512]{1,0:T(8,128)(2,1)S(1)}, bf16[160,512]{1,0:T(8,128)(2,1)S(1)}, u32[]{:S(2)}, u32[]{:S(2)}) collective-permute-start(bf16[160,512]{1,0:T(8,128)(2,1)S(1)} %add_convert_fusion.1), channel_id=1, source_target_pairs={{0,2},{1,3},{2,0},{3,1},{4,6},{5,7},{6,4},{7,5},{8,10},{9,11},{10,... | collective-permute-start | bytes 491528 | tf_op jit(solution)/shard_map/ppermute | solution.py:422
  83.2 8.9 %collective-permute-start.19 = (bf16[40,512]{1,0:T(8,128)(2,1)S(1)}, bf16[40,512]{1,0:T(8,128)(2,1)S(1)}, u32[]{:S(2)}, u32[]{:S(2)}) collective-permute-start(bf16[40,512]{1,0:T(8,128)(2,1)S(1)} %get-tuple-element.139), channel_id=1, source_target_pairs={{0,4},{4,0},{8,12},{12,8},{16,20},{20,16},{24,28},{28,24},{1,5},{5... | collective-permute-start | bytes 122888 | tf_op jit(solution)/shard_map/ppermute | solution.py:422
  86.1 10.0 %collective-permute-start.32 = (bf16[40,512]{1,0:T(8,128)(2,1)S(1)}, bf16[40,512]{1,0:T(8,128)(2,1)S(1)}, u32[]{:S(2)}, u32[]{:S(2)}) collective-permute-start(bf16[40,512]{1,0:T(8,128)(2,1)S(1)} %get-tuple-element.136), channel_id=1, source_target_pairs={{0,16},{4,20},{8,24},{12,28},{16,0},{20,4},{24,8},{28,12},{1,17},{... | collective-permute-start | bytes 122888 | tf_op jit(solution)/shard_map/ppermute | solution.py:422
  87.7 7.6 %collective-permute-start.20 = (bf16[40,512]{1,0:T(8,128)(2,1)S(1)}, bf16[40,512]{1,0:T(8,128)(2,1)S(1)}, u32[]{:S(2)}, u32[]{:S(2)}) collective-permute-start(bf16[40,512]{1,0:T(8,128)(2,1)S(1)} %get-tuple-element.138), channel_id=1, source_target_pairs={{0,8},{4,12},{8,0},{12,4},{16,24},{20,28},{24,16},{28,20},{1,9},{5... | collective-permute-start | bytes 122888 | tf_op jit(solution)/shard_map/ppermute | solution.py:422
  89.9 6.2 %collective-permute-start.21 = (bf16[40,512]{1,0:T(8,128)(2,1)S(1)}, bf16[40,512]{1,0:T(8,128)(2,1)S(1)}, u32[]{:S(2)}, u32[]{:S(2)}) collective-permute-start(bf16[40,512]{1,0:T(8,128)(2,1)S(1)} %get-tuple-element.137), channel_id=1, source_target_pairs={{0,12},{4,8},{8,4},{12,0},{16,28},{20,24},{24,20},{28,16},{1,13},{... | collective-permute-start | bytes 122888 | tf_op jit(solution)/shard_map/ppermute | solution.py:422
  90.6 6.2 %collective-permute-start.33 = (bf16[40,512]{1,0:T(8,128)(2,1)S(1)}, bf16[40,512]{1,0:T(8,128)(2,1)S(1)}, u32[]{:S(2)}, u32[]{:S(2)}) collective-permute-start(bf16[40,512]{1,0:T(8,128)(2,1)S(1)} %get-tuple-element.135), channel_id=1, source_target_pairs={{0,20},{4,16},{8,28},{12,24},{16,4},{20,0},{24,12},{28,8},{1,21},{... | collective-permute-start | bytes 122888 | tf_op jit(solution)/shard_map/ppermute | solution.py:422
  92.1 5.8 %collective-permute-start.34 = (bf16[40,512]{1,0:T(8,128)(2,1)S(1)}, bf16[40,512]{1,0:T(8,128)(2,1)S(1)}, u32[]{:S(2)}, u32[]{:S(2)}) collective-permute-start(bf16[40,512]{1,0:T(8,128)(2,1)S(1)} %get-tuple-element.134), channel_id=1, source_target_pairs={{0,24},{4,28},{8,16},{12,20},{16,8},{20,12},{24,0},{28,4},{1,25},{... | collective-permute-start | bytes 122888 | tf_op jit(solution)/shard_map/ppermute | solution.py:422
  95.2 6.7 %collective-permute-start.35 = (bf16[40,512]{1,0:T(8,128)(2,1)S(1)}, bf16[40,512]{1,0:T(8,128)(2,1)S(1)}, u32[]{:S(2)}, u32[]{:S(2)}) collective-permute-start(bf16[40,512]{1,0:T(8,128)(2,1)S(1)} %get-tuple-element.133), channel_id=1, source_target_pairs={{0,28},{4,24},{8,20},{12,16},{16,12},{20,8},{24,4},{28,0},{1,29},{... | collective-permute-start | bytes 122888 | tf_op jit(solution)/shard_map/ppermute | solution.py:422
  102.3 3.1 %collective-permute-start.36 = (f32[2,128]{1,0:T(2,128)S(1)}, f32[2,128]{1,0:T(2,128)S(1)}, u32[]{:S(2)}, u32[]{:S(2)}) collective-permute-start(f32[2,128]{1,0:T(2,128)S(1)} %pad_maximum_fusion), channel_id=1, source_target_pairs={{0,3},{1,2},{2,1},{3,0},{4,7},{5,6},{6,5},{7,4},{8,11},{9,10},{10,... | collective-permute-start | bytes 3080 | tf_op jit(solution)/shard_map/ppermute | solution.py:422
  102.4 3.6 %collective-permute-start.37 = (f32[2,128]{1,0:T(2,128)S(1)}, f32[2,128]{1,0:T(2,128)S(1)}, u32[]{:S(2)}, u32[]{:S(2)}) collective-permute-start(f32[2,128]{1,0:T(2,128)S(1)} %pad_maximum_fusion), channel_id=1, source_target_pairs={{0,2},{1,3},{2,0},{3,1},{4,6},{5,7},{6,4},{7,5},{8,10},{9,11},{10,... | collective-permute-start | bytes 3080 | tf_op jit(solution)/shard_map/ppermute | solution.py:422
  104.0 2.0 %collective-permute-start.38 = (f32[2,128]{1,0:T(2,128)S(1)}, f32[2,128]{1,0:T(2,128)S(1)}, u32[]{:S(2)}, u32[]{:S(2)}) collective-permute-start(f32[2,128]{1,0:T(2,128)S(1)} %pad_maximum_fusion), channel_id=1, source_target_pairs={{0,1},{1,0},{2,3},{3,2},{4,5},{5,4},{6,7},{7,6},{8,9},{9,8},{10,11... | collective-permute-start | bytes 3080 | tf_op jit(solution)/shard_map/ppermute | solution.py:422
